TPU v7x, 128 devices: a whole 4x4x4 slice. The times are simulated.
128 devices in a mesh: rep: 2 (over z_hi), fs: 32 (over z_lo, y, x), tp: 2 (over core).
Axes of the slice: x: 4, y: 4, z: 4 (z_hi: 2, z_lo: 2; z = z_hi * 2 + z_lo), core: 2. Of those that a mesh axis runs over, the one named last changes fastest.
Arguments:
- tokens: bfloat16 [65536, 2048], P(('rep', 'fs'), 'tp'), may hold values from -6 to 6
- attention_pre_gain: float32 [2048], replicated, may hold values from 0.1 to 1.9
- query_matrix: bfloat16 [2048, 512], P('fs', 'tp'), may hold values from -0.125 to 0.125
- key_matrix: bfloat16 [2048, 512], P('fs', 'tp'), may hold values from -0.125 to 0.125
- value_matrix: bfloat16 [2048, 1024], P('fs', 'tp'), may hold values from -0.125 to 0.125
- decay_first_weight: bfloat16 [2048, 16], replicated, may hold values from -0.125 to 0.125
- decay_second_weight: bfloat16 [16, 512], P(None, 'tp'), may hold values from -1.5 to 1.5
- decay_offset_bias: float32 [512], P('tp'), may hold values from 0 to 6
- extra_log_surge: float32 [65536, 2], P(('rep', 'fs'), 'tp'), may hold values from -0.7 to 0
- readout_head_gain: float32 [512], replicated, may hold values from 0.1 to 1.9
- output_matrix: bfloat16 [1024, 2048], P('tp', 'fs'), may hold values from -2.4375 to 2.4375
- attention_post_gain: float32 [2048], P('tp'), may hold values from 0.1 to 1.9
- feedforward_pre_gain: float32 [2048], replicated, may hold values from 0.1 to 1.9
- up_matrix: bfloat16 [2048, 4096], P('fs', 'tp'), may hold values from -0.125 to 0.125
- down_matrix: bfloat16 [4096, 2048], P('tp', 'fs'), may hold values from -1.21875 to 1.21875
- feedforward_post_gain: float32 [2048], P('tp'), may hold values from 0.1 to 1.9
Outputs:
- layer_out: bfloat16 [65536, 2048], P(('rep', 'fs'), 'tp')
All inputs are finite; a program needn't handle non-finite values.
Results may differ from a plain program's by a relative error of at most 0.017.
Values may be sent and summed in bfloat16 or wider, within the bound.
No kernel may reach another device: no remote copies, remote signals or barrier semaphores. Data moves between devices by JAX's collectives and lax.ppermute only.
A program may use at most 128 MiB of HBM per device.

v0:
```python
import jax
import jax.numpy as jnp
import numpy as np
from jax import lax
from jax.experimental import pallas as pl
from jax.experimental.pallas import tpu as pltpu
from jax.sharding import Mesh
from jax.sharding import PartitionSpec as P


FS = ("fs_0", "fs_1", "fs_2")
REP_FS = ("rep", "fs_0", "fs_1", "fs_2")
ALL = ("rep", "fs_0", "fs_1", "fs_2", "tp")
EPS = 1e-06
CHUNK = 256
HALF = 32
BF = jnp.bfloat16
F32 = jnp.float32


CLASSES = (("x", 1), ("y", 1), ("z", 1), ("x", 3), ("y", 3), ("z", 3))


def link_class(step, chain, core):
    return CLASSES[(step + 2 * chain + core) % 6]


def partner_pairs(step, chain):
    pairs = []
    for z in range(4):
        for y in range(4):
            for x in range(4):
                for core in range(2):
                    axis, flip = link_class(step, chain, core)
                    to = {"x": x, "y": y, "z": z}
                    to[axis] ^= flip
                    source = ((z * 4 + y) * 4 + x) * 2 + core
                    target = ((to["z"] * 4 + to["y"]) * 4 + to["x"]) * 2 + core
                    pairs.append((source, target))
    return pairs


def row_block(z, y, x):
    return (((z & 1) * 16 + y * 4 + x) << 1) | (z >> 1)


def block_offsets():
    table = np.zeros((2, 3, 64), np.int32)
    for core in range(2):
        for chain in range(3):
            for place in range(64):
                total = 0
                for step in range(6):
                    if place >> step & 1:
                        axis, flip = link_class(step, chain, core)
                        at = {"x": 0, "y": 0, "z": 0}
                        at[axis] = flip
                        total ^= row_block(at["z"], at["y"], at["x"])
                table[core, chain, place] = total
    return table


OFFSETS = block_offsets()


def swap_cores(array):
    return lax.ppermute(array, "tp", [(0, 1), (1, 0)])


def over_link(array, step, chain):
    return lax.ppermute(array, ALL, partner_pairs(step, chain))


def stacked(a, b, lane, width):
    return jnp.concatenate([a[:, lane : lane + width], b[:, lane : lane + width]], axis=0)


MERGED_STEPS = 3


def gather_chain(first, up, down, chain):
    widths = (first.shape[1], up.shape[1], down.shape[1])
    held = jnp.concatenate([first, up, down], axis=1)
    for step in range(MERGED_STEPS):
        came = over_link(held, step, chain)
        if step < MERGED_STEPS - 1:
            held = jnp.concatenate([held, came], axis=0)
    first = stacked(held, came, 0, widths[0])
    feed = stacked(held, came, widths[0], widths[1] + widths[2])
    for step in range(MERGED_STEPS, 5):
        first = jnp.concatenate([first, over_link(first, step, chain)], axis=0)
    first = [first, over_link(first, 5, chain)]
    for step in range(MERGED_STEPS, 5):
        came = over_link(feed, step, chain)
        if step < 4:
            feed = jnp.concatenate([feed, came], axis=0)
    up = stacked(feed, came, 0, widths[1])
    down = stacked(feed, came, widths[1], widths[2])
    up = [up, over_link(up, 5, chain)]
    down = [down, over_link(down, 5, chain)]
    return first, up, down


def start_pieces(table, pieces, chain, lanes, target, target_lane, sem, first_block=None):
    place = 0
    for piece in pieces:
        count = piece.shape[0] // HALF

        def one(i, carry, piece=piece, place=place):
            block = table[chain, place + i]

            def copy(to):
                pltpu.make_async_copy(
                    piece.at[pl.ds(pl.multiple_of(i * HALF, HALF), HALF), pl.ds(*lanes)],
                    target.at[
                        pl.ds(pl.multiple_of(to * HALF, HALF), HALF), pl.ds(target_lane, lanes[1])
                    ],
                    sem,
                ).start()

            if first_block is None:
                copy(block)
            else:
                to = block - first_block
                pl.when((to >= 0) & (to < 32))(lambda: copy(to))
            return carry

        lax.fori_loop(0, count, one, 0, unroll=8)
        place += count


def wait_part(target, lane, width, sem):
    part = target.at[:, pl.ds(lane, width)]
    pltpu.make_async_copy(part, part, sem).wait()


def nt_dot(a, b):
    return lax.dot_general(a, b, (((1,), (1,)), ((), ())), preferred_element_type=F32)


def tn_dot(a, b):
    return lax.dot_general(a, b, (((0,), (0,)), ((), ())), preferred_element_type=F32)


def ordered(core, own, other):
    first = core == 0
    return jnp.concatenate([jnp.where(first, own, other), jnp.where(first, other, own)], axis=1)


def norm_kernel(core, own, other, gain, first, second, bias, surge, normed_out, decay_out):
    rows = ordered(core[0], own[...], other[...]).astype(F32)
    scale = lax.rsqrt(jnp.mean(rows * rows, axis=-1, keepdims=True) + EPS)
    normed = (rows * scale * gain[...]).astype(BF)
    normed_out[...] = normed
    rank = jnp.dot(normed, first[...], preferred_element_type=F32).astype(BF)
    gate = jnp.dot(rank, second[...], preferred_element_type=F32) + bias[...]
    decay_out[...] = jax.nn.log_sigmoid(gate) / 16.0 + surge[...]


def small_level_matrices():
    i = np.arange(CHUNK)[:, None]
    t = np.arange(CHUNK)[None, :]
    mats = []
    for size in (2, 4):
        same = i // (2 * size) == t // (2 * size)
        upper_i, upper_t = i % (2 * size) >= size, t % (2 * size) >= size
        mats.append(same & ((upper_i & upper_t & (t <= i)) | (~upper_i & ~upper_t & (t > i))))
    same = i // 8 == t // 8
    mats.append(same & (t <= i))
    mats.append(same & (t > i))
    return np.concatenate(mats, axis=0)


def level_of_pairs():
    i = np.arange(CHUNK)[:, None]
    j = np.arange(CHUNK)[None, :]
    level = np.floor(np.log2(np.maximum(i ^ j, 1))).astype(np.int32)
    return np.where(j < i, level, -1).astype(np.int32)


SMALL_LEVELS = small_level_matrices()
PAIR_LEVELS = level_of_pairs()


def attention_kernel(table, normed, decay, mats, pair_level, gain, *rest):
    pieces = (rest[0:2], rest[2:4], rest[4:6])
    partial_out, w_qk, w_v, w_out, state, sems = rest[6:]
    weights = (w_qk, w_v, w_out)
    first_step = pl.program_id(0) == 0

    @pl.when(first_step)
    def _():
        for c in range(3):
            start_pieces(table, pieces[c], c, (0, 512), weights[c], 0, sems.at[c])
        state[...] = jnp.zeros_like(state)

    g = decay[...]
    g_hi = g.astype(BF)
    g_lo = (g - g_hi.astype(F32)).astype(BF)

    def summed(index):
        mat = mats[pl.ds(index * CHUNK, CHUNK), :]
        return jnp.dot(mat, g_hi, preferred_element_type=F32) + jnp.dot(
            mat, g_lo, preferred_element_type=F32
        )

    before, after = summed(2), summed(3)
    row = lax.broadcasted_iota(jnp.int32, (CHUNK, CHUNK), 0)
    spans = [jnp.where((row & 1) != 0, g, 0.0), summed(0), summed(1)]
    size = 8
    while size < CHUNK:
        b = before.reshape(CHUNK // (2 * size), 2, size, CHUNK)
        a = after.reshape(CHUNK // (2 * size), 2, size, CHUNK)
        spans.append(jnp.stack([a[:, 0], b[:, 1]], axis=1).reshape(CHUNK, CHUNK))
        low, high = b[:, 0, size - 1 :, :], b[:, 1, size - 1 :, :]
        before = jnp.stack([b[:, 0], b[:, 1] + low], axis=1).reshape(CHUNK, CHUNK)
        after = jnp.stack([a[:, 0] + high, a[:, 1]], axis=1).reshape(CHUNK, CHUNK)
        size *= 2

    @pl.when(first_step)
    def _():
        for c in range(3):
            wait_part(weights[c], 0, 512, sems.at[c])

    rows = normed[...]
    qk = jnp.dot(rows, w_qk[...], preferred_element_type=F32).astype(BF).astype(F32)
    q, k = qk[:, :256] * (256**-0.5), qk[:, 256:]
    v = jnp.dot(rows, w_v[...], preferred_element_type=F32).astype(BF)
    level_map = pair_level[...]
    scores = jnp.zeros((CHUNK, CHUNK), F32)
    for level, span in enumerate(spans):
        both = (jnp.where((row & (1 << level)) != 0, q, k) * jnp.exp(span)).astype(BF)
        scores = jnp.where(level_map == level, nt_dot(both, both), scores)
    q_in = (q * jnp.exp(before)).astype(BF)
    k_out = (k * jnp.exp(after)).astype(BF)
    old = state[...]
    readout = (
        nt_dot(q_in, old.astype(BF))
        + jnp.dot(scores.astype(BF), v, preferred_element_type=F32)
        + jnp.sum(q * k, axis=1, keepdims=True) * v.astype(F32)
    )
    state[...] = old * jnp.exp(before[CHUNK - 1 :, :]) + tn_dot(v, k_out)
    scale = lax.rsqrt(jnp.mean(readout * readout, axis=-1, keepdims=True) + EPS)
    mixed = (readout * scale * gain[...]).astype(BF)
    partial_out[...] = nt_dot(mixed, w_out[...]).astype(BF)


UP_WIDTHS = (768, 640, 640)
DOWN_WIDTHS = (640, 640, 768)


def start_of(widths, chain):
    return sum(widths[:chain])


def up_kernel(
    core, table, own, other, mine, theirs, post_gain, pre_gain, *rest
):
    pieces = [rest[2 * c : 2 * c + 2] for c in range(3)]
    resid_out, squared_out, weight, sems = rest[6:]
    first_step = pl.program_id(0) == 0

    @pl.when(first_step)
    def _():
        for c in range(3):
            start_pieces(
                table, pieces[c], c, (0, UP_WIDTHS[c]), weight, start_of(UP_WIDTHS, c), sems.at[c]
            )

    rows = ordered(core[0], own[...], other[...]).astype(F32)
    attn = mine[...].astype(F32) + theirs[...].astype(F32)
    scale = lax.rsqrt(jnp.mean(attn * attn, axis=-1, keepdims=True) + EPS)
    resid = (rows + attn * scale * post_gain[...]).astype(BF)
    resid_out[...] = resid
    values = resid.astype(F32)
    scale = lax.rsqrt(jnp.mean(values * values, axis=-1, keepdims=True) + EPS)
    normed = (values * scale * pre_gain[...]).astype(BF)
    for c in range(3):
        at, width = start_of(UP_WIDTHS, c), UP_WIDTHS[c]

        @pl.when(first_step)
        def _(at=at, width=width, c=c):
            wait_part(weight, at, width, sems.at[c])

        hidden = jnp.dot(normed, weight[:, at : at + width], preferred_element_type=F32)
        hidden = jnp.maximum(hidden, 0.0)
        squared_out[:, at : at + width] = (hidden * hidden).astype(BF)


def down_kernel(table, side, squared, *rest):
    pieces = [rest[2 * c : 2 * c + 2] for c in range(3)]
    partial_out, weight, sems = rest[6:]

    @pl.when(pl.program_id(0) == 0)
    def _():
        for c in range(3):
            at, width = start_of(DOWN_WIDTHS, c), DOWN_WIDTHS[c]
            start_pieces(
                table, pieces[c], c, (0, width), weight, at, sems.at[c], side[0] * 32
            )
        for c in range(3):
            wait_part(weight, start_of(DOWN_WIDTHS, c), DOWN_WIDTHS[c], sems.at[c])

    partial_out[...] = nt_dot(squared[...], weight[...]).astype(BF)


SMEM = pl.BlockSpec(memory_space=pltpu.SMEM)
HBM = pl.BlockSpec(memory_space=pltpu.HBM)


def whole(shape):
    return pl.BlockSpec(shape, lambda i: (0,) * len(shape))


def rows_of(count, width):
    return pl.BlockSpec((count, width), lambda i: (i, 0))


def params(flops, nbytes, vmem_mib):
    return dict(
        compiler_params=pltpu.CompilerParams(
            dimension_semantics=("arbitrary",), vmem_limit_bytes=vmem_mib * 1024 * 1024
        ),
        cost_estimate=pl.CostEstimate(flops=flops, bytes_accessed=nbytes, transcendentals=0),
    )


def on_device(
    tokens,
    attention_pre_gain,
    query_matrix,
    key_matrix,
    value_matrix,
    decay_first_weight,
    decay_second_weight,
    decay_offset_bias,
    extra_log_surge,
    readout_head_gain,
    output_matrix,
    attention_post_gain,
    feedforward_pre_gain,
    up_matrix,
    down_matrix,
    feedforward_post_gain,
):
    length = tokens.shape[0]
    rep, core = lax.axis_index("rep"), lax.axis_index("tp")
    fs = lax.axis_index(FS)
    mine = fs * 2 + rep
    core_in = core.astype(jnp.int32).reshape(1)
    table = jnp.asarray(OFFSETS)[core] ^ mine.astype(jnp.int32)

    def half(shard):
        return lax.dynamic_slice_in_dim(shard, rep * HALF, HALF, axis=0)

    firsts = (
        jnp.concatenate([half(query_matrix), half(key_matrix)], axis=1),
        half(value_matrix),
        half(output_matrix.T),
    )
    up, down = half(up_matrix), half(down_matrix.T)
    gathered = []
    for c in range(3):
        a, b = start_of(UP_WIDTHS, c), start_of(DOWN_WIDTHS, c)
        gathered.append(
            gather_chain(
                firsts[c], up[:, a : a + UP_WIDTHS[c]], down[:, b : b + DOWN_WIDTHS[c]], c
            )
        )
    (qk, up_0, down_0), (v, up_1, down_1), (out_w, up_2, down_2) = gathered
    up_w = [*up_0, *up_1, *up_2]
    down_w = [*down_0, *down_1, *down_2]

    other = swap_cores(tokens)
    block = 256
    grid = (length // block,)
    normed, decay = pl.pallas_call(
        norm_kernel,
        grid=grid,
        in_specs=[
            SMEM,
            rows_of(block, 1024),
            rows_of(block, 1024),
            whole((1, 2048)),
            whole((2048, 16)),
            whole((16, 256)),
            whole((1, 256)),
            rows_of(block, 1),
        ],
        out_specs=[rows_of(block, 2048), rows_of(block, 256)],
        out_shape=[
            jax.ShapeDtypeStruct((length, 2048), BF),
            jax.ShapeDtypeStruct((length, 256), F32),
        ],
        name="norm",
        **params(400_000_000, 10_000_000, 16),
    )(
        core_in,
        tokens,
        other,
        attention_pre_gain.reshape(1, -1),
        decay_first_weight,
        decay_second_weight,
        decay_offset_bias.reshape(1, -1),
        extra_log_surge,
    )
    partial_attn = pl.pallas_call(
        attention_kernel,
        grid=(length // CHUNK,),
        in_specs=[
            SMEM,
            rows_of(CHUNK, 2048),
            rows_of(CHUNK, 256),
            whole(SMALL_LEVELS.shape),
            whole(PAIR_LEVELS.shape),
            whole((1, 512)),
        ]
        + [HBM] * 6,
        out_specs=rows_of(CHUNK, 2048),
        out_shape=jax.ShapeDtypeStruct((length, 2048), BF),
        scratch_shapes=[
            pltpu.VMEM((2048, 512), BF),
            pltpu.VMEM((2048, 512), BF),
            pltpu.VMEM((2048, 512), BF),
            pltpu.VMEM((512, 256), F32),
            pltpu.SemaphoreType.DMA((3,)),
        ],
        name="attention",
        **params(11_000_000_000, 14_000_000, 28),
    )(
        table,
        normed,
        decay,
        jnp.asarray(SMALL_LEVELS, BF),
        jnp.asarray(PAIR_LEVELS),
        readout_head_gain.reshape(1, -1),
        *qk,
        *v,
        *out_w,
    )
    other_attn = swap_cores(partial_attn)
    post_gain = lax.all_gather(attention_post_gain, "tp", tiled=True).reshape(1, -1)
    resid, squared = pl.pallas_call(
        up_kernel,
        grid=grid,
        in_specs=[
            SMEM,
            SMEM,
            rows_of(block, 1024),
            rows_of(block, 1024),
            rows_of(block, 2048),
            rows_of(block, 2048),
            whole((1, 2048)),
            whole((1, 2048)),
        ]
        + [HBM] * 6,
        out_specs=[rows_of(block, 2048), rows_of(block, 2048)],
        out_shape=[
            jax.ShapeDtypeStruct((length, 2048), BF),
            jax.ShapeDtypeStruct((length, 2048), BF),
        ],
        scratch_shapes=[pltpu.VMEM((2048, 2048), BF), pltpu.SemaphoreType.DMA((3,))],
        name="up_proj",
        **params(8_700_000_000, 28_000_000, 32),
    )(
        core_in,
        table,
        tokens,
        other,
        partial_attn,
        other_attn,
        post_gain,
        feedforward_pre_gain.reshape(1, -1),
        *up_w,
    )

    def down_half(side):
        return pl.pallas_call(
            down_kernel,
            grid=grid,
            in_specs=[SMEM, SMEM, rows_of(block, 2048)] + [HBM] * 6,
            out_specs=rows_of(block, 1024),
            out_shape=jax.ShapeDtypeStruct((length, 1024), BF),
            scratch_shapes=[pltpu.VMEM((1024, 2048), BF), pltpu.SemaphoreType.DMA((3,))],
            **params(4_300_000_000, 10_000_000, 16),
        )(table, side, squared, *down_w)

    away = down_half(1 - core_in)
    theirs = swap_cores(away)
    mine = down_half(core_in)
    feed = mine.astype(F32) + theirs.astype(F32)
    squares = jnp.sum(feed * feed, axis=1)
    squares_other = swap_cores(squares.reshape(8, 128)).reshape(length)
    scale = lax.rsqrt((squares + squares_other) / 2048 + EPS)[:, None]
    resid_own = lax.dynamic_slice_in_dim(resid, core * 1024, 1024, axis=1)
    return (resid_own.astype(F32) + feed * scale * feedforward_post_gain).astype(BF)


def solution(mesh):
    finer = Mesh(
        mesh.devices.reshape(mesh.shape["rep"], 2, 4, 4, mesh.shape["tp"]),
        ("rep", "fs_0", "fs_1", "fs_2", "tp"),
    )
    in_specs = (
        P(REP_FS, "tp"),
        P(),
        P(FS, "tp"),
        P(FS, "tp"),
        P(FS, "tp"),
        P(),
        P(None, "tp"),
        P("tp"),
        P(REP_FS, "tp"),
        P(),
        P("tp", FS),
        P("tp"),
        P(),
        P(FS, "tp"),
        P("tp", FS),
        P("tp"),
    )

    return jax.shard_map(
        on_device, mesh=finer, in_specs=in_specs, out_specs=P(REP_FS, "tp"), check_vma=False
    )
```

profile of v0, /device:TPU:1, one launch (start us, length us, event | category | flops | bytes accessed | tf_op | source)
XLA Modules:
  0.0 218.0 jit_solution(13004710354628010380)
XLA Ops:
  2.5 2.2 %collective-permute-start.1 = (bf16[32,1920]{1,0:T(8,128)(2,1)S(1)}, bf16[32,1920]{1,0:T(8,128)(2,1)S(1)}, u32[]{:S(2)}, u32[]{:S(2)}) collective-permute-start(bf16[32,1920]{1,0:T(8,128)(2,1)S(1)} %pad_maximum_fusion.27), channel_id=1, source_target_pairs={{0,2},{1,9},{2,0},{3,11},{4,6},{5,13},{6,4},{7,15},{8,10},{9,1},{1... | collective-permute-start | bytes 368648 | tf_op jit(solution)/shard_map/ppermute | solution.py:71
  6.3 2.6 %collective-permute-start.7 = (bf16[32,1792]{1,0:T(8,128)(2,1)S(1)}, bf16[32,1792]{1,0:T(8,128)(2,1)S(1)}, u32[]{:S(2)}, u32[]{:S(2)}) collective-permute-start(bf16[32,1792]{1,0:T(8,128)(2,1)S(1)} %pad_maximum_fusion.29), channel_id=1, source_target_pairs={{0,32},{1,7},{2,34},{3,5},{4,36},{5,3},{6,38},{7,1},{8,40},{9,15},... | collective-permute-start | bytes 344072 | tf_op jit(solution)/shard_map/ppermute | solution.py:71
  9.7 3.8 %collective-permute-start.13 = (bf16[32,1920]{1,0:T(8,128)(2,1)S(1)}, bf16[32,1920]{1,0:T(8,128)(2,1)S(1)}, u32[]{:S(2)}, u32[]{:S(2)}) collective-permute-start(bf16[32,1920]{1,0:T(8,128)(2,1)S(1)} %pad_maximum_fusion.28), channel_id=1, source_target_pairs={{0,24},{1,97},{2,26},{3,99},{4,28},{5,101},{6,30},{7,103},{8,16},{... | collective-permute-start | bytes 368648 | tf_op jit(solution)/shard_map/ppermute | solution.py:71
  13.5 2.0 collective-permute-start.8
  16.2 3.8 %collective-permute-done.8 = bf16[64,1792]{1,0:T(8,128)(2,1)S(1)} collective-permute-done((bf16[64,1792]{1,0:T(8,128)(2,1)S(1)}, bf16[64,1792]{1,0:T(8,128)(2,1)S(1)}, u32[]{:S(2)}, u32[]{:S(2)}) %collective-permute-start.8) | collective-permute-done | bytes 229408 | tf_op jit(solution)/shard_map/ppermute | solution.py:71
  20.0 1.6 collective-permute-start.9
  21.8 2.6 %collective-permute-start.3 = (bf16[128,1920]{1,0:T(8,128)(2,1)S(1)}, bf16[128,1920]{1,0:T(8,128)(2,1)S(1)}, u32[]{:S(2)}, u32[]{:S(2)}) collective-permute-start(bf16[128,1920]{1,0:T(8,128)(2,1)S(1)} %pad_maximum_fusion.18), channel_id=1, source_target_pairs={{0,32},{1,7},{2,34},{3,5},{4,36},{5,3},{6,38},{7,1},{8,40},{9,15},... | collective-permute-start | bytes 1474568 | tf_op jit(solution)/shard_map/ppermute | solution.py:71
  24.4 4.5 %collective-permute-done.9 = bf16[128,1792]{1,0:T(8,128)(2,1)S(1)} collective-permute-done((bf16[128,1792]{1,0:T(8,128)(2,1)S(1)}, bf16[128,1792]{1,0:T(8,128)(2,1)S(1)}, u32[]{:S(2)}, u32[]{:S(2)}) %collective-permute-start.9) | collective-permute-done | bytes 458784 | tf_op jit(solution)/shard_map/ppermute | solution.py:71
  31.9 5.6 %collective-permute-start = (bf16[1024,1024]{1,0:T(8,128)(2,1)S(1)}, bf16[1024,1024]{1,0:T(8,128)(2,1)}, u32[]{:S(2)}, u32[]{:S(2)}) collective-permute-start(bf16[1024,1024]{1,0:T(8,128)(2,1)S(1)} %copy-done.2), channel_id=1, source_target_pairs={{0,1},{1,0},{2,3},{3,2},{4,5},{5,4},{6,7},{7,6},{8,9},{9,8},{10,11... | collective-permute-start | bytes 6291464 | tf_op jit(solution)/shard_map/ppermute | solution.py:67
  39.4 5.5 %collective-permute-start.17 = (bf16[512,512]{1,0:T(8,128)(2,1)S(1)}, bf16[512,512]{1,0:T(8,128)(2,1)S(1)}, u32[]{:S(2)}, u32[]{:S(2)}) collective-permute-start(bf16[512,512]{1,0:T(8,128)(2,1)S(1)} %pad_maximum_fusion.17), channel_id=1, source_target_pairs={{0,32},{1,7},{2,34},{3,5},{4,36},{5,3},{6,38},{7,1},{8,40},{9,15},... | collective-permute-start | bytes 1572872 | tf_op jit(solution)/shard_map/ppermute | solution.py:71
  44.9 3.4 %collective-permute-start.5 = (bf16[512,512]{1,0:T(8,128)(2,1)S(1)}, bf16[512,512]{1,0:T(8,128)(2,1)S(1)}, u32[]{:S(2)}, u32[]{:S(2)}) collective-permute-start(bf16[512,512]{1,0:T(8,128)(2,1)S(1)} %pad_maximum_fusion.15), channel_id=1, source_target_pairs={{0,24},{1,97},{2,26},{3,99},{4,28},{5,101},{6,30},{7,103},{8,16},{... | collective-permute-start | bytes 1572872 | tf_op jit(solution)/shard_map/ppermute | solution.py:71
  49.4 2.2 collective-permute-start.12
  52.7 2.9 %collective-permute-start.18 = (bf16[1024,512]{1,0:T(8,128)(2,1)}, bf16[1024,512]{1,0:T(8,128)(2,1)}, u32[]{:S(2)}, u32[]{:S(2)}) collective-permute-start(bf16[1024,512]{1,0:T(8,128)(2,1)} %pad_maximum_fusion.11.rest_4_), channel_id=1, source_target_pairs={{0,6},{1,25},{2,4},{3,27},{4,2},{5,29},{6,0},{7,31},{8,14},{9,17},... | collective-permute-start | bytes 3145736 | tf_op jit(solution)/shard_map/ppermute | solution.py:71
  63.5 5.1 %norm.1 = (bf16[1024,2048]{1,0:T(8,128)(2,1)S(1)}, f32[1024,256]{1,0:T(8,128)S(1)}) custom-call(s32[1]{0:T(128)} %bitcast.core.side, bf16[1024,1024]{1,0:T(8,128)(2,1)S(1)} %copy-done.2, bf16[1024,1024]{1,0:T(8,128)(2,1)} %collective-permute-done.other, f32[1,2048]{1,0:T(1,128)S(1)} %bitcast.21, bf16[2048,16]{1,0:T(8,128)(2,1)S(1)} %copy.22.first, ...), custom_call_target="tpu_custom_call" | custom-call | flops 400000000 | bytes 10000000 | tf_op jit(solution)/shard_map/norm/pallas_call | solution.py:377
  70.8 15.5 %attention.1.mine = bf16[1024,2048]{1,0:T(8,128)(2,1)S(1)} custom-call(s32[3,64]{1,0:T(4,128)S(1)} %xor_bitcast_fusion.table, bf16[1024,2048]{1,0:T(8,128)(2,1)S(1)} %get-tuple-element.9.normed, f32[1024,256]{1,0:T(8,128)S(1)} %get-tuple-element.10.decay, bf16[1024,256]{1,0:T(8,128)(2,1)S(1)} %copy-done.10, s32[256,256]{1,0:T(8,128)S(1)} %copy-done.11, ...), custom_call_target="tpu_custom_call" | custom-call | flops 11000000512 | bytes 14000000 | tf_op jit(solution)/shard_map/attention/pallas_call | solution.py:407
  86.4 6.1 %collective-permute-start.19 = (bf16[1024,2048]{1,0:T(8,128)(2,1)S(1)}, bf16[1024,2048]{1,0:T(8,128)(2,1)S(1)}, u32[]{:S(2)}, u32[]{:S(2)}) collective-permute-start(bf16[1024,2048]{1,0:T(8,128)(2,1)S(1)} %attention.1.mine), channel_id=1, source_target_pairs={{0,1},{1,0},{2,3},{3,2},{4,5},{5,4},{6,7},{7,6},{8,9},{9,8},{10,11... | collective-permute-start | bytes 12582920 | tf_op jit(solution)/shard_map/ppermute | solution.py:67
  92.5 5.2 %collective-permute-start.20 = (bf16[256,1408]{1,0:T(8,128)(2,1)S(1)}, bf16[256,1408]{1,0:T(8,128)(2,1)S(1)}, u32[]{:S(2)}, u32[]{:S(2)}) collective-permute-start(bf16[256,1408]{1,0:T(8,128)(2,1)S(1)} %pad_maximum_fusion.12), channel_id=1, source_target_pairs={{0,6},{1,25},{2,4},{3,27},{4,2},{5,29},{6,0},{7,31},{8,14},{9,17},... | collective-permute-start | bytes 2162696 | tf_op jit(solution)/shard_map/ppermute | solution.py:71
  98.0 2.1 collective-permute-start.27
  100.1 6.5 %collective-permute-done.20 = bf16[256,1408]{1,0:T(8,128)(2,1)S(1)} collective-permute-done((bf16[256,1408]{1,0:T(8,128)(2,1)S(1)}, bf16[256,1408]{1,0:T(8,128)(2,1)S(1)}, u32[]{:S(2)}, u32[]{:S(2)}) %collective-permute-start.20) | collective-permute-done | bytes 720928 | tf_op jit(solution)/shard_map/ppermute | solution.py:71
  106.8 1.7 collective-permute-start.21
  108.7 5.9 %collective-permute-done.24 = bf16[512,1280]{1,0:T(8,128)(2,1)S(1)} collective-permute-done((bf16[512,1280]{1,0:T(8,128)(2,1)S(1)}, bf16[512,1280]{1,0:T(8,128)(2,1)S(1)}, u32[]{:S(2)}, u32[]{:S(2)}) %collective-permute-start.24) | collective-permute-done | bytes 1310752 | tf_op jit(solution)/shard_map/ppermute | solution.py:71
  114.9 6.2 %collective-permute-done.27 = bf16[512,1408]{1,0:T(8,128)(2,1)S(1)} collective-permute-done((bf16[512,1408]{1,0:T(8,128)(2,1)S(1)}, bf16[512,1408]{1,0:T(8,128)(2,1)S(1)}, u32[]{:S(2)}, u32[]{:S(2)}) %collective-permute-start.27) | collective-permute-done | bytes 1441824 | tf_op jit(solution)/shard_map/ppermute | solution.py:71
  121.3 4.1 %collective-permute-start.28 = (bf16[1024,640]{1,0:T(8,128)(2,1)S(1)}, bf16[1024,640]{1,0:T(8,128)(2,1)S(1)}, u32[]{:S(2)}, u32[]{:S(2)}) collective-permute-start(bf16[1024,640]{1,0:T(8,128)(2,1)S(1)} %pad_maximum_fusion.6.rest_4_), channel_id=1, source_target_pairs={{0,6},{1,25},{2,4},{3,27},{4,2},{5,29},{6,0},{7,31},{8,14},{9,17},... | collective-permute-start | bytes 3932168 | tf_op jit(solution)/shard_map/ppermute | solution.py:71
  127.5 2.8 %collective-permute-start.31 = (bf16[1024,768]{1,0:T(8,128)(2,1)S(1)}, bf16[1024,768]{1,0:T(8,128)(2,1)S(1)}, u32[]{:S(2)}, u32[]{:S(2)}) collective-permute-start(bf16[1024,768]{1,0:T(8,128)(2,1)S(1)} %pad_maximum_fusion.1.rest_4_), channel_id=1, source_target_pairs={{0,6},{1,25},{2,4},{3,27},{4,2},{5,29},{6,0},{7,31},{8,14},{9,17},... | collective-permute-start | bytes 4718600 | tf_op jit(solution)/shard_map/ppermute | solution.py:71
  131.7 17.3 %collective-permute-done.28.rest_5_ = bf16[1024,640]{1,0:T(8,128)(2,1)S(1)} collective-permute-done((bf16[1024,640]{1,0:T(8,128)(2,1)S(1)}, bf16[1024,640]{1,0:T(8,128)(2,1)S(1)}, u32[]{:S(2)}, u32[]{:S(2)}) %collective-permute-start.28) | collective-permute-done | bytes 1310752 | tf_op jit(solution)/shard_map/ppermute | solution.py:71
  149.0 1.8 all_gather.3
  150.9 2.0 copy-done.27
  152.9 24.1 %up_proj.1 = (bf16[1024,2048]{1,0:T(8,128)(2,1)S(1)}, bf16[1024,2048]{1,0:T(8,128)(2,1)S(1)}) custom-call(s32[1]{0:T(128)} %bitcast.core.side, s32[3,64]{1,0:T(4,128)S(1)} %xor_bitcast_fusion.table, bf16[1024,1024]{1,0:T(8,128)(2,1)S(1)} %copy-done.2, bf16[1024,1024]{1,0:T(8,128)(2,1)} %collective-permute-done.other, bf16[1024,2048]{1,0:T(8,128)(2,1)} %copy-done.7, ...), custom_call_target="tpu_custom_call" | custom-call | flops 8700000256 | bytes 28000000 | tf_op jit(solution)/shard_map/up_proj/pallas_call | solution.py:443
  177.0 9.0 %shard_map.182 = bf16[1024,1024]{1,0:T(8,128)(2,1)S(1)} custom-call(s32[3,64]{1,0:T(4,128)S(1)} %xor_bitcast_fusion.table, s32[1]{0:T(128)S(6)} %sub.3.side, bf16[1024,2048]{1,0:T(8,128)(2,1)S(1)} %get-tuple-element.12.squared, bf16[1024,640]{1,0:T(8,128)(2,1)S(1)} %pad_maximum_fusion.7.rest_0_, bf16[1024,640]{1,0:T(8,128)(2,1)} %collective-permute-done.29.rest_1_, ...), custom_call_target="tpu_custom_call" | custom-call | flops 4300000256 | bytes 10000000 | tf_op jit(solution)/shard_map/pallas_call | solution.py:478
  186.0 15.0 %collective-permute-start.32 = (bf16[1024,1024]{1,0:T(8,128)(2,1)S(1)}, bf16[1024,1024]{1,0:T(8,128)(2,1)S(1)}, u32[]{:S(2)}, u32[]{:S(2)}) collective-permute-start(bf16[1024,1024]{1,0:T(8,128)(2,1)S(1)} %shard_map.182), channel_id=1, source_target_pairs={{0,1},{1,0},{2,3},{3,2},{4,5},{5,4},{6,7},{7,6},{8,9},{9,8},{10,11... | collective-permute-start | bytes 6291464 | tf_op jit(solution)/shard_map/ppermute | solution.py:67
  201.0 9.0 %shard_map.181 = bf16[1024,1024]{1,0:T(8,128)(2,1)S(1)} custom-call(s32[3,64]{1,0:T(4,128)S(1)} %xor_bitcast_fusion.table, s32[1]{0:T(128)} %bitcast.core.side, bf16[1024,2048]{1,0:T(8,128)(2,1)S(1)} %get-tuple-element.12.squared, bf16[1024,640]{1,0:T(8,128)(2,1)S(1)} %pad_maximum_fusion.7.rest_0_, bf16[1024,640]{1,0:T(8,128)(2,1)} %collective-permute-done.29.rest_1_, ...), custom_call_target="tpu_custom_call" | custom-call | flops 4300000256 | bytes 10000000 | tf_op jit(solution)/shard_map/pallas_call | solution.py:478
  213.4 4.6 %add_convert_fusion = bf16[1024,1024]{1,0:T(8,128)(2,1)} fusion(bf16[1024,1024]{1,0:T(8,128)(2,1)} %copy-done.12, bf16[1024,1024]{1,0:T(8,128)(2,1)S(1)} %shard_map.181, f32[1024]{0:T(1024)S(1)} %copy-done.23, f32[1024]{0:T(1024)S(1)} %fusion.2, bf16[1024,2048]{1,0:T(8,128)(2,1)} %copy-done.3, s32[]{:T(128)S(6)} %select_n.16), kind=kLoop, calls=%fused_computation | loop fusion | flops 8388608 | bytes 8396804 | tf_op jit(solution)/shard_map/convert_element_type | solution.py:496
  (164 shorter events, 30.5 us)
Async XLA Ops:
  2.5 13.6 %collective-permute-start.1 = (bf16[32,1920]{1,0:T(8,128)(2,1)S(1)}, bf16[32,1920]{1,0:T(8,128)(2,1)S(1)}, u32[]{:S(2)}, u32[]{:S(2)}) collective-permute-start(bf16[32,1920]{1,0:T(8,128)(2,1)S(1)} %pad_maximum_fusion.27), channel_id=1, source_target_pairs={{0,2},{1,9},{2,0},{3,11},{4,6},{5,13},{6,4},{7,15},{8,10},{9,1},{1... | collective-permute-start | bytes 368648 | tf_op jit(solution)/shard_map/ppermute | solution.py:71
  6.3 7.2 %collective-permute-start.7 = (bf16[32,1792]{1,0:T(8,128)(2,1)S(1)}, bf16[32,1792]{1,0:T(8,128)(2,1)S(1)}, u32[]{:S(2)}, u32[]{:S(2)}) collective-permute-start(bf16[32,1792]{1,0:T(8,128)(2,1)S(1)} %pad_maximum_fusion.29), channel_id=1, source_target_pairs={{0,32},{1,7},{2,34},{3,5},{4,36},{5,3},{6,38},{7,1},{8,40},{9,15},... | collective-permute-start | bytes 344072 | tf_op jit(solution)/shard_map/ppermute | solution.py:71
  9.7 6.1 %collective-permute-start.13 = (bf16[32,1920]{1,0:T(8,128)(2,1)S(1)}, bf16[32,1920]{1,0:T(8,128)(2,1)S(1)}, u32[]{:S(2)}, u32[]{:S(2)}) collective-permute-start(bf16[32,1920]{1,0:T(8,128)(2,1)S(1)} %pad_maximum_fusion.28), channel_id=1, source_target_pairs={{0,24},{1,97},{2,26},{3,99},{4,28},{5,101},{6,30},{7,103},{8,16},{... | collective-permute-start | bytes 368648 | tf_op jit(solution)/shard_map/ppermute | solution.py:71
  13.5 6.5 %collective-permute-start.8 = (bf16[64,1792]{1,0:T(8,128)(2,1)S(1)}, bf16[64,1792]{1,0:T(8,128)(2,1)S(1)}, u32[]{:S(2)}, u32[]{:S(2)}) collective-permute-start(bf16[64,1792]{1,0:T(8,128)(2,1)S(1)} %pad_maximum_fusion.26), channel_id=1, source_target_pairs={{0,6},{1,25},{2,4},{3,27},{4,2},{5,29},{6,0},{7,31},{8,14},{9,17},... | collective-permute-start | bytes 688136 | tf_op jit(solution)/shard_map/ppermute | solution.py:71
  15.8 5.8 %collective-permute-start.14 = (bf16[64,1920]{1,0:T(8,128)(2,1)S(1)}, bf16[64,1920]{1,0:T(8,128)(2,1)S(1)}, u32[]{:S(2)}, u32[]{:S(2)}) collective-permute-start(bf16[64,1920]{1,0:T(8,128)(2,1)S(1)} %pad_maximum_fusion.25), channel_id=1, source_target_pairs={{0,96},{1,3},{2,98},{3,1},{4,100},{5,7},{6,102},{7,5},{8,104},{9,1... | collective-permute-start | bytes 737288 | tf_op jit(solution)/shard_map/ppermute | solution.py:71
  20.0 8.9 %collective-permute-start.9 = (bf16[128,1792]{1,0:T(8,128)(2,1)S(1)}, bf16[128,1792]{1,0:T(8,128)(2,1)S(1)}, u32[]{:S(2)}, u32[]{:S(2)}) collective-permute-start(bf16[128,1792]{1,0:T(8,128)(2,1)S(1)} %pad_maximum_fusion.20), channel_id=1, source_target_pairs={{0,24},{1,97},{2,26},{3,99},{4,28},{5,101},{6,30},{7,103},{8,16},{... | collective-permute-start | bytes 1376264 | tf_op jit(solution)/shard_map/ppermute | solution.py:71
  21.7 8.3 %collective-permute-start.15 = (bf16[128,1920]{1,0:T(8,128)(2,1)S(1)}, bf16[128,1920]{1,0:T(8,128)(2,1)S(1)}, u32[]{:S(2)}, u32[]{:S(2)}) collective-permute-start(bf16[128,1920]{1,0:T(8,128)(2,1)S(1)} %pad_maximum_fusion.19), channel_id=1, source_target_pairs={{0,2},{1,9},{2,0},{3,11},{4,6},{5,13},{6,4},{7,15},{8,10},{9,1},{1... | collective-permute-start | bytes 1474568 | tf_op jit(solution)/shard_map/ppermute | solution.py:71
  21.8 15.7 %collective-permute-start.3 = (bf16[128,1920]{1,0:T(8,128)(2,1)S(1)}, bf16[128,1920]{1,0:T(8,128)(2,1)S(1)}, u32[]{:S(2)}, u32[]{:S(2)}) collective-permute-start(bf16[128,1920]{1,0:T(8,128)(2,1)S(1)} %pad_maximum_fusion.18), channel_id=1, source_target_pairs={{0,32},{1,7},{2,34},{3,5},{4,36},{5,3},{6,38},{7,1},{8,40},{9,15},... | collective-permute-start | bytes 1474568 | tf_op jit(solution)/shard_map/ppermute | solution.py:71
  29.0 10.1 %collective-permute-start.10 = (bf16[256,512]{1,0:T(8,128)(2,1)S(1)}, bf16[256,512]{1,0:T(8,128)(2,1)S(1)}, u32[]{:S(2)}, u32[]{:S(2)}) collective-permute-start(bf16[256,512]{1,0:T(8,128)(2,1)S(1)} %pad_maximum_fusion.22), channel_id=1, source_target_pairs={{0,96},{1,3},{2,98},{3,1},{4,100},{5,7},{6,102},{7,5},{8,104},{9,1... | collective-permute-start | bytes 786440 | tf_op jit(solution)/shard_map/ppermute | solution.py:71
  30.7 8.6 %collective-permute-start.16 = (bf16[256,512]{1,0:T(8,128)(2,1)S(1)}, bf16[256,512]{1,0:T(8,128)(2,1)S(1)}, u32[]{:S(2)}, u32[]{:S(2)}) collective-permute-start(bf16[256,512]{1,0:T(8,128)(2,1)S(1)} %pad_maximum_fusion.23), channel_id=1, source_target_pairs={{0,8},{1,33},{2,10},{3,35},{4,12},{5,37},{6,14},{7,39},{8,0},{9,41... | collective-permute-start | bytes 786440 | tf_op jit(solution)/shard_map/ppermute | solution.py:71
  31.9 30.2 %collective-permute-start = (bf16[1024,1024]{1,0:T(8,128)(2,1)S(1)}, bf16[1024,1024]{1,0:T(8,128)(2,1)}, u32[]{:S(2)}, u32[]{:S(2)}) collective-permute-start(bf16[1024,1024]{1,0:T(8,128)(2,1)S(1)} %copy-done.2), channel_id=1, source_target_pairs={{0,1},{1,0},{2,3},{3,2},{4,5},{5,4},{6,7},{7,6},{8,9},{9,8},{10,11... | collective-permute-start | bytes 6291464 | tf_op jit(solution)/shard_map/ppermute | solution.py:67
  37.6 7.3 %collective-permute-start.4 = (bf16[256,512]{1,0:T(8,128)(2,1)S(1)}, bf16[256,512]{1,0:T(8,128)(2,1)S(1)}, u32[]{:S(2)}, u32[]{:S(2)}) collective-permute-start(bf16[256,512]{1,0:T(8,128)(2,1)S(1)} %pad_maximum_fusion.21), channel_id=1, source_target_pairs={{0,6},{1,25},{2,4},{3,27},{4,2},{5,29},{6,0},{7,31},{8,14},{9,17},... | collective-permute-start | bytes 786440 | tf_op jit(solution)/shard_map/ppermute | solution.py:71
  39.2 9.2 %collective-permute-start.11 = (bf16[512,512]{1,0:T(8,128)(2,1)S(1)}, bf16[512,512]{1,0:T(8,128)(2,1)S(1)}, u32[]{:S(2)}, u32[]{:S(2)}) collective-permute-start(bf16[512,512]{1,0:T(8,128)(2,1)S(1)} %pad_maximum_fusion.16), channel_id=1, source_target_pairs={{0,2},{1,9},{2,0},{3,11},{4,6},{5,13},{6,4},{7,15},{8,10},{9,1},{1... | collective-permute-start | bytes 1572872 | tf_op jit(solution)/shard_map/ppermute | solution.py:71
  39.4 12.3 %collective-permute-start.17 = (bf16[512,512]{1,0:T(8,128)(2,1)S(1)}, bf16[512,512]{1,0:T(8,128)(2,1)S(1)}, u32[]{:S(2)}, u32[]{:S(2)}) collective-permute-start(bf16[512,512]{1,0:T(8,128)(2,1)S(1)} %pad_maximum_fusion.17), channel_id=1, source_target_pairs={{0,32},{1,7},{2,34},{3,5},{4,36},{5,3},{6,38},{7,1},{8,40},{9,15},... | collective-permute-start | bytes 1572872 | tf_op jit(solution)/shard_map/ppermute | solution.py:71
  44.9 10.6 %collective-permute-start.5 = (bf16[512,512]{1,0:T(8,128)(2,1)S(1)}, bf16[512,512]{1,0:T(8,128)(2,1)S(1)}, u32[]{:S(2)}, u32[]{:S(2)}) collective-permute-start(bf16[512,512]{1,0:T(8,128)(2,1)S(1)} %pad_maximum_fusion.15), channel_id=1, source_target_pairs={{0,24},{1,97},{2,26},{3,99},{4,28},{5,101},{6,30},{7,103},{8,16},{... | collective-permute-start | bytes 1572872 | tf_op jit(solution)/shard_map/ppermute | solution.py:71
  49.4 19.2 %collective-permute-start.12 = (bf16[1024,512]{1,0:T(8,128)(2,1)}, bf16[1024,512]{1,0:T(8,128)(2,1)}, u32[]{:S(2)}, u32[]{:S(2)}) collective-permute-start(bf16[1024,512]{1,0:T(8,128)(2,1)} %pad_maximum_fusion.10.rest_2_), channel_id=1, source_target_pairs={{0,8},{1,33},{2,10},{3,35},{4,12},{5,37},{6,14},{7,39},{8,0},{9,41... | collective-permute-start | bytes 3145736 | tf_op jit(solution)/shard_map/ppermute | solution.py:71
  52.7 16.7 %collective-permute-start.18 = (bf16[1024,512]{1,0:T(8,128)(2,1)}, bf16[1024,512]{1,0:T(8,128)(2,1)}, u32[]{:S(2)}, u32[]{:S(2)}) collective-permute-start(bf16[1024,512]{1,0:T(8,128)(2,1)} %pad_maximum_fusion.11.rest_4_), channel_id=1, source_target_pairs={{0,6},{1,25},{2,4},{3,27},{4,2},{5,29},{6,0},{7,31},{8,14},{9,17},... | collective-permute-start | bytes 3145736 | tf_op jit(solution)/shard_map/ppermute | solution.py:71
  56.6 14.3 %collective-permute-start.6 = (bf16[1024,512]{1,0:T(8,128)(2,1)}, bf16[1024,512]{1,0:T(8,128)(2,1)}, u32[]{:S(2)}, u32[]{:S(2)}) collective-permute-start(bf16[1024,512]{1,0:T(8,128)(2,1)} %pad_maximum_fusion.9.rest_0_), channel_id=1, source_target_pairs={{0,96},{1,3},{2,98},{3,1},{4,100},{5,7},{6,102},{7,5},{8,104},{9,1... | collective-permute-start | bytes 3145736 | tf_op jit(solution)/shard_map/ppermute | solution.py:71
  60.9 36.8 %collective-permute-start.23 = (bf16[256,1280]{1,0:T(8,128)(2,1)S(1)}, bf16[256,1280]{1,0:T(8,128)(2,1)S(1)}, u32[]{:S(2)}, u32[]{:S(2)}) collective-permute-start(bf16[256,1280]{1,0:T(8,128)(2,1)S(1)} %pad_maximum_fusion.14), channel_id=1, source_target_pairs={{0,96},{1,3},{2,98},{3,1},{4,100},{5,7},{6,102},{7,5},{8,104},{9,1... | collective-permute-start | bytes 1966088 | tf_op jit(solution)/shard_map/ppermute | solution.py:71
  62.1 35.7 %collective-permute-start.26 = (bf16[256,1408]{1,0:T(8,128)(2,1)S(1)}, bf16[256,1408]{1,0:T(8,128)(2,1)S(1)}, u32[]{:S(2)}, u32[]{:S(2)}) collective-permute-start(bf16[256,1408]{1,0:T(8,128)(2,1)S(1)} %pad_maximum_fusion.13), channel_id=1, source_target_pairs={{0,8},{1,33},{2,10},{3,35},{4,12},{5,37},{6,14},{7,39},{8,0},{9,41... | collective-permute-start | bytes 2162696 | tf_op jit(solution)/shard_map/ppermute | solution.py:71
  86.4 64.4 %collective-permute-start.19 = (bf16[1024,2048]{1,0:T(8,128)(2,1)S(1)}, bf16[1024,2048]{1,0:T(8,128)(2,1)S(1)}, u32[]{:S(2)}, u32[]{:S(2)}) collective-permute-start(bf16[1024,2048]{1,0:T(8,128)(2,1)S(1)} %attention.1.mine), channel_id=1, source_target_pairs={{0,1},{1,0},{2,3},{3,2},{4,5},{5,4},{6,7},{7,6},{8,9},{9,8},{10,11... | collective-permute-start | bytes 12582920 | tf_op jit(solution)/shard_map/ppermute | solution.py:67
  92.5 14.1 %collective-permute-start.20 = (bf16[256,1408]{1,0:T(8,128)(2,1)S(1)}, bf16[256,1408]{1,0:T(8,128)(2,1)S(1)}, u32[]{:S(2)}, u32[]{:S(2)}) collective-permute-start(bf16[256,1408]{1,0:T(8,128)(2,1)S(1)} %pad_maximum_fusion.12), channel_id=1, source_target_pairs={{0,6},{1,25},{2,4},{3,27},{4,2},{5,29},{6,0},{7,31},{8,14},{9,17},... | collective-permute-start | bytes 2162696 | tf_op jit(solution)/shard_map/ppermute | solution.py:71
  97.8 16.8 %collective-permute-start.24 = (bf16[512,1280]{1,0:T(8,128)(2,1)S(1)}, bf16[512,1280]{1,0:T(8,128)(2,1)S(1)}, u32[]{:S(2)}, u32[]{:S(2)}) collective-permute-start(bf16[512,1280]{1,0:T(8,128)(2,1)S(1)} %pad_maximum_fusion.4), channel_id=1, source_target_pairs={{0,2},{1,9},{2,0},{3,11},{4,6},{5,13},{6,4},{7,15},{8,10},{9,1},{1... | collective-permute-start | bytes 3932168 | tf_op jit(solution)/shard_map/ppermute | solution.py:71
  98.0 23.1 %collective-permute-start.27 = (bf16[512,1408]{1,0:T(8,128)(2,1)S(1)}, bf16[512,1408]{1,0:T(8,128)(2,1)S(1)}, u32[]{:S(2)}, u32[]{:S(2)}) collective-permute-start(bf16[512,1408]{1,0:T(8,128)(2,1)S(1)} %pad_maximum_fusion.3), channel_id=1, source_target_pairs={{0,32},{1,7},{2,34},{3,5},{4,36},{5,3},{6,38},{7,1},{8,40},{9,15},... | collective-permute-start | bytes 4325384 | tf_op jit(solution)/shard_map/ppermute | solution.py:71
  106.8 19.4 %collective-permute-start.21 = (bf16[512,1408]{1,0:T(8,128)(2,1)S(1)}, bf16[512,1408]{1,0:T(8,128)(2,1)S(1)}, u32[]{:S(2)}, u32[]{:S(2)}) collective-permute-start(bf16[512,1408]{1,0:T(8,128)(2,1)S(1)} %pad_maximum_fusion.2), channel_id=1, source_target_pairs={{0,24},{1,97},{2,26},{3,99},{4,28},{5,101},{6,30},{7,103},{8,16},{... | collective-permute-start | bytes 4325384 | tf_op jit(solution)/shard_map/ppermute | solution.py:71
  114.8 16.8 %collective-permute-start.25 = (bf16[1024,640]{1,0:T(8,128)(2,1)S(1)}, bf16[1024,640]{1,0:T(8,128)(2,1)S(1)}, u32[]{:S(2)}, u32[]{:S(2)}) collective-permute-start(bf16[1024,640]{1,0:T(8,128)(2,1)S(1)} %pad_maximum_fusion.5.rest_2_), channel_id=1, source_target_pairs={{0,8},{1,33},{2,10},{3,35},{4,12},{5,37},{6,14},{7,39},{8,0},{9,41... | collective-permute-start | bytes 3932168 | tf_op jit(solution)/shard_map/ppermute | solution.py:71
  121.3 27.7 %collective-permute-start.28 = (bf16[1024,640]{1,0:T(8,128)(2,1)S(1)}, bf16[1024,640]{1,0:T(8,128)(2,1)S(1)}, u32[]{:S(2)}, u32[]{:S(2)}) collective-permute-start(bf16[1024,640]{1,0:T(8,128)(2,1)S(1)} %pad_maximum_fusion.6.rest_4_), channel_id=1, source_target_pairs={{0,6},{1,25},{2,4},{3,27},{4,2},{5,29},{6,0},{7,31},{8,14},{9,17},... | collective-permute-start | bytes 3932168 | tf_op jit(solution)/shard_map/ppermute | solution.py:71
  126.4 24.5 %collective-permute-start.22 = (bf16[1024,768]{1,0:T(8,128)(2,1)S(1)}, bf16[1024,768]{1,0:T(8,128)(2,1)S(1)}, u32[]{:S(2)}, u32[]{:S(2)}) collective-permute-start(bf16[1024,768]{1,0:T(8,128)(2,1)S(1)} %pad_maximum_fusion.rest_0_), channel_id=1, source_target_pairs={{0,96},{1,3},{2,98},{3,1},{4,100},{5,7},{6,102},{7,5},{8,104},{9,1... | collective-permute-start | bytes 4718600 | tf_op jit(solution)/shard_map/ppermute | solution.py:71
  127.5 49.4 %collective-permute-start.31 = (bf16[1024,768]{1,0:T(8,128)(2,1)S(1)}, bf16[1024,768]{1,0:T(8,128)(2,1)S(1)}, u32[]{:S(2)}, u32[]{:S(2)}) collective-permute-start(bf16[1024,768]{1,0:T(8,128)(2,1)S(1)} %pad_maximum_fusion.1.rest_4_), channel_id=1, source_target_pairs={{0,6},{1,25},{2,4},{3,27},{4,2},{5,29},{6,0},{7,31},{8,14},{9,17},... | collective-permute-start | bytes 4718600 | tf_op jit(solution)/shard_map/ppermute | solution.py:71
  131.7 45.3 %collective-permute-start.30 = (bf16[1024,640]{1,0:T(8,128)(2,1)S(1)}, bf16[1024,640]{1,0:T(8,128)(2,1)S(1)}, u32[]{:S(2)}, u32[]{:S(2)}) collective-permute-start(bf16[1024,640]{1,0:T(8,128)(2,1)S(1)} %pad_maximum_fusion.8.rest_2_), channel_id=1, source_target_pairs={{0,8},{1,33},{2,10},{3,35},{4,12},{5,37},{6,14},{7,39},{8,0},{9,41... | collective-permute-start | bytes 3932168 | tf_op jit(solution)/shard_map/ppermute | solution.py:71
  149.0 27.9 %collective-permute-start.29 = (bf16[1024,640]{1,0:T(8,128)(2,1)S(1)}, bf16[1024,640]{1,0:T(8,128)(2,1)}, u32[]{:S(2)}, u32[]{:S(2)}) collective-permute-start(bf16[1024,640]{1,0:T(8,128)(2,1)S(1)} %pad_maximum_fusion.7.rest_0_), channel_id=1, source_target_pairs={{0,96},{1,3},{2,98},{3,1},{4,100},{5,7},{6,102},{7,5},{8,104},{9,1... | collective-permute-start | bytes 3932168 | tf_op jit(solution)/shard_map/ppermute | solution.py:71
  186.0 24.0 %collective-permute-start.32 = (bf16[1024,1024]{1,0:T(8,128)(2,1)S(1)}, bf16[1024,1024]{1,0:T(8,128)(2,1)S(1)}, u32[]{:S(2)}, u32[]{:S(2)}) collective-permute-start(bf16[1024,1024]{1,0:T(8,128)(2,1)S(1)} %shard_map.182), channel_id=1, source_target_pairs={{0,1},{1,0},{2,3},{3,2},{4,5},{5,4},{6,7},{7,6},{8,9},{9,8},{10,11... | collective-permute-start | bytes 6291464 | tf_op jit(solution)/shard_map/ppermute | solution.py:67
  (30 other events, 215.9 us)
where the time goes:
time: 219 us; the launch traced here: 218 us
  starting transfers between devices  78.7 us (36%)
  Pallas kernels  62.7 us (29%)
  waiting for transfers between devices  50.5 us (23%)
  local copies, waits for them, and re-layouts  13.5 us (6%)
  other arithmetic  10.1 us (5%)
    ppermute x30, starting transfers between devices, over_link(): return lax.ppermute(array, ALL, partner_pairs(step, chain))  51.9 us
    ppermute x30, waiting for transfers between devices, over_link(): return lax.ppermute(array, ALL, partner_pairs(step, chain))  49.3 us
    ppermute x4, starting transfers between devices, swap_cores(): return lax.ppermute(array, 'tp', [(0, 1), (1, 0)])  26.8 us
    pallas_call x1, Pallas kernels, on_device(): pl.pallas_call(up_kernel, grid=grid, in_specs=[SMEM, SMEM, rows_of(block,...  24.1 us
    pallas_call x2, Pallas kernels, down_half(): pl.pallas_call(down_kernel, grid=grid, in_specs=[SMEM, SMEM, rows_of(bloc...  18 us
    pallas_call x1, Pallas kernels, on_device(): pl.pallas_call(attention_kernel, grid=(length // CHUNK,), in_specs=[SMEM,...  15.5 us
    unnamed x58, local copies, waits for them, and re-layouts  5.65 us
    pallas_call x1, Pallas kernels, on_device(): pl.pallas_call(norm_kernel, grid=grid, in_specs=[SMEM, rows_of(block, 102...  5.1 us
  transfers between devices with their start and end apart: 34, of which 13 were waited for; matrix products, arithmetic and copies ran while one was open for 5% of the time, Pallas kernels for 25%

commit v1 on v0

v1 whole, which is shorter than its diff:
```python
import jax
import jax.numpy as jnp
import numpy as np
from jax import lax
from jax.experimental import pallas as pl
from jax.experimental.pallas import tpu as pltpu
from jax.sharding import Mesh
from jax.sharding import PartitionSpec as P


FS = ("fs_0", "fs_1", "fs_2")
REP_FS = ("rep", "fs_0", "fs_1", "fs_2")
ALL = ("rep", "fs_0", "fs_1", "fs_2", "tp")
EPS = 1e-06
CHUNK = 256
HALF = 32
BF = jnp.bfloat16
F32 = jnp.float32


CLASSES = (("x", 1), ("y", 1), ("z", 1), ("x", 3), ("y", 3), ("z", 3))


def link_class(step, chain, core):
    if step < 3:
        return CLASSES[3 * core + step]
    return CLASSES[3 * (1 - core) + (step + chain) % 3]


def partner_pairs(step, chain):
    pairs = []
    for z in range(4):
        for y in range(4):
            for x in range(4):
                for core in range(2):
                    axis, flip = link_class(step, chain, core)
                    to = {"x": x, "y": y, "z": z}
                    to[axis] ^= flip
                    source = ((z * 4 + y) * 4 + x) * 2 + core
                    target = ((to["z"] * 4 + to["y"]) * 4 + to["x"]) * 2 + core
                    pairs.append((source, target))
    return pairs


def row_block(z, y, x):
    return (((z & 1) * 16 + y * 4 + x) << 1) | (z >> 1)


def block_offsets():
    table = np.zeros((2, 6, 64), np.int32)
    for core in range(2):
        for row in range(6):
            for place in range(64):
                total = 0
                for step in range(6):
                    if place >> step & 1:
                        axis, flip = link_class(step, row % 3, core)
                        at = {"x": 0, "y": 0, "z": 0}
                        at[axis] = flip
                        total ^= row_block(at["z"], at["y"], at["x"])
                table[core, row, place] = total
    return table


OFFSETS = block_offsets()


def half_places():
    lists = np.zeros((2, 2, 6, 16), np.int32)
    for core in range(2):
        for high in range(2):
            for chain in range(3):
                for piece in range(2):
                    offsets = OFFSETS[core, 3 + chain, 32 * piece : 32 * piece + 32]
                    lists[core, high, 2 * chain + piece] = np.flatnonzero(offsets >> 5 == high)
    return lists


HALF_PLACES = half_places()


def half_targets():
    targets = np.zeros_like(HALF_PLACES)
    for core, high, row in np.ndindex(2, 2, 6):
        places = HALF_PLACES[core, high, row] + 32 * (row % 2)
        targets[core, high, row] = OFFSETS[core, 3 + row // 2, places] & 31
    return targets


HALF_TARGETS = half_targets()


def swap_cores(array):
    return lax.ppermute(array, "tp", [(0, 1), (1, 0)])


def over_link(array, step, chain):
    return lax.ppermute(array, ALL, partner_pairs(step, chain))


def joined(a, b):
    return jnp.concatenate([a, b], axis=0)


def gather_start(own):
    held = own
    for step in range(3):
        came = over_link(held, step, 0)
        if step < 2:
            held = joined(held, came)
    return held, came


def columns(pair, lane, width):
    return joined(*(a[:, lane : lane + width] for a in pair))


def block_copy(piece, at, target, to, lane, sem):
    pltpu.make_async_copy(
        piece.at[pl.ds(pl.multiple_of(at * HALF, HALF), HALF), :],
        target.at[pl.ds(pl.multiple_of(to * HALF, HALF), HALF), pl.ds(lane, piece.shape[1])],
        sem,
    ).start()


def place_blocks(table, row, pieces, target, lane, sem):
    place = 0
    for piece in pieces:
        count = piece.shape[0] // HALF

        def one(i, carry, piece=piece, place=place):
            block_copy(piece, i, target, table[row, place + i], lane, sem)
            return carry

        lax.fori_loop(0, count, one, 0, unroll=4)
        place += count


def place_half(places, targets, row, pieces, target, lane, sem):
    for k, piece in enumerate(pieces):

        def one(i, carry, piece=piece, k=k):
            block_copy(
                piece, places[2 * row + k, i], target, targets[2 * row + k, i], lane, sem
            )
            return carry

        lax.fori_loop(0, 16, one, 0, unroll=4)


def wait_part(target, lane, width, sem):
    part = target.at[:, pl.ds(lane, width)]
    pltpu.make_async_copy(part, part, sem).wait()


def nt_dot(a, b):
    return lax.dot_general(a, b, (((1,), (1,)), ((), ())), preferred_element_type=F32)


def tn_dot(a, b):
    return lax.dot_general(a, b, (((0,), (0,)), ((), ())), preferred_element_type=F32)


def ordered(core, own, other):
    first = core == 0
    return jnp.concatenate([jnp.where(first, own, other), jnp.where(first, other, own)], axis=1)


def norm_kernel(core, own, other, gain, first, second, bias, surge, normed_out, decay_out):
    rows = ordered(core[0], own[...], other[...]).astype(F32)
    scale = lax.rsqrt(jnp.mean(rows * rows, axis=-1, keepdims=True) + EPS)
    normed = (rows * scale * gain[...]).astype(BF)
    normed_out[...] = normed
    rank = jnp.dot(normed, first[...], preferred_element_type=F32).astype(BF)
    gate = jnp.dot(rank, second[...], preferred_element_type=F32) + bias[...]
    decay_out[...] = jax.nn.log_sigmoid(gate) / 16.0 + surge[...]


def small_level_matrices():
    i = np.arange(CHUNK)[:, None]
    t = np.arange(CHUNK)[None, :]
    mats = []
    for size in (2, 4):
        same = i // (2 * size) == t // (2 * size)
        upper_i, upper_t = i % (2 * size) >= size, t % (2 * size) >= size
        mats.append(same & ((upper_i & upper_t & (t <= i)) | (~upper_i & ~upper_t & (t > i))))
    same = i // 8 == t // 8
    mats.append(same & (t <= i))
    mats.append(same & (t > i))
    return np.concatenate(mats, axis=0)


def level_of_pairs():
    i = np.arange(CHUNK)[:, None]
    j = np.arange(CHUNK)[None, :]
    level = np.floor(np.log2(np.maximum(i ^ j, 1))).astype(np.int32)
    return np.where(j < i, level, -1).astype(np.int32)


SMALL_LEVELS = small_level_matrices()
PAIR_LEVELS = level_of_pairs()


def attention_kernel(table, normed, decay, mats, pair_level, gain, *rest):
    pieces = (rest[0:2], rest[2:4], rest[4:6])
    partial_out, w_qk, w_v, w_out, state, sems = rest[6:]
    weights = (w_qk, w_v, w_out)
    for c in range(3):
        place_blocks(table, c, pieces[c], weights[c], 0, sems.at[c])
    state[...] = jnp.zeros_like(state)
    for c in range(3):
        wait_part(weights[c], 0, 512, sems.at[c])

    def one(i, carry):
        here = pl.ds(pl.multiple_of(i * CHUNK, CHUNK), CHUNK)
        partial_out[here, :] = attention_chunk(
            normed[here, :], decay[here, :], mats, pair_level, gain, w_qk, w_v, w_out, state
        )
        return carry

    lax.fori_loop(0, normed.shape[0] // CHUNK, one, 0)


def attention_chunk(rows, g, mats, pair_level, gain, w_qk, w_v, w_out, state):
    g_hi = g.astype(BF)
    g_lo = (g - g_hi.astype(F32)).astype(BF)

    def summed(index):
        mat = mats[pl.ds(index * CHUNK, CHUNK), :]
        return jnp.dot(mat, g_hi, preferred_element_type=F32) + jnp.dot(
            mat, g_lo, preferred_element_type=F32
        )

    before, after = summed(2), summed(3)
    row = lax.broadcasted_iota(jnp.int32, (CHUNK, CHUNK), 0)
    spans = [jnp.where((row & 1) != 0, g, 0.0), summed(0), summed(1)]
    size = 8
    while size < CHUNK:
        b = before.reshape(CHUNK // (2 * size), 2, size, CHUNK)
        a = after.reshape(CHUNK // (2 * size), 2, size, CHUNK)
        spans.append(jnp.stack([a[:, 0], b[:, 1]], axis=1).reshape(CHUNK, CHUNK))
        low, high = b[:, 0, size - 1 :, :], b[:, 1, size - 1 :, :]
        before = jnp.stack([b[:, 0], b[:, 1] + low], axis=1).reshape(CHUNK, CHUNK)
        after = jnp.stack([a[:, 0] + high, a[:, 1]], axis=1).reshape(CHUNK, CHUNK)
        size *= 2

    qk = jnp.dot(rows, w_qk[...], preferred_element_type=F32).astype(BF).astype(F32)
    q, k = qk[:, :256] * (256**-0.5), qk[:, 256:]
    v = jnp.dot(rows, w_v[...], preferred_element_type=F32).astype(BF)
    level_map = pair_level[...]
    scores = jnp.zeros((CHUNK, CHUNK), F32)
    for level, span in enumerate(spans):
        both = (jnp.where((row & (1 << level)) != 0, q, k) * jnp.exp(span)).astype(BF)
        scores = jnp.where(level_map == level, nt_dot(both, both), scores)
    q_in = (q * jnp.exp(before)).astype(BF)
    k_out = (k * jnp.exp(after)).astype(BF)
    old = state[...]
    readout = (
        nt_dot(q_in, old.astype(BF))
        + jnp.dot(scores.astype(BF), v, preferred_element_type=F32)
        + jnp.sum(q * k, axis=1, keepdims=True) * v.astype(F32)
    )
    state[...] = old * jnp.exp(before[CHUNK - 1 :, :]) + tn_dot(v, k_out)
    scale = lax.rsqrt(jnp.mean(readout * readout, axis=-1, keepdims=True) + EPS)
    mixed = (readout * scale * gain[...]).astype(BF)
    return nt_dot(mixed, w_out[...]).astype(BF)


UP_WIDTHS = (768, 640, 640)
DOWN_WIDTHS = (640, 640, 768)


def start_of(widths, chain):
    return sum(widths[:chain])


def middle_kernel(core, own, other, mine, theirs, gain_own, gain_other, pre_gain, resid_out, out):
    first = core[0] == 0
    rows = ordered(core[0], own[...], other[...]).astype(F32)
    post_gain = ordered(core[0], gain_own[...], gain_other[...])
    attn = mine[...].astype(F32) + theirs[...].astype(F32)
    scale = lax.rsqrt(jnp.mean(attn * attn, axis=-1, keepdims=True) + EPS)
    resid = (rows + attn * scale * post_gain).astype(BF)
    resid_out[...] = jnp.where(first, resid[:, :1024], resid[:, 1024:])
    values = resid.astype(F32)
    scale = lax.rsqrt(jnp.mean(values * values, axis=-1, keepdims=True) + EPS)
    out[...] = (values * scale * pre_gain[...]).astype(BF)


def up_kernel(table, normed, *rest):
    squared_out, weight, sems = rest[6:]
    for c in range(3):
        at = start_of(UP_WIDTHS, c)
        place_blocks(table, 3 + c, rest[2 * c : 2 * c + 2], weight, at, sems.at[c])
    for c in range(3):
        at, width = start_of(UP_WIDTHS, c), UP_WIDTHS[c]
        wait_part(weight, at, width, sems.at[c])

        def one(i, carry, at=at, width=width):
            here = pl.ds(pl.multiple_of(i * 256, 256), 256)
            hidden = jnp.dot(
                normed[here, :], weight[:, at : at + width], preferred_element_type=F32
            )
            hidden = jnp.maximum(hidden, 0.0)
            squared_out[here, at : at + width] = (hidden * hidden).astype(BF)
            return carry

        lax.fori_loop(0, normed.shape[0] // 256, one, 0)


def down_kernel(places, targets, squared, *rest):
    partial_out, weight, sems = rest[6:]
    for c in range(3):
        at = start_of(DOWN_WIDTHS, c)
        place_half(places, targets, c, rest[2 * c : 2 * c + 2], weight, at, sems.at[c])
    for c in range(3):
        wait_part(weight, start_of(DOWN_WIDTHS, c), DOWN_WIDTHS[c], sems.at[c])

    def one(i, carry):
        here = pl.ds(pl.multiple_of(i * 256, 256), 256)
        partial_out[here, :] = nt_dot(squared[here, :], weight[...]).astype(BF)
        return carry

    lax.fori_loop(0, squared.shape[0] // 256, one, 0)


SMEM = pl.BlockSpec(memory_space=pltpu.SMEM)
VMEM = pl.BlockSpec(memory_space=pltpu.VMEM)
HBM = pl.BlockSpec(memory_space=pltpu.HBM)


def whole(shape):
    return pl.BlockSpec(shape, lambda i: (0,) * len(shape))


def rows_of(count, width):
    return pl.BlockSpec((count, width), lambda i: (i, 0))


def params(flops, nbytes, vmem_mib):
    return dict(
        compiler_params=pltpu.CompilerParams(vmem_limit_bytes=vmem_mib * 1024 * 1024),
        cost_estimate=pl.CostEstimate(flops=flops, bytes_accessed=nbytes, transcendentals=0),
    )


def on_device(
    tokens,
    attention_pre_gain,
    query_matrix,
    key_matrix,
    value_matrix,
    decay_first_weight,
    decay_second_weight,
    decay_offset_bias,
    extra_log_surge,
    readout_head_gain,
    output_matrix,
    attention_post_gain,
    feedforward_pre_gain,
    up_matrix,
    down_matrix,
    feedforward_post_gain,
):
    length = tokens.shape[0]
    rep, core = lax.axis_index("rep"), lax.axis_index("tp")
    fs = lax.axis_index(FS)
    mine_block = (fs * 2 + rep).astype(jnp.int32)
    core_in = core.astype(jnp.int32).reshape(1)
    table = jnp.asarray(OFFSETS)[core] ^ mine_block

    def half(shard):
        return lax.dynamic_slice_in_dim(shard, rep * HALF, HALF, axis=0)

    first = jnp.concatenate(
        [half(query_matrix), half(key_matrix), half(value_matrix), half(output_matrix.T)], axis=1
    )
    first = gather_start(first)
    up, down = half(up_matrix), half(down_matrix.T)
    feed = []
    for c in range(3):
        a, b = start_of(UP_WIDTHS, c), start_of(DOWN_WIDTHS, c)
        feed += [up[:, a : a + UP_WIDTHS[c]], down[:, b : b + DOWN_WIDTHS[c]]]
    feed = gather_start(jnp.concatenate(feed, axis=1))
    first_w, up_w, down_w = [], [], []
    lane = 0
    for c in range(3):
        held = columns(first, 512 * c, 512)
        for step in (3, 4):
            held = joined(held, over_link(held, step, c))
        first_w += [held, over_link(held, 5, c)]

        a, b = UP_WIDTHS[c], DOWN_WIDTHS[c]
        held = columns(feed, lane, a + b)
        lane += a + b
        held = joined(held, over_link(held, 3, c))
        pair = held, over_link(held, 4, c)
        held = columns(pair, 0, a)
        up_w += [held, over_link(held, 5, c)]
        held = columns(pair, a, b)
        down_w += [held, over_link(held, 5, c)]

    other = swap_cores(tokens)
    block = 256
    grid = (length // block,)
    normed, decay = pl.pallas_call(
        norm_kernel,
        grid=grid,
        in_specs=[
            SMEM,
            rows_of(block, 1024),
            rows_of(block, 1024),
            whole((1, 2048)),
            whole((2048, 16)),
            whole((16, 256)),
            whole((1, 256)),
            rows_of(block, 1),
        ],
        out_specs=[rows_of(block, 2048), rows_of(block, 256)],
        out_shape=[
            jax.ShapeDtypeStruct((length, 2048), BF),
            jax.ShapeDtypeStruct((length, 256), F32),
        ],
        name="norm",
        **params(400_000_000, 10_000_000, 16),
    )(
        core_in,
        tokens,
        other,
        attention_pre_gain.reshape(1, -1),
        decay_first_weight,
        decay_second_weight,
        decay_offset_bias.reshape(1, -1),
        extra_log_surge,
    )
    partial_attn = pl.pallas_call(
        attention_kernel,
        in_specs=[SMEM] + [VMEM] * 5 + [HBM] * 6,
        out_specs=VMEM,
        out_shape=jax.ShapeDtypeStruct((length, 2048), BF),
        scratch_shapes=[
            pltpu.VMEM((2048, 512), BF),
            pltpu.VMEM((2048, 512), BF),
            pltpu.VMEM((2048, 512), BF),
            pltpu.VMEM((512, 256), F32),
            pltpu.SemaphoreType.DMA((3,)),
        ],
        name="attention",
        **params(11_000_000_000, 14_000_000, 26),
    )(
        table,
        normed,
        decay,
        jnp.asarray(SMALL_LEVELS, BF),
        jnp.asarray(PAIR_LEVELS),
        readout_head_gain.reshape(1, -1),
        *first_w,
    )
    other_attn = swap_cores(partial_attn)
    other_gain = swap_cores(attention_post_gain)
    resid, normed_mid = pl.pallas_call(
        middle_kernel,
        grid=grid,
        in_specs=[
            SMEM,
            rows_of(block, 1024),
            rows_of(block, 1024),
            rows_of(block, 2048),
            rows_of(block, 2048),
            whole((1, 1024)),
            whole((1, 1024)),
            whole((1, 2048)),
        ],
        out_specs=[rows_of(block, 1024), rows_of(block, 2048)],
        out_shape=[
            jax.ShapeDtypeStruct((length, 1024), BF),
            jax.ShapeDtypeStruct((length, 2048), BF),
        ],
        name="middle",
        **params(60_000_000, 18_000_000, 20),
    )(
        core_in,
        tokens,
        other,
        partial_attn,
        other_attn,
        attention_post_gain.reshape(1, -1),
        other_gain.reshape(1, -1),
        feedforward_pre_gain.reshape(1, -1),
    )
    squared = pl.pallas_call(
        up_kernel,
        in_specs=[SMEM, VMEM] + [HBM] * 6,
        out_specs=VMEM,
        out_shape=jax.ShapeDtypeStruct((length, 2048), BF),
        scratch_shapes=[pltpu.VMEM((2048, 2048), BF), pltpu.SemaphoreType.DMA((3,))],
        name="up_proj",
        **params(8_700_000_000, 16_000_000, 24),
    )(table, normed_mid, *up_w)

    def down_half(side):
        return pl.pallas_call(
            down_kernel,
            in_specs=[SMEM, SMEM, VMEM] + [HBM] * 6,
            out_specs=VMEM,
            out_shape=jax.ShapeDtypeStruct((length, 1024), BF),
            scratch_shapes=[pltpu.VMEM((1024, 2048), BF), pltpu.SemaphoreType.DMA((3,))],
            **params(4_300_000_000, 10_000_000, 20),
        )(
            jnp.asarray(HALF_PLACES)[core, side ^ (mine_block >> 5)],
            jnp.asarray(HALF_TARGETS)[core, side ^ (mine_block >> 5)] ^ (mine_block & 31),
            squared,
            *down_w,
        )

    away = down_half(1 - core)
    theirs = swap_cores(away)
    mine = down_half(core)
    feed = mine.astype(F32) + theirs.astype(F32)
    squares = jnp.sum(feed * feed, axis=1)
    squares_other = swap_cores(squares.reshape(8, 128)).reshape(length)
    scale = lax.rsqrt((squares + squares_other) / 2048 + EPS)[:, None]
    return (resid.astype(F32) + feed * scale * feedforward_post_gain).astype(BF)


def solution(mesh):
    finer = Mesh(
        mesh.devices.reshape(mesh.shape["rep"], 2, 4, 4, mesh.shape["tp"]),
        ("rep", "fs_0", "fs_1", "fs_2", "tp"),
    )
    in_specs = (
        P(REP_FS, "tp"),
        P(),
        P(FS, "tp"),
        P(FS, "tp"),
        P(FS, "tp"),
        P(),
        P(None, "tp"),
        P("tp"),
        P(REP_FS, "tp"),
        P(),
        P("tp", FS),
        P("tp"),
        P(),
        P(FS, "tp"),
        P("tp", FS),
        P("tp"),
    )

    return jax.shard_map(
        on_device, mesh=finer, in_specs=in_specs, out_specs=P(REP_FS, "tp"), check_vma=False
    )
```

time: 219 us -> 196 us (0.89)
  starting transfers between devices: 78.7 us -> 54 us
  Pallas kernels: 62.7 us -> 57.2 us
  local copies, waits for them, and re-layouts: 13.5 us -> 17.8 us
  other arithmetic: 10.1 us -> 14.3 us
    ppermute x30 -> x27, starting transfers between devices: 51.9 us -> 27.1 us  [over_link(): return lax.ppermute(array, ALL, partner_pairs(step, chain))]
    concatenate x30 -> x26, other arithmetic: 4.65 us -> 11.1 us  [the longest x25 11.1 us: joined(): return jnp.concatenate([a, b], axis=0)]
    pallas_call x4 -> x5, Pallas kernels: 57.6 us -> 52.1 us  [the longest x2 16.6 us: down_half(): pl.pallas_call(down_kernel, in_specs=[SMEM, SMEM, VMEM] + [HBM] * 6, out_...]
    unnamed x58 -> x53, local copies, waits for them, and re-layouts: 5.65 us -> 10.5 us
    convert_element_type x1, other arithmetic: 4.63 us -> 2.4 us  [on_device(): return (resid.astype(F32) + feed * scale * feedforward_post_gain).astype(BF)]
    slice x26 -> x16, local copies, waits for them, and re-layouts: 5.58 us -> 5.01 us  [columns(): return joined(*(a[:, lane:lane + width] for a in pair))]
    ppermute x30 -> x27, waiting for transfers between devices: 49.3 us -> 49.7 us  [over_link(): return lax.ppermute(array, ALL, partner_pairs(step, chain))]
    ppermute x4 -> x5, starting transfers between devices: 26.8 us -> 26.9 us  [swap_cores(): return lax.ppermute(array, 'tp', [(0, 1), (1, 0)])]
  transfers between devices with their start and end apart: 34 -> 32, of which waited for: 13 -> 14; matrix products, arithmetic and copies ran while one was open for 5% -> 10% of each run, Pallas kernels for 25% -> 25%
where the time goes in v1:
time: 196 us; the launch traced here: 195 us
  Pallas kernels  57.2 us (29%)
  starting transfers between devices  54 us (28%)
  waiting for transfers between devices  50.9 us (26%)
  local copies, waits for them, and re-layouts  17.8 us (9%)
  other arithmetic  14.3 us (7%)
    ppermute x27, waiting for transfers between devices, over_link(): return lax.ppermute(array, ALL, partner_pairs(step, chain))  49.7 us
    ppermute x27, starting transfers between devices, over_link(): return lax.ppermute(array, ALL, partner_pairs(step, chain))  27.1 us
    ppermute x5, starting transfers between devices, swap_cores(): return lax.ppermute(array, 'tp', [(0, 1), (1, 0)])  26.9 us
    pallas_call x2, Pallas kernels, down_half(): pl.pallas_call(down_kernel, in_specs=[SMEM, SMEM, VMEM] + [HBM] * 6, out_...  16.6 us
    pallas_call x1, Pallas kernels, on_device(): pl.pallas_call(attention_kernel, in_specs=[SMEM] + [VMEM] * 5 + [HBM] * 6...  15.3 us
    pallas_call x1, Pallas kernels, on_device(): pl.pallas_call(up_kernel, in_specs=[SMEM, VMEM] + [HBM] * 6, out_specs=VM...  14.8 us
    concatenate x25, other arithmetic, joined(): return jnp.concatenate([a, b], axis=0)  11.1 us
    unnamed x53, local copies, waits for them, and re-layouts  10.5 us
  transfers between devices with their start and end apart: 32, of which 14 were waited for; matrix products, arithmetic and copies ran while one was open for 10% of the time, Pallas kernels for 25%

profile of v1, /device:TPU:1, one launch (start us, length us, event | category | flops | bytes accessed | tf_op | source)
XLA Modules:
  0.0 194.8 jit_solution(9997027871303150392)
XLA Ops:
  2.3 3.4 %collective-permute-start.1 = (bf16[32,1536]{1,0:T(8,128)(2,1)S(1)}, bf16[32,1536]{1,0:T(8,128)(2,1)S(1)}, u32[]{:S(2)}, u32[]{:S(2)}) collective-permute-start(bf16[32,1536]{1,0:T(8,128)(2,1)S(1)} %pad_maximum_fusion.25), channel_id=1, source_target_pairs={{0,2},{1,7},{2,0},{3,5},{4,6},{5,3},{6,4},{7,1},{8,10},{9,15},{10,... | collective-permute-start | bytes 294920 | tf_op jit(solution)/shard_map/ppermute | solution.py:98
  7.7 3.0 %collective-permute-start.2 = (bf16[64,1536]{1,0:T(8,128)(2,1)S(1)}, bf16[64,1536]{1,0:T(8,128)(2,1)S(1)}, u32[]{:S(2)}, u32[]{:S(2)}) collective-permute-start(bf16[64,1536]{1,0:T(8,128)(2,1)S(1)} %pad_maximum_fusion.24), channel_id=1, source_target_pairs={{0,8},{1,25},{2,10},{3,27},{4,12},{5,29},{6,14},{7,31},{8,0},{9,17... | collective-permute-start | bytes 589832 | tf_op jit(solution)/shard_map/ppermute | solution.py:98
  11.5 2.3 %collective-permute-done.2 = bf16[64,1536]{1,0:T(8,128)(2,1)S(1)} collective-permute-done((bf16[64,1536]{1,0:T(8,128)(2,1)S(1)}, bf16[64,1536]{1,0:T(8,128)(2,1)S(1)}, u32[]{:S(2)}, u32[]{:S(2)}) %collective-permute-start.2) | collective-permute-done | bytes 196640 | tf_op jit(solution)/shard_map/ppermute | solution.py:98
  13.8 3.8 %collective-permute-start.3 = (bf16[128,1536]{1,0:T(8,128)(2,1)S(1)}, bf16[128,1536]{1,0:T(8,128)(2,1)S(1)}, u32[]{:S(2)}, u32[]{:S(2)}) collective-permute-start(bf16[128,1536]{1,0:T(8,128)(2,1)S(1)} %pad_maximum_fusion.20), channel_id=1, source_target_pairs={{0,32},{1,97},{2,34},{3,99},{4,36},{5,101},{6,38},{7,103},{8,40},{... | collective-permute-start | bytes 1179656 | tf_op jit(solution)/shard_map/ppermute | solution.py:98
  17.7 2.5 %collective-permute-start.15 = (bf16[32,4096]{1,0:T(8,128)(2,1)S(1)}, bf16[32,4096]{1,0:T(8,128)(2,1)S(1)}, u32[]{:S(2)}, u32[]{:S(2)}) collective-permute-start(bf16[32,4096]{1,0:T(8,128)(2,1)S(1)} %slice_dynamic-update-slice_fusion), channel_id=1, source_target_pairs={{0,2},{1,7},{2,0},{3,5},{4,6},{5,3},{6,4},{7,1},{8,10},{9,15},{10,... | collective-permute-start | bytes 786440 | tf_op jit(solution)/shard_map/ppermute | solution.py:98
  20.2 2.6 %collective-permute-done.3 = bf16[128,1536]{1,0:T(8,128)(2,1)S(1)} collective-permute-done((bf16[128,1536]{1,0:T(8,128)(2,1)S(1)}, bf16[128,1536]{1,0:T(8,128)(2,1)S(1)}, u32[]{:S(2)}, u32[]{:S(2)}) %collective-permute-start.3) | collective-permute-done | bytes 393248 | tf_op jit(solution)/shard_map/ppermute | solution.py:98
  24.1 2.8 %collective-permute-start.16 = (bf16[64,4096]{1,0:T(8,128)(2,1)S(1)}, bf16[64,4096]{1,0:T(8,128)(2,1)S(1)}, u32[]{:S(2)}, u32[]{:S(2)}) collective-permute-start(bf16[64,4096]{1,0:T(8,128)(2,1)S(1)} %pad_maximum_fusion.19), channel_id=1, source_target_pairs={{0,8},{1,25},{2,10},{3,27},{4,12},{5,29},{6,14},{7,31},{8,0},{9,17... | collective-permute-start | bytes 1572872 | tf_op jit(solution)/shard_map/ppermute | solution.py:98
  27.1 6.1 %collective-permute-start = (bf16[1024,1024]{1,0:T(8,128)(2,1)S(1)}, bf16[1024,1024]{1,0:T(8,128)(2,1)}, u32[]{:S(2)}, u32[]{:S(2)}) collective-permute-start(bf16[1024,1024]{1,0:T(8,128)(2,1)S(1)} %copy-done.2), channel_id=1, source_target_pairs={{0,1},{1,0},{2,3},{3,2},{4,5},{5,4},{6,7},{7,6},{8,9},{9,8},{10,11... | collective-permute-start | bytes 6291464 | tf_op jit(solution)/shard_map/ppermute | solution.py:94
  33.7 1.6 collective-permute-done.7
  37.3 2.3 %collective-permute-start.17 = (bf16[128,4096]{1,0:T(8,128)(2,1)}, bf16[128,4096]{1,0:T(8,128)(2,1)}, u32[]{:S(2)}, u32[]{:S(2)}) collective-permute-start(bf16[128,4096]{1,0:T(8,128)(2,1)} %pad_maximum_fusion.12), channel_id=1, source_target_pairs={{0,32},{1,97},{2,34},{3,99},{4,36},{5,101},{6,38},{7,103},{8,40},{... | collective-permute-start | bytes 3145736 | tf_op jit(solution)/shard_map/ppermute | solution.py:98
  39.6 2.7 %collective-permute-done.5 = bf16[512,512]{1,0:T(8,128)(2,1)S(1)} collective-permute-done((bf16[512,512]{1,0:T(8,128)(2,1)S(1)}, bf16[512,512]{1,0:T(8,128)(2,1)S(1)}, u32[]{:S(2)}, u32[]{:S(2)}) %collective-permute-start.5) | collective-permute-done | bytes 524320 | tf_op jit(solution)/shard_map/ppermute | solution.py:98
  49.9 14.2 %collective-permute-done.17 = bf16[128,4096]{1,0:T(8,128)(2,1)} collective-permute-done((bf16[128,4096]{1,0:T(8,128)(2,1)}, bf16[128,4096]{1,0:T(8,128)(2,1)}, u32[]{:S(2)}, u32[]{:S(2)}) %collective-permute-start.17) | collective-permute-done | bytes 1048608 | tf_op jit(solution)/shard_map/ppermute | solution.py:98
  65.3 5.1 %norm.1 = (bf16[1024,2048]{1,0:T(8,128)(2,1)S(1)}, f32[1024,256]{1,0:T(8,128)S(1)}) custom-call(s32[1]{0:T(128)} %bitcast.core, bf16[1024,1024]{1,0:T(8,128)(2,1)S(1)} %copy-done.2, bf16[1024,1024]{1,0:T(8,128)(2,1)} %collective-permute-done.other, f32[1,2048]{1,0:T(1,128)S(1)} %bitcast.30, bf16[2048,16]{1,0:T(8,128)(2,1)S(1)} %copy.22.first, ...), custom_call_target="tpu_custom_call" | custom-call | flops 400000000 | bytes 10000000 | tf_op jit(solution)/shard_map/norm/pallas_call | solution.py:406
  70.4 15.3 %attention.1.mine = bf16[1024,2048]{1,0:T(8,128)(2,1)S(1)} custom-call(s32[6,64]{1,0:T(8,128)S(1)} %xor_bitcast_fusion.2.table, bf16[1024,2048]{1,0:T(8,128)(2,1)S(1)} %get-tuple-element.9.normed, f32[1024,256]{1,0:T(8,128)S(1)} %get-tuple-element.10.decay, bf16[1024,256]{1,0:T(8,128)(2,1)S(1)} %copy-done.15, s32[256,256]{1,0:T(8,128)S(1)} %copy-done.16, ...), custom_call_target="tpu_custom_call" | custom-call | flops 11000000512 | bytes 14000000 | tf_op jit(solution)/shard_map/attention/pallas_call | solution.py:436
  85.7 7.0 %collective-permute-start.13 = (bf16[1024,2048]{1,0:T(8,128)(2,1)S(1)}, bf16[1024,2048]{1,0:T(8,128)(2,1)S(1)}, u32[]{:S(2)}, u32[]{:S(2)}) collective-permute-start(bf16[1024,2048]{1,0:T(8,128)(2,1)S(1)} %attention.1.mine), channel_id=1, source_target_pairs={{0,1},{1,0},{2,3},{3,2},{4,5},{5,4},{6,7},{7,6},{8,9},{9,8},{10,11... | collective-permute-start | bytes 12582920 | tf_op jit(solution)/shard_map/ppermute | solution.py:94
  94.6 1.5 collective-permute-start.22
  96.1 8.3 %collective-permute-done.18 = bf16[256,1408]{1,0:T(8,128)(2,1)S(1)} collective-permute-done((bf16[256,1408]{1,0:T(8,128)(2,1)S(1)}, bf16[256,1408]{1,0:T(8,128)(2,1)S(1)}, u32[]{:S(2)}, u32[]{:S(2)}) %collective-permute-start.18) | collective-permute-done | bytes 720928 | tf_op jit(solution)/shard_map/ppermute | solution.py:98
  105.0 1.4 collective-permute-start.25
  106.5 12.4 %collective-permute-done.22 = bf16[512,1280]{1,0:T(8,128)(2,1)S(1)} collective-permute-done((bf16[512,1280]{1,0:T(8,128)(2,1)S(1)}, bf16[512,1280]{1,0:T(8,128)(2,1)S(1)}, u32[]{:S(2)}, u32[]{:S(2)}) %collective-permute-start.22) | collective-permute-done | bytes 1310752 | tf_op jit(solution)/shard_map/ppermute | solution.py:98
  120.4 2.3 %collective-permute-done.19 = bf16[512,1408]{1,0:T(8,128)(2,1)S(1)} collective-permute-done((bf16[512,1408]{1,0:T(8,128)(2,1)S(1)}, bf16[512,1408]{1,0:T(8,128)(2,1)S(1)}, u32[]{:S(2)}, u32[]{:S(2)}) %collective-permute-start.19) | collective-permute-done | bytes 1441824 | tf_op jit(solution)/shard_map/ppermute | solution.py:98
  122.8 1.2 pad_maximum_fusion.rest_0_
  125.8 6.8 %collective-permute-start.14 = (f32[1024]{0:T(1024)S(1)}, f32[1024]{0:T(1024)S(1)}, u32[]{:S(2)}, u32[]{:S(2)}) collective-permute-start(f32[1024]{0:T(1024)S(1)} %copy-done.10), channel_id=1, source_target_pairs={{0,1},{1,0},{2,3},{3,2},{4,5},{5,4},{6,7},{7,6},{8,9},{9,8},{10,11... | collective-permute-start | bytes 12296 | tf_op jit(solution)/shard_map/ppermute | solution.py:94
  132.8 1.3 pad_maximum_fusion.1.rest_4_
  139.8 2.0 %copy-done.5 = bf16[1024,2048]{1,0:T(8,128)(2,1)} copy-done((bf16[1024,2048]{1,0:T(8,128)(2,1)}, bf16[1024,2048]{1,0:T(8,128)(2,1)S(1)}, u32[]{:S(2)}) %copy-start.5) | copy-done | bytes 4194328
  142.1 2.2 %copy-done.4 = bf16[1024,2048]{1,0:T(8,128)(2,1)S(1)} copy-done((bf16[1024,2048]{1,0:T(8,128)(2,1)S(1)}, bf16[1024,2048]{1,0:T(8,128)(2,1)}, u32[]{:S(2)}) %copy-start.4) | copy-done | bytes 4194328
  144.3 2.2 %copy-done.6 = bf16[1024,2048]{1,0:T(8,128)(2,1)S(1)} copy-done((bf16[1024,2048]{1,0:T(8,128)(2,1)S(1)}, bf16[1024,2048]{1,0:T(8,128)(2,1)}, u32[]{:S(2)}) %copy-start.6) | copy-done | bytes 4194328
  146.4 5.5 %middle.1 = (bf16[1024,1024]{1,0:T(8,128)(2,1)S(1)}, bf16[1024,2048]{1,0:T(8,128)(2,1)S(1)}) custom-call(s32[1]{0:T(128)} %bitcast.core, bf16[1024,1024]{1,0:T(8,128)(2,1)S(1)} %copy-done.2, bf16[1024,1024]{1,0:T(8,128)(2,1)} %collective-permute-done.other, bf16[1024,2048]{1,0:T(8,128)(2,1)S(1)} %copy-done.4, bf16[1024,2048]{1,0:T(8,128)(2,1)S(1)} %copy-done.6, ...), custom_call_target="tpu_custom_call" | custom-call | flops 60000000 | bytes 18000000 | tf_op jit(solution)/shard_map/middle/pallas_call | solution.py:461
  152.0 14.8 %up_proj.1.squared = bf16[1024,2048]{1,0:T(8,128)(2,1)S(1)} custom-call(s32[6,64]{1,0:T(8,128)S(1)} %xor_bitcast_fusion.2.table, bf16[1024,2048]{1,0:T(8,128)(2,1)S(1)} %get-tuple-element.12.normed, bf16[1024,768]{1,0:T(8,128)(2,1)} %pad_maximum_fusion.rest_0_, bf16[1024,768]{1,0:T(8,128)(2,1)} %collective-permute-done.20.rest_1_, ...), custom_call_target="tpu_custom_call" | custom-call | flops 8700000256 | bytes 16000000 | tf_op jit(solution)/shard_map/up_proj/pallas_call | solution.py:491
  166.8 8.3 %shard_map.200 = bf16[1024,1024]{1,0:T(8,128)(2,1)S(1)} custom-call(s32[6,16]{1,0:T(8,128)S(1)} %get-tuple-element.33.places, s32[6,16]{1,0:T(8,128)S(1)} %get-tuple-element.28.targets, bf16[1024,2048]{1,0:T(8,128)(2,1)S(1)} %up_proj.1.squared, bf16[1024,640]{1,0:T(8,128)(2,1)} %pad_maximum_fusion.7.rest_0_, ...), custom_call_target="tpu_custom_call" | custom-call | flops 4300000256 | bytes 10000000 | tf_op jit(solution)/shard_map/pallas_call | solution.py:502
  175.1 7.0 %collective-permute-start.30 = (bf16[1024,1024]{1,0:T(8,128)(2,1)S(1)}, bf16[1024,1024]{1,0:T(8,128)(2,1)S(1)}, u32[]{:S(2)}, u32[]{:S(2)}) collective-permute-start(bf16[1024,1024]{1,0:T(8,128)(2,1)S(1)} %shard_map.200), channel_id=1, source_target_pairs={{0,1},{1,0},{2,3},{3,2},{4,5},{5,4},{6,7},{7,6},{8,9},{9,8},{10,11... | collective-permute-start | bytes 6291464 | tf_op jit(solution)/shard_map/ppermute | solution.py:94
  182.0 8.3 %shard_map.199 = bf16[1024,1024]{1,0:T(8,128)(2,1)S(1)} custom-call(s32[6,16]{1,0:T(8,128)S(1)} %get-tuple-element.34.places, s32[6,16]{1,0:T(8,128)S(1)} %get-tuple-element.27.targets, bf16[1024,2048]{1,0:T(8,128)(2,1)S(1)} %up_proj.1.squared, bf16[1024,640]{1,0:T(8,128)(2,1)} %pad_maximum_fusion.7.rest_0_, ...), custom_call_target="tpu_custom_call" | custom-call | flops 4300000256 | bytes 10000000 | tf_op jit(solution)/shard_map/pallas_call | solution.py:502
  192.4 2.4 %add_convert_fusion = bf16[1024,1024]{1,0:T(8,128)(2,1)} fusion(bf16[1024,1024]{1,0:T(8,128)(2,1)S(1)} %get-tuple-element.11, bf16[1024,1024]{1,0:T(8,128)(2,1)S(1)} %collective-permute-done.30, bf16[1024,1024]{1,0:T(8,128)(2,1)S(1)} %shard_map.199, f32[1024]{0:T(1024)S(1)} %copy-done.18, f32[1024]{0:T(1024)S(1)} %fusion.2), kind=kLoop, calls=%fused_computation | loop fusion | flops 8388608 | bytes 8396800 | tf_op jit(solution)/shard_map/convert_element_type | solution.py:523
  (143 shorter events, 31.7 us)
Async XLA Ops:
  2.3 5.4 %collective-permute-start.1 = (bf16[32,1536]{1,0:T(8,128)(2,1)S(1)}, bf16[32,1536]{1,0:T(8,128)(2,1)S(1)}, u32[]{:S(2)}, u32[]{:S(2)}) collective-permute-start(bf16[32,1536]{1,0:T(8,128)(2,1)S(1)} %pad_maximum_fusion.25), channel_id=1, source_target_pairs={{0,2},{1,7},{2,0},{3,5},{4,6},{5,3},{6,4},{7,1},{8,10},{9,15},{10,... | collective-permute-start | bytes 294920 | tf_op jit(solution)/shard_map/ppermute | solution.py:98
  7.7 6.1 %collective-permute-start.2 = (bf16[64,1536]{1,0:T(8,128)(2,1)S(1)}, bf16[64,1536]{1,0:T(8,128)(2,1)S(1)}, u32[]{:S(2)}, u32[]{:S(2)}) collective-permute-start(bf16[64,1536]{1,0:T(8,128)(2,1)S(1)} %pad_maximum_fusion.24), channel_id=1, source_target_pairs={{0,8},{1,25},{2,10},{3,27},{4,12},{5,29},{6,14},{7,31},{8,0},{9,17... | collective-permute-start | bytes 589832 | tf_op jit(solution)/shard_map/ppermute | solution.py:98
  13.8 9.0 %collective-permute-start.3 = (bf16[128,1536]{1,0:T(8,128)(2,1)S(1)}, bf16[128,1536]{1,0:T(8,128)(2,1)S(1)}, u32[]{:S(2)}, u32[]{:S(2)}) collective-permute-start(bf16[128,1536]{1,0:T(8,128)(2,1)S(1)} %pad_maximum_fusion.20), channel_id=1, source_target_pairs={{0,32},{1,97},{2,34},{3,99},{4,36},{5,101},{6,38},{7,103},{8,40},{... | collective-permute-start | bytes 1179656 | tf_op jit(solution)/shard_map/ppermute | solution.py:98
  17.7 6.4 %collective-permute-start.15 = (bf16[32,4096]{1,0:T(8,128)(2,1)S(1)}, bf16[32,4096]{1,0:T(8,128)(2,1)S(1)}, u32[]{:S(2)}, u32[]{:S(2)}) collective-permute-start(bf16[32,4096]{1,0:T(8,128)(2,1)S(1)} %slice_dynamic-update-slice_fusion), channel_id=1, source_target_pairs={{0,2},{1,7},{2,0},{3,5},{4,6},{5,3},{6,4},{7,1},{8,10},{9,15},{10,... | collective-permute-start | bytes 786440 | tf_op jit(solution)/shard_map/ppermute | solution.py:98
  22.9 10.3 %collective-permute-start.4 = (bf16[256,512]{1,0:T(8,128)(2,1)S(1)}, bf16[256,512]{1,0:T(8,128)(2,1)S(1)}, u32[]{:S(2)}, u32[]{:S(2)}) collective-permute-start(bf16[256,512]{1,0:T(8,128)(2,1)S(1)} %pad_maximum_fusion.21), channel_id=1, source_target_pairs={{0,6},{1,3},{2,4},{3,1},{4,2},{5,7},{6,0},{7,5},{8,14},{9,11},{10,... | collective-permute-start | bytes 786440 | tf_op jit(solution)/shard_map/ppermute | solution.py:98
  24.1 12.2 %collective-permute-start.16 = (bf16[64,4096]{1,0:T(8,128)(2,1)S(1)}, bf16[64,4096]{1,0:T(8,128)(2,1)S(1)}, u32[]{:S(2)}, u32[]{:S(2)}) collective-permute-start(bf16[64,4096]{1,0:T(8,128)(2,1)S(1)} %pad_maximum_fusion.19), channel_id=1, source_target_pairs={{0,8},{1,25},{2,10},{3,27},{4,12},{5,29},{6,14},{7,31},{8,0},{9,17... | collective-permute-start | bytes 1572872 | tf_op jit(solution)/shard_map/ppermute | solution.py:98
  26.9 8.4 %collective-permute-start.7 = (bf16[256,512]{1,0:T(8,128)(2,1)S(1)}, bf16[256,512]{1,0:T(8,128)(2,1)S(1)}, u32[]{:S(2)}, u32[]{:S(2)}) collective-permute-start(bf16[256,512]{1,0:T(8,128)(2,1)S(1)} %pad_maximum_fusion.22), channel_id=1, source_target_pairs={{0,24},{1,9},{2,26},{3,11},{4,28},{5,13},{6,30},{7,15},{8,16},{9,1... | collective-permute-start | bytes 786440 | tf_op jit(solution)/shard_map/ppermute | solution.py:98
  27.0 8.4 %collective-permute-start.10 = (bf16[256,512]{1,0:T(8,128)(2,1)S(1)}, bf16[256,512]{1,0:T(8,128)(2,1)S(1)}, u32[]{:S(2)}, u32[]{:S(2)}) collective-permute-start(bf16[256,512]{1,0:T(8,128)(2,1)S(1)} %pad_maximum_fusion.23), channel_id=1, source_target_pairs={{0,96},{1,33},{2,98},{3,35},{4,100},{5,37},{6,102},{7,39},{8,104},... | collective-permute-start | bytes 786440 | tf_op jit(solution)/shard_map/ppermute | solution.py:98
  27.1 38.1 %collective-permute-start = (bf16[1024,1024]{1,0:T(8,128)(2,1)S(1)}, bf16[1024,1024]{1,0:T(8,128)(2,1)}, u32[]{:S(2)}, u32[]{:S(2)}) collective-permute-start(bf16[1024,1024]{1,0:T(8,128)(2,1)S(1)} %copy-done.2), channel_id=1, source_target_pairs={{0,1},{1,0},{2,3},{3,2},{4,5},{5,4},{6,7},{7,6},{8,9},{9,8},{10,11... | collective-permute-start | bytes 6291464 | tf_op jit(solution)/shard_map/ppermute | solution.py:94
  33.2 9.2 %collective-permute-start.5 = (bf16[512,512]{1,0:T(8,128)(2,1)S(1)}, bf16[512,512]{1,0:T(8,128)(2,1)S(1)}, u32[]{:S(2)}, u32[]{:S(2)}) collective-permute-start(bf16[512,512]{1,0:T(8,128)(2,1)S(1)} %pad_maximum_fusion.16), channel_id=1, source_target_pairs={{0,24},{1,9},{2,26},{3,11},{4,28},{5,13},{6,30},{7,15},{8,16},{9,1... | collective-permute-start | bytes 1572872 | tf_op jit(solution)/shard_map/ppermute | solution.py:98
  35.3 9.0 %collective-permute-start.8 = (bf16[512,512]{1,0:T(8,128)(2,1)S(1)}, bf16[512,512]{1,0:T(8,128)(2,1)S(1)}, u32[]{:S(2)}, u32[]{:S(2)}) collective-permute-start(bf16[512,512]{1,0:T(8,128)(2,1)S(1)} %pad_maximum_fusion.17), channel_id=1, source_target_pairs={{0,96},{1,33},{2,98},{3,35},{4,100},{5,37},{6,102},{7,39},{8,104},... | collective-permute-start | bytes 1572872 | tf_op jit(solution)/shard_map/ppermute | solution.py:98
  35.5 10.6 %collective-permute-start.11 = (bf16[512,512]{1,0:T(8,128)(2,1)S(1)}, bf16[512,512]{1,0:T(8,128)(2,1)S(1)}, u32[]{:S(2)}, u32[]{:S(2)}) collective-permute-start(bf16[512,512]{1,0:T(8,128)(2,1)S(1)} %pad_maximum_fusion.18), channel_id=1, source_target_pairs={{0,6},{1,3},{2,4},{3,1},{4,2},{5,7},{6,0},{7,5},{8,14},{9,11},{10,... | collective-permute-start | bytes 1572872 | tf_op jit(solution)/shard_map/ppermute | solution.py:98
  37.3 26.7 %collective-permute-start.17 = (bf16[128,4096]{1,0:T(8,128)(2,1)}, bf16[128,4096]{1,0:T(8,128)(2,1)}, u32[]{:S(2)}, u32[]{:S(2)}) collective-permute-start(bf16[128,4096]{1,0:T(8,128)(2,1)} %pad_maximum_fusion.12), channel_id=1, source_target_pairs={{0,32},{1,97},{2,34},{3,99},{4,36},{5,101},{6,38},{7,103},{8,40},{... | collective-permute-start | bytes 3145736 | tf_op jit(solution)/shard_map/ppermute | solution.py:98
  43.4 26.9 %collective-permute-start.6 = (bf16[1024,512]{1,0:T(8,128)(2,1)}, bf16[1024,512]{1,0:T(8,128)(2,1)}, u32[]{:S(2)}, u32[]{:S(2)}) collective-permute-start(bf16[1024,512]{1,0:T(8,128)(2,1)} %pad_maximum_fusion.9.rest_0_), channel_id=1, source_target_pairs={{0,96},{1,33},{2,98},{3,35},{4,100},{5,37},{6,102},{7,39},{8,104},... | collective-permute-start | bytes 3145736 | tf_op jit(solution)/shard_map/ppermute | solution.py:98
  45.4 24.9 %collective-permute-start.9 = (bf16[1024,512]{1,0:T(8,128)(2,1)}, bf16[1024,512]{1,0:T(8,128)(2,1)}, u32[]{:S(2)}, u32[]{:S(2)}) collective-permute-start(bf16[1024,512]{1,0:T(8,128)(2,1)} %pad_maximum_fusion.10.rest_2_), channel_id=1, source_target_pairs={{0,6},{1,3},{2,4},{3,1},{4,2},{5,7},{6,0},{7,5},{8,14},{9,11},{10,... | collective-permute-start | bytes 3145736 | tf_op jit(solution)/shard_map/ppermute | solution.py:98
  47.1 23.3 %collective-permute-start.12 = (bf16[1024,512]{1,0:T(8,128)(2,1)}, bf16[1024,512]{1,0:T(8,128)(2,1)}, u32[]{:S(2)}, u32[]{:S(2)}) collective-permute-start(bf16[1024,512]{1,0:T(8,128)(2,1)} %pad_maximum_fusion.11.rest_4_), channel_id=1, source_target_pairs={{0,24},{1,9},{2,26},{3,11},{4,28},{5,13},{6,30},{7,15},{8,16},{9,1... | collective-permute-start | bytes 3145736 | tf_op jit(solution)/shard_map/ppermute | solution.py:98
  65.1 29.4 %collective-permute-start.21 = (bf16[256,1280]{1,0:T(8,128)(2,1)S(1)}, bf16[256,1280]{1,0:T(8,128)(2,1)S(1)}, u32[]{:S(2)}, u32[]{:S(2)}) collective-permute-start(bf16[256,1280]{1,0:T(8,128)(2,1)S(1)} %pad_maximum_fusion.15), channel_id=1, source_target_pairs={{0,24},{1,9},{2,26},{3,11},{4,28},{5,13},{6,30},{7,15},{8,16},{9,1... | collective-permute-start | bytes 1966088 | tf_op jit(solution)/shard_map/ppermute | solution.py:98
  85.7 54.1 %collective-permute-start.13 = (bf16[1024,2048]{1,0:T(8,128)(2,1)S(1)}, bf16[1024,2048]{1,0:T(8,128)(2,1)S(1)}, u32[]{:S(2)}, u32[]{:S(2)}) collective-permute-start(bf16[1024,2048]{1,0:T(8,128)(2,1)S(1)} %attention.1.mine), channel_id=1, source_target_pairs={{0,1},{1,0},{2,3},{3,2},{4,5},{5,4},{6,7},{7,6},{8,9},{9,8},{10,11... | collective-permute-start | bytes 12582920 | tf_op jit(solution)/shard_map/ppermute | solution.py:94
  93.9 10.5 %collective-permute-start.18 = (bf16[256,1408]{1,0:T(8,128)(2,1)S(1)}, bf16[256,1408]{1,0:T(8,128)(2,1)S(1)}, u32[]{:S(2)}, u32[]{:S(2)}) collective-permute-start(bf16[256,1408]{1,0:T(8,128)(2,1)S(1)} %pad_maximum_fusion.13), channel_id=1, source_target_pairs={{0,6},{1,3},{2,4},{3,1},{4,2},{5,7},{6,0},{7,5},{8,14},{9,11},{10,... | collective-permute-start | bytes 2162696 | tf_op jit(solution)/shard_map/ppermute | solution.py:98
  94.4 10.5 %collective-permute-start.24 = (bf16[256,1408]{1,0:T(8,128)(2,1)S(1)}, bf16[256,1408]{1,0:T(8,128)(2,1)S(1)}, u32[]{:S(2)}, u32[]{:S(2)}) collective-permute-start(bf16[256,1408]{1,0:T(8,128)(2,1)S(1)} %pad_maximum_fusion.14), channel_id=1, source_target_pairs={{0,96},{1,33},{2,98},{3,35},{4,100},{5,37},{6,102},{7,39},{8,104},... | collective-permute-start | bytes 2162696 | tf_op jit(solution)/shard_map/ppermute | solution.py:98
  94.6 24.4 %collective-permute-start.22 = (bf16[512,1280]{1,0:T(8,128)(2,1)S(1)}, bf16[512,1280]{1,0:T(8,128)(2,1)S(1)}, u32[]{:S(2)}, u32[]{:S(2)}) collective-permute-start(bf16[512,1280]{1,0:T(8,128)(2,1)S(1)} %pad_maximum_fusion.4), channel_id=1, source_target_pairs={{0,96},{1,33},{2,98},{3,35},{4,100},{5,37},{6,102},{7,39},{8,104},... | collective-permute-start | bytes 3932168 | tf_op jit(solution)/shard_map/ppermute | solution.py:98
  104.5 18.2 %collective-permute-start.19 = (bf16[512,1408]{1,0:T(8,128)(2,1)S(1)}, bf16[512,1408]{1,0:T(8,128)(2,1)S(1)}, u32[]{:S(2)}, u32[]{:S(2)}) collective-permute-start(bf16[512,1408]{1,0:T(8,128)(2,1)S(1)} %pad_maximum_fusion.2), channel_id=1, source_target_pairs={{0,24},{1,9},{2,26},{3,11},{4,28},{5,13},{6,30},{7,15},{8,16},{9,1... | collective-permute-start | bytes 4325384 | tf_op jit(solution)/shard_map/ppermute | solution.py:98
  105.0 19.3 %collective-permute-start.25 = (bf16[512,1408]{1,0:T(8,128)(2,1)S(1)}, bf16[512,1408]{1,0:T(8,128)(2,1)S(1)}, u32[]{:S(2)}, u32[]{:S(2)}) collective-permute-start(bf16[512,1408]{1,0:T(8,128)(2,1)S(1)} %pad_maximum_fusion.3), channel_id=1, source_target_pairs={{0,6},{1,3},{2,4},{3,1},{4,2},{5,7},{6,0},{7,5},{8,14},{9,11},{10,... | collective-permute-start | bytes 4325384 | tf_op jit(solution)/shard_map/ppermute | solution.py:98
  119.2 18.4 %collective-permute-start.23 = (bf16[1024,640]{1,0:T(8,128)(2,1)S(1)}, bf16[1024,640]{1,0:T(8,128)(2,1)S(1)}, u32[]{:S(2)}, u32[]{:S(2)}) collective-permute-start(bf16[1024,640]{1,0:T(8,128)(2,1)S(1)} %pad_maximum_fusion.5.rest_2_), channel_id=1, source_target_pairs={{0,6},{1,3},{2,4},{3,1},{4,2},{5,7},{6,0},{7,5},{8,14},{9,11},{10,... | collective-permute-start | bytes 3932168 | tf_op jit(solution)/shard_map/ppermute | solution.py:98
  124.1 27.9 %collective-permute-start.20 = (bf16[1024,768]{1,0:T(8,128)(2,1)}, bf16[1024,768]{1,0:T(8,128)(2,1)}, u32[]{:S(2)}, u32[]{:S(2)}) collective-permute-start(bf16[1024,768]{1,0:T(8,128)(2,1)} %pad_maximum_fusion.rest_0_), channel_id=1, source_target_pairs={{0,96},{1,33},{2,98},{3,35},{4,100},{5,37},{6,102},{7,39},{8,104},... | collective-permute-start | bytes 4718600 | tf_op jit(solution)/shard_map/ppermute | solution.py:98
  125.6 26.4 %collective-permute-start.26 = (bf16[1024,640]{1,0:T(8,128)(2,1)}, bf16[1024,640]{1,0:T(8,128)(2,1)}, u32[]{:S(2)}, u32[]{:S(2)}) collective-permute-start(bf16[1024,640]{1,0:T(8,128)(2,1)} %pad_maximum_fusion.6.rest_4_), channel_id=1, source_target_pairs={{0,24},{1,9},{2,26},{3,11},{4,28},{5,13},{6,30},{7,15},{8,16},{9,1... | collective-permute-start | bytes 3932168 | tf_op jit(solution)/shard_map/ppermute | solution.py:98
  125.8 8.3 %collective-permute-start.14 = (f32[1024]{0:T(1024)S(1)}, f32[1024]{0:T(1024)S(1)}, u32[]{:S(2)}, u32[]{:S(2)}) collective-permute-start(f32[1024]{0:T(1024)S(1)} %copy-done.10), channel_id=1, source_target_pairs={{0,1},{1,0},{2,3},{3,2},{4,5},{5,4},{6,7},{7,6},{8,9},{9,8},{10,11... | collective-permute-start | bytes 12296 | tf_op jit(solution)/shard_map/ppermute | solution.py:94
  134.1 32.7 %collective-permute-start.29 = (bf16[1024,768]{1,0:T(8,128)(2,1)}, bf16[1024,768]{1,0:T(8,128)(2,1)}, u32[]{:S(2)}, u32[]{:S(2)}) collective-permute-start(bf16[1024,768]{1,0:T(8,128)(2,1)} %pad_maximum_fusion.1.rest_4_), channel_id=1, source_target_pairs={{0,24},{1,9},{2,26},{3,11},{4,28},{5,13},{6,30},{7,15},{8,16},{9,1... | collective-permute-start | bytes 4718600 | tf_op jit(solution)/shard_map/ppermute | solution.py:98
  138.7 28.1 %collective-permute-start.28 = (bf16[1024,640]{1,0:T(8,128)(2,1)}, bf16[1024,640]{1,0:T(8,128)(2,1)}, u32[]{:S(2)}, u32[]{:S(2)}) collective-permute-start(bf16[1024,640]{1,0:T(8,128)(2,1)} %pad_maximum_fusion.8.rest_2_), channel_id=1, source_target_pairs={{0,6},{1,3},{2,4},{3,1},{4,2},{5,7},{6,0},{7,5},{8,14},{9,11},{10,... | collective-permute-start | bytes 3932168 | tf_op jit(solution)/shard_map/ppermute | solution.py:98
  141.8 24.9 %collective-permute-start.27 = (bf16[1024,640]{1,0:T(8,128)(2,1)}, bf16[1024,640]{1,0:T(8,128)(2,1)}, u32[]{:S(2)}, u32[]{:S(2)}) collective-permute-start(bf16[1024,640]{1,0:T(8,128)(2,1)} %pad_maximum_fusion.7.rest_0_), channel_id=1, source_target_pairs={{0,96},{1,33},{2,98},{3,35},{4,100},{5,37},{6,102},{7,39},{8,104},... | collective-permute-start | bytes 3932168 | tf_op jit(solution)/shard_map/ppermute | solution.py:98
  175.1 15.2 %collective-permute-start.30 = (bf16[1024,1024]{1,0:T(8,128)(2,1)S(1)}, bf16[1024,1024]{1,0:T(8,128)(2,1)S(1)}, u32[]{:S(2)}, u32[]{:S(2)}) collective-permute-start(bf16[1024,1024]{1,0:T(8,128)(2,1)S(1)} %shard_map.200), channel_id=1, source_target_pairs={{0,1},{1,0},{2,3},{3,2},{4,5},{5,4},{6,7},{7,6},{8,9},{9,8},{10,11... | collective-permute-start | bytes 6291464 | tf_op jit(solution)/shard_map/ppermute | solution.py:94
  191.1 1.2 collective-permute-start.31
  (23 other events, 142.0 us)

commit v2 on v1

--- a/solution.py
+++ b/solution.py
@@ -267,7 +267,7 @@
 
 
 UP_WIDTHS = (768, 640, 640)
-DOWN_WIDTHS = (640, 640, 768)
+DOWN_WIDTHS = (640, 768, 640)
 
 
 def start_of(widths, chain):
@@ -287,25 +287,25 @@
     out[...] = (values * scale * pre_gain[...]).astype(BF)
 
 
-def up_kernel(table, normed, *rest):
-    squared_out, weight, sems = rest[6:]
+def up_kernel(table, normed_hbm, *rest):
+    squared_out, weight, normed, sems = rest[6:]
+    fetch = pltpu.make_async_copy(normed_hbm, normed, sems.at[3])
+    fetch.start()
     for c in range(3):
         at = start_of(UP_WIDTHS, c)
         place_blocks(table, 3 + c, rest[2 * c : 2 * c + 2], weight, at, sems.at[c])
     for c in range(3):
-        at, width = start_of(UP_WIDTHS, c), UP_WIDTHS[c]
-        wait_part(weight, at, width, sems.at[c])
-
-        def one(i, carry, at=at, width=width):
-            here = pl.ds(pl.multiple_of(i * 256, 256), 256)
-            hidden = jnp.dot(
-                normed[here, :], weight[:, at : at + width], preferred_element_type=F32
-            )
-            hidden = jnp.maximum(hidden, 0.0)
-            squared_out[here, at : at + width] = (hidden * hidden).astype(BF)
-            return carry
-
-        lax.fori_loop(0, normed.shape[0] // 256, one, 0)
+        wait_part(weight, start_of(UP_WIDTHS, c), UP_WIDTHS[c], sems.at[c])
+    fetch.wait()
+
+    def one(i, carry):
+        here = pl.ds(pl.multiple_of(i * 256, 256), 256)
+        hidden = jnp.dot(normed[here, :], weight[...], preferred_element_type=F32)
+        hidden = jnp.maximum(hidden, 0.0)
+        squared_out[here, :] = (hidden * hidden).astype(BF)
+        return carry
+
+    lax.fori_loop(0, normed.shape[0] // 256, one, 0)
 
 
 def down_kernel(places, targets, squared, *rest):
@@ -474,7 +474,7 @@
         out_specs=[rows_of(block, 1024), rows_of(block, 2048)],
         out_shape=[
             jax.ShapeDtypeStruct((length, 1024), BF),
-            jax.ShapeDtypeStruct((length, 2048), BF),
+            pltpu.HBM((length, 2048), BF),
         ],
         name="middle",
         **params(60_000_000, 18_000_000, 20),
@@ -488,12 +488,17 @@
         other_gain.reshape(1, -1),
         feedforward_pre_gain.reshape(1, -1),
     )
+    normed_mid = pltpu.with_memory_space_constraint(normed_mid, pltpu.HBM)
     squared = pl.pallas_call(
         up_kernel,
-        in_specs=[SMEM, VMEM] + [HBM] * 6,
+        in_specs=[SMEM] + [HBM] * 7,
         out_specs=VMEM,
         out_shape=jax.ShapeDtypeStruct((length, 2048), BF),
-        scratch_shapes=[pltpu.VMEM((2048, 2048), BF), pltpu.SemaphoreType.DMA((3,))],
+        scratch_shapes=[
+            pltpu.VMEM((2048, 2048), BF),
+            pltpu.VMEM((length, 2048), BF),
+            pltpu.SemaphoreType.DMA((4,)),
+        ],
         name="up_proj",
         **params(8_700_000_000, 16_000_000, 24),
     )(table, normed_mid, *up_w)

time: 196 us -> 195 us (level)
  starting transfers between devices: 54 us -> 50.3 us
  waiting for transfers between devices: 50.9 us -> 53.4 us
    ppermute x27, starting transfers between devices: 27.1 us -> 23.2 us  [over_link(): return lax.ppermute(array, ALL, partner_pairs(step, chain))]
    ppermute x27, waiting for transfers between devices: 49.7 us -> 52.2 us  [over_link(): return lax.ppermute(array, ALL, partner_pairs(step, chain))]
  transfers between devices with their start and end apart: 32 -> 32, of which waited for: 14 -> 13; matrix products, arithmetic and copies ran while one was open for 10% -> 10% of each run, Pallas kernels for 25% -> 25%
where the time goes in v2:
time: 195 us; the launch traced here: 194 us
  Pallas kernels  57.5 us (29%)
  waiting for transfers between devices  53.4 us (27%)
  starting transfers between devices  50.3 us (26%)
  local copies, waits for them, and re-layouts  17.8 us (9%)
  other arithmetic  14.4 us (7%)
    ppermute x27, waiting for transfers between devices, over_link(): return lax.ppermute(array, ALL, partner_pairs(step, chain))  52.2 us
    ppermute x5, starting transfers between devices, swap_cores(): return lax.ppermute(array, 'tp', [(0, 1), (1, 0)])  27.2 us
    ppermute x27, starting transfers between devices, over_link(): return lax.ppermute(array, ALL, partner_pairs(step, chain))  23.2 us
    pallas_call x2, Pallas kernels, down_half(): pl.pallas_call(down_kernel, in_specs=[SMEM, SMEM, VMEM] + [HBM] * 6, out_...  16.5 us
    pallas_call x1, Pallas kernels, on_device(): pl.pallas_call(attention_kernel, in_specs=[SMEM] + [VMEM] * 5 + [HBM] * 6...  15.3 us
    pallas_call x1, Pallas kernels, on_device(): pl.pallas_call(up_kernel, in_specs=[SMEM] + [HBM] * 7, out_specs=VMEM, ou...  13.8 us
    concatenate x25, other arithmetic, joined(): return jnp.concatenate([a, b], axis=0)  11.2 us
    unnamed x53, local copies, waits for them, and re-layouts  10.5 us
  transfers between devices with their start and end apart: 32, of which 13 were waited for; matrix products, arithmetic and copies ran while one was open for 10% of the time, Pallas kernels for 25%

profile of v2, /device:TPU:1, one launch (start us, length us, event | category | flops | bytes accessed | tf_op | source)
XLA Modules:
  0.0 194.1 jit_solution(12908494894515723130)
XLA Ops:
  2.3 3.4 %collective-permute-start.1 = (bf16[32,1536]{1,0:T(8,128)(2,1)S(1)}, bf16[32,1536]{1,0:T(8,128)(2,1)S(1)}, u32[]{:S(2)}, u32[]{:S(2)}) collective-permute-start(bf16[32,1536]{1,0:T(8,128)(2,1)S(1)} %pad_maximum_fusion.25), channel_id=1, source_target_pairs={{0,2},{1,7},{2,0},{3,5},{4,6},{5,3},{6,4},{7,1},{8,10},{9,15},{10,... | collective-permute-start | bytes 294920 | tf_op jit(solution)/shard_map/ppermute | solution.py:98
  7.7 3.0 %collective-permute-start.2 = (bf16[64,1536]{1,0:T(8,128)(2,1)S(1)}, bf16[64,1536]{1,0:T(8,128)(2,1)S(1)}, u32[]{:S(2)}, u32[]{:S(2)}) collective-permute-start(bf16[64,1536]{1,0:T(8,128)(2,1)S(1)} %pad_maximum_fusion.24), channel_id=1, source_target_pairs={{0,8},{1,25},{2,10},{3,27},{4,12},{5,29},{6,14},{7,31},{8,0},{9,17... | collective-permute-start | bytes 589832 | tf_op jit(solution)/shard_map/ppermute | solution.py:98
  11.5 2.3 %collective-permute-done.2 = bf16[64,1536]{1,0:T(8,128)(2,1)S(1)} collective-permute-done((bf16[64,1536]{1,0:T(8,128)(2,1)S(1)}, bf16[64,1536]{1,0:T(8,128)(2,1)S(1)}, u32[]{:S(2)}, u32[]{:S(2)}) %collective-permute-start.2) | collective-permute-done | bytes 196640 | tf_op jit(solution)/shard_map/ppermute | solution.py:98
  13.8 3.8 %collective-permute-start.3 = (bf16[128,1536]{1,0:T(8,128)(2,1)S(1)}, bf16[128,1536]{1,0:T(8,128)(2,1)S(1)}, u32[]{:S(2)}, u32[]{:S(2)}) collective-permute-start(bf16[128,1536]{1,0:T(8,128)(2,1)S(1)} %pad_maximum_fusion.20), channel_id=1, source_target_pairs={{0,32},{1,97},{2,34},{3,99},{4,36},{5,101},{6,38},{7,103},{8,40},{... | collective-permute-start | bytes 1179656 | tf_op jit(solution)/shard_map/ppermute | solution.py:98
  17.7 2.6 %collective-permute-start.15 = (bf16[32,4096]{1,0:T(8,128)(2,1)S(1)}, bf16[32,4096]{1,0:T(8,128)(2,1)S(1)}, u32[]{:S(2)}, u32[]{:S(2)}) collective-permute-start(bf16[32,4096]{1,0:T(8,128)(2,1)S(1)} %slice_dynamic-update-slice_fusion.1), channel_id=1, source_target_pairs={{0,2},{1,7},{2,0},{3,5},{4,6},{5,3},{6,4},{7,1},{8,10},{9,15},{10,... | collective-permute-start | bytes 786440 | tf_op jit(solution)/shard_map/ppermute | solution.py:98
  20.3 2.6 %collective-permute-done.3 = bf16[128,1536]{1,0:T(8,128)(2,1)S(1)} collective-permute-done((bf16[128,1536]{1,0:T(8,128)(2,1)S(1)}, bf16[128,1536]{1,0:T(8,128)(2,1)S(1)}, u32[]{:S(2)}, u32[]{:S(2)}) %collective-permute-start.3) | collective-permute-done | bytes 393248 | tf_op jit(solution)/shard_map/ppermute | solution.py:98
  23.0 1.2 collective-permute-done.15
  24.2 2.8 %collective-permute-start.16 = (bf16[64,4096]{1,0:T(8,128)(2,1)S(1)}, bf16[64,4096]{1,0:T(8,128)(2,1)S(1)}, u32[]{:S(2)}, u32[]{:S(2)}) collective-permute-start(bf16[64,4096]{1,0:T(8,128)(2,1)S(1)} %pad_maximum_fusion.19), channel_id=1, source_target_pairs={{0,8},{1,25},{2,10},{3,27},{4,12},{5,29},{6,14},{7,31},{8,0},{9,17... | collective-permute-start | bytes 1572872 | tf_op jit(solution)/shard_map/ppermute | solution.py:98
  27.2 6.0 %collective-permute-start = (bf16[1024,1024]{1,0:T(8,128)(2,1)S(1)}, bf16[1024,1024]{1,0:T(8,128)(2,1)}, u32[]{:S(2)}, u32[]{:S(2)}) collective-permute-start(bf16[1024,1024]{1,0:T(8,128)(2,1)S(1)} %copy-done.2), channel_id=1, source_target_pairs={{0,1},{1,0},{2,3},{3,2},{4,5},{5,4},{6,7},{7,6},{8,9},{9,8},{10,11... | collective-permute-start | bytes 6291464 | tf_op jit(solution)/shard_map/ppermute | solution.py:94
  33.7 1.7 collective-permute-done.7
  37.5 2.1 %collective-permute-start.17 = (bf16[128,4096]{1,0:T(8,128)(2,1)}, bf16[128,4096]{1,0:T(8,128)(2,1)}, u32[]{:S(2)}, u32[]{:S(2)}) collective-permute-start(bf16[128,4096]{1,0:T(8,128)(2,1)} %pad_maximum_fusion.12), channel_id=1, source_target_pairs={{0,32},{1,97},{2,34},{3,99},{4,36},{5,101},{6,38},{7,103},{8,40},{... | collective-permute-start | bytes 3145736 | tf_op jit(solution)/shard_map/ppermute | solution.py:98
  39.6 2.7 %collective-permute-done.5 = bf16[512,512]{1,0:T(8,128)(2,1)S(1)} collective-permute-done((bf16[512,512]{1,0:T(8,128)(2,1)S(1)}, bf16[512,512]{1,0:T(8,128)(2,1)S(1)}, u32[]{:S(2)}, u32[]{:S(2)}) %collective-permute-start.5) | collective-permute-done | bytes 524320 | tf_op jit(solution)/shard_map/ppermute | solution.py:98
  49.9 14.3 %collective-permute-done.17 = bf16[128,4096]{1,0:T(8,128)(2,1)} collective-permute-done((bf16[128,4096]{1,0:T(8,128)(2,1)}, bf16[128,4096]{1,0:T(8,128)(2,1)}, u32[]{:S(2)}, u32[]{:S(2)}) %collective-permute-start.17) | collective-permute-done | bytes 1048608 | tf_op jit(solution)/shard_map/ppermute | solution.py:98
  65.6 5.1 %norm.1 = (bf16[1024,2048]{1,0:T(8,128)(2,1)S(1)}, f32[1024,256]{1,0:T(8,128)S(1)}) custom-call(s32[1]{0:T(128)} %bitcast.core, bf16[1024,1024]{1,0:T(8,128)(2,1)S(1)} %copy-done.2, bf16[1024,1024]{1,0:T(8,128)(2,1)} %collective-permute-done.other, f32[1,2048]{1,0:T(1,128)S(1)} %bitcast.30, bf16[2048,16]{1,0:T(8,128)(2,1)S(1)} %copy.22.first, ...), custom_call_target="tpu_custom_call" | custom-call | flops 400000000 | bytes 10000000 | tf_op jit(solution)/shard_map/norm/pallas_call | solution.py:406
  70.8 15.3 %attention.1.mine = bf16[1024,2048]{1,0:T(8,128)(2,1)S(1)} custom-call(s32[6,64]{1,0:T(8,128)S(1)} %xor_bitcast_fusion.2.table, bf16[1024,2048]{1,0:T(8,128)(2,1)S(1)} %get-tuple-element.9.normed, f32[1024,256]{1,0:T(8,128)S(1)} %get-tuple-element.10.decay, bf16[1024,256]{1,0:T(8,128)(2,1)S(1)} %copy-done.15, s32[256,256]{1,0:T(8,128)S(1)} %copy-done.16, ...), custom_call_target="tpu_custom_call" | custom-call | flops 11000000512 | bytes 14000000 | tf_op jit(solution)/shard_map/attention/pallas_call | solution.py:436
  86.1 6.0 %collective-permute-start.13 = (bf16[1024,2048]{1,0:T(8,128)(2,1)S(1)}, bf16[1024,2048]{1,0:T(8,128)(2,1)S(1)}, u32[]{:S(2)}, u32[]{:S(2)}) collective-permute-start(bf16[1024,2048]{1,0:T(8,128)(2,1)S(1)} %attention.1.mine), channel_id=1, source_target_pairs={{0,1},{1,0},{2,3},{3,2},{4,5},{5,4},{6,7},{7,6},{8,9},{9,8},{10,11... | collective-permute-start | bytes 12582920 | tf_op jit(solution)/shard_map/ppermute | solution.py:94
  95.1 8.6 %collective-permute-done.18 = bf16[256,1408]{1,0:T(8,128)(2,1)S(1)} collective-permute-done((bf16[256,1408]{1,0:T(8,128)(2,1)S(1)}, bf16[256,1408]{1,0:T(8,128)(2,1)S(1)}, u32[]{:S(2)}, u32[]{:S(2)}) %collective-permute-start.18) | collective-permute-done | bytes 720928 | tf_op jit(solution)/shard_map/ppermute | solution.py:98
  104.5 13.3 %collective-permute-done.25 = bf16[512,1280]{1,0:T(8,128)(2,1)S(1)} collective-permute-done((bf16[512,1280]{1,0:T(8,128)(2,1)S(1)}, bf16[512,1280]{1,0:T(8,128)(2,1)S(1)}, u32[]{:S(2)}, u32[]{:S(2)}) %collective-permute-start.25) | collective-permute-done | bytes 1310752 | tf_op jit(solution)/shard_map/ppermute | solution.py:98
  118.2 3.9 %collective-permute-done.19 = bf16[512,1408]{1,0:T(8,128)(2,1)S(1)} collective-permute-done((bf16[512,1408]{1,0:T(8,128)(2,1)S(1)}, bf16[512,1408]{1,0:T(8,128)(2,1)S(1)}, u32[]{:S(2)}, u32[]{:S(2)}) %collective-permute-start.19) | collective-permute-done | bytes 1441824 | tf_op jit(solution)/shard_map/ppermute | solution.py:98
  122.2 1.2 pad_maximum_fusion.rest_0_
  125.2 6.6 %collective-permute-start.14 = (f32[1024]{0:T(1024)S(1)}, f32[1024]{0:T(1024)S(1)}, u32[]{:S(2)}, u32[]{:S(2)}) collective-permute-start(f32[1024]{0:T(1024)S(1)} %copy-done.10), channel_id=1, source_target_pairs={{0,1},{1,0},{2,3},{3,2},{4,5},{5,4},{6,7},{7,6},{8,9},{9,8},{10,11... | collective-permute-start | bytes 12296 | tf_op jit(solution)/shard_map/ppermute | solution.py:94
  131.9 1.3 pad_maximum_fusion.1.rest_2_
  133.2 1.2 pad_maximum_fusion.8.rest_4_
  137.4 2.0 %copy-done.5 = bf16[1024,2048]{1,0:T(8,128)(2,1)} copy-done((bf16[1024,2048]{1,0:T(8,128)(2,1)}, bf16[1024,2048]{1,0:T(8,128)(2,1)S(1)}, u32[]{:S(2)}) %copy-start.5) | copy-done | bytes 4194328
  139.5 2.2 %copy-done.4 = bf16[1024,2048]{1,0:T(8,128)(2,1)S(1)} copy-done((bf16[1024,2048]{1,0:T(8,128)(2,1)S(1)}, bf16[1024,2048]{1,0:T(8,128)(2,1)}, u32[]{:S(2)}) %copy-start.4) | copy-done | bytes 4194328
  141.6 2.2 %copy-done.6 = bf16[1024,2048]{1,0:T(8,128)(2,1)S(1)} copy-done((bf16[1024,2048]{1,0:T(8,128)(2,1)S(1)}, bf16[1024,2048]{1,0:T(8,128)(2,1)}, u32[]{:S(2)}) %copy-start.6) | copy-done | bytes 4194328
  143.8 6.8 %middle.1 = (bf16[1024,1024]{1,0:T(8,128)(2,1)S(1)}, bf16[1024,2048]{1,0:T(8,128)(2,1)}) custom-call(s32[1]{0:T(128)} %bitcast.core, bf16[1024,1024]{1,0:T(8,128)(2,1)S(1)} %copy-done.2, bf16[1024,1024]{1,0:T(8,128)(2,1)} %collective-permute-done.other, bf16[1024,2048]{1,0:T(8,128)(2,1)S(1)} %copy-done.4, bf16[1024,2048]{1,0:T(8,128)(2,1)S(1)} %copy-done.6, ...), custom_call_target="tpu_custom_call" | custom-call | flops 60000000 | bytes 18000000 | tf_op jit(solution)/shard_map/middle/pallas_call | solution.py:461
  150.7 13.8 %up_proj.1.squared = bf16[1024,2048]{1,0:T(8,128)(2,1)S(1)} custom-call(s32[6,64]{1,0:T(8,128)S(1)} %xor_bitcast_fusion.2.table, bf16[1024,2048]{1,0:T(8,128)(2,1)} %get-tuple-element.12.normed_hbm, bf16[1024,768]{1,0:T(8,128)(2,1)} %pad_maximum_fusion.rest_0_, bf16[1024,768]{1,0:T(8,128)(2,1)} %collective-permute-done.20.rest_1_, ...), custom_call_target="tpu_custom_call" | custom-call | flops 8700000256 | bytes 16000000 | tf_op jit(solution)/shard_map/up_proj/pallas_call | solution.py:492
  164.5 8.3 %shard_map.200 = bf16[1024,1024]{1,0:T(8,128)(2,1)S(1)} custom-call(s32[6,16]{1,0:T(8,128)S(1)} %get-tuple-element.33.places, s32[6,16]{1,0:T(8,128)S(1)} %get-tuple-element.28.targets, bf16[1024,2048]{1,0:T(8,128)(2,1)S(1)} %up_proj.1.squared, bf16[1024,640]{1,0:T(8,128)(2,1)} %pad_maximum_fusion.7.rest_0_, ...), custom_call_target="tpu_custom_call" | custom-call | flops 4300000256 | bytes 10000000 | tf_op jit(solution)/shard_map/pallas_call | solution.py:507
  172.8 8.6 %collective-permute-start.30 = (bf16[1024,1024]{1,0:T(8,128)(2,1)S(1)}, bf16[1024,1024]{1,0:T(8,128)(2,1)S(1)}, u32[]{:S(2)}, u32[]{:S(2)}) collective-permute-start(bf16[1024,1024]{1,0:T(8,128)(2,1)S(1)} %shard_map.200), channel_id=1, source_target_pairs={{0,1},{1,0},{2,3},{3,2},{4,5},{5,4},{6,7},{7,6},{8,9},{9,8},{10,11... | collective-permute-start | bytes 6291464 | tf_op jit(solution)/shard_map/ppermute | solution.py:94
  181.4 8.2 %shard_map.199 = bf16[1024,1024]{1,0:T(8,128)(2,1)S(1)} custom-call(s32[6,16]{1,0:T(8,128)S(1)} %get-tuple-element.34.places, s32[6,16]{1,0:T(8,128)S(1)} %get-tuple-element.27.targets, bf16[1024,2048]{1,0:T(8,128)(2,1)S(1)} %up_proj.1.squared, bf16[1024,640]{1,0:T(8,128)(2,1)} %pad_maximum_fusion.7.rest_0_, ...), custom_call_target="tpu_custom_call" | custom-call | flops 4300000256 | bytes 10000000 | tf_op jit(solution)/shard_map/pallas_call | solution.py:507
  191.7 2.4 %add_convert_fusion = bf16[1024,1024]{1,0:T(8,128)(2,1)} fusion(bf16[1024,1024]{1,0:T(8,128)(2,1)S(1)} %get-tuple-element.11, bf16[1024,1024]{1,0:T(8,128)(2,1)S(1)} %collective-permute-done.30, bf16[1024,1024]{1,0:T(8,128)(2,1)S(1)} %shard_map.199, f32[1024]{0:T(1024)S(1)} %copy-done.18, f32[1024]{0:T(1024)S(1)} %fusion.2), kind=kLoop, calls=%fused_computation | loop fusion | flops 8388608 | bytes 8396800 | tf_op jit(solution)/shard_map/convert_element_type | solution.py:528
  (143 shorter events, 28.1 us)
Async XLA Ops:
  2.3 5.4 %collective-permute-start.1 = (bf16[32,1536]{1,0:T(8,128)(2,1)S(1)}, bf16[32,1536]{1,0:T(8,128)(2,1)S(1)}, u32[]{:S(2)}, u32[]{:S(2)}) collective-permute-start(bf16[32,1536]{1,0:T(8,128)(2,1)S(1)} %pad_maximum_fusion.25), channel_id=1, source_target_pairs={{0,2},{1,7},{2,0},{3,5},{4,6},{5,3},{6,4},{7,1},{8,10},{9,15},{10,... | collective-permute-start | bytes 294920 | tf_op jit(solution)/shard_map/ppermute | solution.py:98
  7.7 6.1 %collective-permute-start.2 = (bf16[64,1536]{1,0:T(8,128)(2,1)S(1)}, bf16[64,1536]{1,0:T(8,128)(2,1)S(1)}, u32[]{:S(2)}, u32[]{:S(2)}) collective-permute-start(bf16[64,1536]{1,0:T(8,128)(2,1)S(1)} %pad_maximum_fusion.24), channel_id=1, source_target_pairs={{0,8},{1,25},{2,10},{3,27},{4,12},{5,29},{6,14},{7,31},{8,0},{9,17... | collective-permute-start | bytes 589832 | tf_op jit(solution)/shard_map/ppermute | solution.py:98
  13.8 9.0 %collective-permute-start.3 = (bf16[128,1536]{1,0:T(8,128)(2,1)S(1)}, bf16[128,1536]{1,0:T(8,128)(2,1)S(1)}, u32[]{:S(2)}, u32[]{:S(2)}) collective-permute-start(bf16[128,1536]{1,0:T(8,128)(2,1)S(1)} %pad_maximum_fusion.20), channel_id=1, source_target_pairs={{0,32},{1,97},{2,34},{3,99},{4,36},{5,101},{6,38},{7,103},{8,40},{... | collective-permute-start | bytes 1179656 | tf_op jit(solution)/shard_map/ppermute | solution.py:98
  17.7 6.5 %collective-permute-start.15 = (bf16[32,4096]{1,0:T(8,128)(2,1)S(1)}, bf16[32,4096]{1,0:T(8,128)(2,1)S(1)}, u32[]{:S(2)}, u32[]{:S(2)}) collective-permute-start(bf16[32,4096]{1,0:T(8,128)(2,1)S(1)} %slice_dynamic-update-slice_fusion.1), channel_id=1, source_target_pairs={{0,2},{1,7},{2,0},{3,5},{4,6},{5,3},{6,4},{7,1},{8,10},{9,15},{10,... | collective-permute-start | bytes 786440 | tf_op jit(solution)/shard_map/ppermute | solution.py:98
  22.9 10.3 %collective-permute-start.4 = (bf16[256,512]{1,0:T(8,128)(2,1)S(1)}, bf16[256,512]{1,0:T(8,128)(2,1)S(1)}, u32[]{:S(2)}, u32[]{:S(2)}) collective-permute-start(bf16[256,512]{1,0:T(8,128)(2,1)S(1)} %pad_maximum_fusion.21), channel_id=1, source_target_pairs={{0,6},{1,3},{2,4},{3,1},{4,2},{5,7},{6,0},{7,5},{8,14},{9,11},{10,... | collective-permute-start | bytes 786440 | tf_op jit(solution)/shard_map/ppermute | solution.py:98
  24.2 12.2 %collective-permute-start.16 = (bf16[64,4096]{1,0:T(8,128)(2,1)S(1)}, bf16[64,4096]{1,0:T(8,128)(2,1)S(1)}, u32[]{:S(2)}, u32[]{:S(2)}) collective-permute-start(bf16[64,4096]{1,0:T(8,128)(2,1)S(1)} %pad_maximum_fusion.19), channel_id=1, source_target_pairs={{0,8},{1,25},{2,10},{3,27},{4,12},{5,29},{6,14},{7,31},{8,0},{9,17... | collective-permute-start | bytes 1572872 | tf_op jit(solution)/shard_map/ppermute | solution.py:98
  27.0 8.4 %collective-permute-start.7 = (bf16[256,512]{1,0:T(8,128)(2,1)S(1)}, bf16[256,512]{1,0:T(8,128)(2,1)S(1)}, u32[]{:S(2)}, u32[]{:S(2)}) collective-permute-start(bf16[256,512]{1,0:T(8,128)(2,1)S(1)} %pad_maximum_fusion.22), channel_id=1, source_target_pairs={{0,24},{1,9},{2,26},{3,11},{4,28},{5,13},{6,30},{7,15},{8,16},{9,1... | collective-permute-start | bytes 786440 | tf_op jit(solution)/shard_map/ppermute | solution.py:98
  27.1 8.4 %collective-permute-start.10 = (bf16[256,512]{1,0:T(8,128)(2,1)S(1)}, bf16[256,512]{1,0:T(8,128)(2,1)S(1)}, u32[]{:S(2)}, u32[]{:S(2)}) collective-permute-start(bf16[256,512]{1,0:T(8,128)(2,1)S(1)} %pad_maximum_fusion.23), channel_id=1, source_target_pairs={{0,96},{1,33},{2,98},{3,35},{4,100},{5,37},{6,102},{7,39},{8,104},... | collective-permute-start | bytes 786440 | tf_op jit(solution)/shard_map/ppermute | solution.py:98
  27.2 38.4 %collective-permute-start = (bf16[1024,1024]{1,0:T(8,128)(2,1)S(1)}, bf16[1024,1024]{1,0:T(8,128)(2,1)}, u32[]{:S(2)}, u32[]{:S(2)}) collective-permute-start(bf16[1024,1024]{1,0:T(8,128)(2,1)S(1)} %copy-done.2), channel_id=1, source_target_pairs={{0,1},{1,0},{2,3},{3,2},{4,5},{5,4},{6,7},{7,6},{8,9},{9,8},{10,11... | collective-permute-start | bytes 6291464 | tf_op jit(solution)/shard_map/ppermute | solution.py:94
  33.2 9.2 %collective-permute-start.5 = (bf16[512,512]{1,0:T(8,128)(2,1)S(1)}, bf16[512,512]{1,0:T(8,128)(2,1)S(1)}, u32[]{:S(2)}, u32[]{:S(2)}) collective-permute-start(bf16[512,512]{1,0:T(8,128)(2,1)S(1)} %pad_maximum_fusion.16), channel_id=1, source_target_pairs={{0,24},{1,9},{2,26},{3,11},{4,28},{5,13},{6,30},{7,15},{8,16},{9,1... | collective-permute-start | bytes 1572872 | tf_op jit(solution)/shard_map/ppermute | solution.py:98
  35.4 9.0 %collective-permute-start.8 = (bf16[512,512]{1,0:T(8,128)(2,1)S(1)}, bf16[512,512]{1,0:T(8,128)(2,1)S(1)}, u32[]{:S(2)}, u32[]{:S(2)}) collective-permute-start(bf16[512,512]{1,0:T(8,128)(2,1)S(1)} %pad_maximum_fusion.17), channel_id=1, source_target_pairs={{0,96},{1,33},{2,98},{3,35},{4,100},{5,37},{6,102},{7,39},{8,104},... | collective-permute-start | bytes 1572872 | tf_op jit(solution)/shard_map/ppermute | solution.py:98
  35.6 10.5 %collective-permute-start.11 = (bf16[512,512]{1,0:T(8,128)(2,1)S(1)}, bf16[512,512]{1,0:T(8,128)(2,1)S(1)}, u32[]{:S(2)}, u32[]{:S(2)}) collective-permute-start(bf16[512,512]{1,0:T(8,128)(2,1)S(1)} %pad_maximum_fusion.18), channel_id=1, source_target_pairs={{0,6},{1,3},{2,4},{3,1},{4,2},{5,7},{6,0},{7,5},{8,14},{9,11},{10,... | collective-permute-start | bytes 1572872 | tf_op jit(solution)/shard_map/ppermute | solution.py:98
  37.5 26.7 %collective-permute-start.17 = (bf16[128,4096]{1,0:T(8,128)(2,1)}, bf16[128,4096]{1,0:T(8,128)(2,1)}, u32[]{:S(2)}, u32[]{:S(2)}) collective-permute-start(bf16[128,4096]{1,0:T(8,128)(2,1)} %pad_maximum_fusion.12), channel_id=1, source_target_pairs={{0,32},{1,97},{2,34},{3,99},{4,36},{5,101},{6,38},{7,103},{8,40},{... | collective-permute-start | bytes 3145736 | tf_op jit(solution)/shard_map/ppermute | solution.py:98
  43.4 27.3 %collective-permute-start.6 = (bf16[1024,512]{1,0:T(8,128)(2,1)}, bf16[1024,512]{1,0:T(8,128)(2,1)}, u32[]{:S(2)}, u32[]{:S(2)}) collective-permute-start(bf16[1024,512]{1,0:T(8,128)(2,1)} %pad_maximum_fusion.9.rest_0_), channel_id=1, source_target_pairs={{0,96},{1,33},{2,98},{3,35},{4,100},{5,37},{6,102},{7,39},{8,104},... | collective-permute-start | bytes 3145736 | tf_op jit(solution)/shard_map/ppermute | solution.py:98
  45.5 25.2 %collective-permute-start.9 = (bf16[1024,512]{1,0:T(8,128)(2,1)}, bf16[1024,512]{1,0:T(8,128)(2,1)}, u32[]{:S(2)}, u32[]{:S(2)}) collective-permute-start(bf16[1024,512]{1,0:T(8,128)(2,1)} %pad_maximum_fusion.10.rest_2_), channel_id=1, source_target_pairs={{0,6},{1,3},{2,4},{3,1},{4,2},{5,7},{6,0},{7,5},{8,14},{9,11},{10,... | collective-permute-start | bytes 3145736 | tf_op jit(solution)/shard_map/ppermute | solution.py:98
  47.1 23.6 %collective-permute-start.12 = (bf16[1024,512]{1,0:T(8,128)(2,1)}, bf16[1024,512]{1,0:T(8,128)(2,1)}, u32[]{:S(2)}, u32[]{:S(2)}) collective-permute-start(bf16[1024,512]{1,0:T(8,128)(2,1)} %pad_maximum_fusion.11.rest_4_), channel_id=1, source_target_pairs={{0,24},{1,9},{2,26},{3,11},{4,28},{5,13},{6,30},{7,15},{8,16},{9,1... | collective-permute-start | bytes 3145736 | tf_op jit(solution)/shard_map/ppermute | solution.py:98
  65.3 29.3 %collective-permute-start.24 = (bf16[256,1280]{1,0:T(8,128)(2,1)S(1)}, bf16[256,1280]{1,0:T(8,128)(2,1)S(1)}, u32[]{:S(2)}, u32[]{:S(2)}) collective-permute-start(bf16[256,1280]{1,0:T(8,128)(2,1)S(1)} %pad_maximum_fusion.15), channel_id=1, source_target_pairs={{0,96},{1,33},{2,98},{3,35},{4,100},{5,37},{6,102},{7,39},{8,104},... | collective-permute-start | bytes 1966088 | tf_op jit(solution)/shard_map/ppermute | solution.py:98
  86.1 51.3 %collective-permute-start.13 = (bf16[1024,2048]{1,0:T(8,128)(2,1)S(1)}, bf16[1024,2048]{1,0:T(8,128)(2,1)S(1)}, u32[]{:S(2)}, u32[]{:S(2)}) collective-permute-start(bf16[1024,2048]{1,0:T(8,128)(2,1)S(1)} %attention.1.mine), channel_id=1, source_target_pairs={{0,1},{1,0},{2,3},{3,2},{4,5},{5,4},{6,7},{7,6},{8,9},{9,8},{10,11... | collective-permute-start | bytes 12582920 | tf_op jit(solution)/shard_map/ppermute | solution.py:94
  93.3 10.5 %collective-permute-start.18 = (bf16[256,1408]{1,0:T(8,128)(2,1)S(1)}, bf16[256,1408]{1,0:T(8,128)(2,1)S(1)}, u32[]{:S(2)}, u32[]{:S(2)}) collective-permute-start(bf16[256,1408]{1,0:T(8,128)(2,1)S(1)} %pad_maximum_fusion.13), channel_id=1, source_target_pairs={{0,6},{1,3},{2,4},{3,1},{4,2},{5,7},{6,0},{7,5},{8,14},{9,11},{10,... | collective-permute-start | bytes 2162696 | tf_op jit(solution)/shard_map/ppermute | solution.py:98
  93.4 10.6 %collective-permute-start.21 = (bf16[256,1408]{1,0:T(8,128)(2,1)S(1)}, bf16[256,1408]{1,0:T(8,128)(2,1)S(1)}, u32[]{:S(2)}, u32[]{:S(2)}) collective-permute-start(bf16[256,1408]{1,0:T(8,128)(2,1)S(1)} %pad_maximum_fusion.14), channel_id=1, source_target_pairs={{0,24},{1,9},{2,26},{3,11},{4,28},{5,13},{6,30},{7,15},{8,16},{9,1... | collective-permute-start | bytes 2162696 | tf_op jit(solution)/shard_map/ppermute | solution.py:98
  94.6 23.2 %collective-permute-start.25 = (bf16[512,1280]{1,0:T(8,128)(2,1)S(1)}, bf16[512,1280]{1,0:T(8,128)(2,1)S(1)}, u32[]{:S(2)}, u32[]{:S(2)}) collective-permute-start(bf16[512,1280]{1,0:T(8,128)(2,1)S(1)} %pad_maximum_fusion.5), channel_id=1, source_target_pairs={{0,6},{1,3},{2,4},{3,1},{4,2},{5,7},{6,0},{7,5},{8,14},{9,11},{10,... | collective-permute-start | bytes 3932168 | tf_op jit(solution)/shard_map/ppermute | solution.py:98
  103.9 18.2 %collective-permute-start.19 = (bf16[512,1408]{1,0:T(8,128)(2,1)S(1)}, bf16[512,1408]{1,0:T(8,128)(2,1)S(1)}, u32[]{:S(2)}, u32[]{:S(2)}) collective-permute-start(bf16[512,1408]{1,0:T(8,128)(2,1)S(1)} %pad_maximum_fusion.2), channel_id=1, source_target_pairs={{0,24},{1,9},{2,26},{3,11},{4,28},{5,13},{6,30},{7,15},{8,16},{9,1... | collective-permute-start | bytes 4325384 | tf_op jit(solution)/shard_map/ppermute | solution.py:98
  104.1 19.4 %collective-permute-start.22 = (bf16[512,1408]{1,0:T(8,128)(2,1)S(1)}, bf16[512,1408]{1,0:T(8,128)(2,1)S(1)}, u32[]{:S(2)}, u32[]{:S(2)}) collective-permute-start(bf16[512,1408]{1,0:T(8,128)(2,1)S(1)} %pad_maximum_fusion.3), channel_id=1, source_target_pairs={{0,96},{1,33},{2,98},{3,35},{4,100},{5,37},{6,102},{7,39},{8,104},... | collective-permute-start | bytes 4325384 | tf_op jit(solution)/shard_map/ppermute | solution.py:98
  118.1 18.2 %collective-permute-start.26 = (bf16[1024,640]{1,0:T(8,128)(2,1)S(1)}, bf16[1024,640]{1,0:T(8,128)(2,1)S(1)}, u32[]{:S(2)}, u32[]{:S(2)}) collective-permute-start(bf16[1024,640]{1,0:T(8,128)(2,1)S(1)} %pad_maximum_fusion.6.rest_4_), channel_id=1, source_target_pairs={{0,24},{1,9},{2,26},{3,11},{4,28},{5,13},{6,30},{7,15},{8,16},{9,1... | collective-permute-start | bytes 3932168 | tf_op jit(solution)/shard_map/ppermute | solution.py:98
  123.4 27.3 %collective-permute-start.20 = (bf16[1024,768]{1,0:T(8,128)(2,1)}, bf16[1024,768]{1,0:T(8,128)(2,1)}, u32[]{:S(2)}, u32[]{:S(2)}) collective-permute-start(bf16[1024,768]{1,0:T(8,128)(2,1)} %pad_maximum_fusion.rest_0_), channel_id=1, source_target_pairs={{0,96},{1,33},{2,98},{3,35},{4,100},{5,37},{6,102},{7,39},{8,104},... | collective-permute-start | bytes 4718600 | tf_op jit(solution)/shard_map/ppermute | solution.py:98
  124.8 25.9 %collective-permute-start.23 = (bf16[1024,640]{1,0:T(8,128)(2,1)}, bf16[1024,640]{1,0:T(8,128)(2,1)}, u32[]{:S(2)}, u32[]{:S(2)}) collective-permute-start(bf16[1024,640]{1,0:T(8,128)(2,1)} %pad_maximum_fusion.4.rest_2_), channel_id=1, source_target_pairs={{0,6},{1,3},{2,4},{3,1},{4,2},{5,7},{6,0},{7,5},{8,14},{9,11},{10,... | collective-permute-start | bytes 3932168 | tf_op jit(solution)/shard_map/ppermute | solution.py:98
  125.2 8.0 %collective-permute-start.14 = (f32[1024]{0:T(1024)S(1)}, f32[1024]{0:T(1024)S(1)}, u32[]{:S(2)}, u32[]{:S(2)}) collective-permute-start(f32[1024]{0:T(1024)S(1)} %copy-done.10), channel_id=1, source_target_pairs={{0,1},{1,0},{2,3},{3,2},{4,5},{5,4},{6,7},{7,6},{8,9},{9,8},{10,11... | collective-permute-start | bytes 12296 | tf_op jit(solution)/shard_map/ppermute | solution.py:94
  133.2 31.3 %collective-permute-start.28 = (bf16[1024,768]{1,0:T(8,128)(2,1)}, bf16[1024,768]{1,0:T(8,128)(2,1)}, u32[]{:S(2)}, u32[]{:S(2)}) collective-permute-start(bf16[1024,768]{1,0:T(8,128)(2,1)} %pad_maximum_fusion.1.rest_2_), channel_id=1, source_target_pairs={{0,6},{1,3},{2,4},{3,1},{4,2},{5,7},{6,0},{7,5},{8,14},{9,11},{10,... | collective-permute-start | bytes 4718600 | tf_op jit(solution)/shard_map/ppermute | solution.py:98
  137.4 27.1 %collective-permute-start.29 = (bf16[1024,640]{1,0:T(8,128)(2,1)}, bf16[1024,640]{1,0:T(8,128)(2,1)}, u32[]{:S(2)}, u32[]{:S(2)}) collective-permute-start(bf16[1024,640]{1,0:T(8,128)(2,1)} %pad_maximum_fusion.8.rest_4_), channel_id=1, source_target_pairs={{0,24},{1,9},{2,26},{3,11},{4,28},{5,13},{6,30},{7,15},{8,16},{9,1... | collective-permute-start | bytes 3932168 | tf_op jit(solution)/shard_map/ppermute | solution.py:98
  139.4 25.1 %collective-permute-start.27 = (bf16[1024,640]{1,0:T(8,128)(2,1)}, bf16[1024,640]{1,0:T(8,128)(2,1)}, u32[]{:S(2)}, u32[]{:S(2)}) collective-permute-start(bf16[1024,640]{1,0:T(8,128)(2,1)} %pad_maximum_fusion.7.rest_0_), channel_id=1, source_target_pairs={{0,96},{1,33},{2,98},{3,35},{4,100},{5,37},{6,102},{7,39},{8,104},... | collective-permute-start | bytes 3932168 | tf_op jit(solution)/shard_map/ppermute | solution.py:98
  172.8 16.8 %collective-permute-start.30 = (bf16[1024,1024]{1,0:T(8,128)(2,1)S(1)}, bf16[1024,1024]{1,0:T(8,128)(2,1)S(1)}, u32[]{:S(2)}, u32[]{:S(2)}) collective-permute-start(bf16[1024,1024]{1,0:T(8,128)(2,1)S(1)} %shard_map.200), channel_id=1, source_target_pairs={{0,1},{1,0},{2,3},{3,2},{4,5},{5,4},{6,7},{7,6},{8,9},{9,8},{10,11... | collective-permute-start | bytes 6291464 | tf_op jit(solution)/shard_map/ppermute | solution.py:94
  190.4 1.2 collective-permute-start.31
  (23 other events, 137.9 us)

commit v3 on v2

--- a/solution.py
+++ b/solution.py
@@ -208,20 +208,26 @@
     for c in range(3):
         place_blocks(table, c, pieces[c], weights[c], 0, sems.at[c])
     state[...] = jnp.zeros_like(state)
-    for c in range(3):
+    for c in range(2):
         wait_part(weights[c], 0, 512, sems.at[c])
 
     def one(i, carry):
         here = pl.ds(pl.multiple_of(i * CHUNK, CHUNK), CHUNK)
-        partial_out[here, :] = attention_chunk(
-            normed[here, :], decay[here, :], mats, pair_level, gain, w_qk, w_v, w_out, state
+        mixed = attention_chunk(
+            normed[here, :], decay[here, :], mats, pair_level, gain, w_qk, w_v, state
         )
+
+        @pl.when(i == 0)
+        def _():
+            wait_part(w_out, 0, 512, sems.at[2])
+
+        partial_out[here, :] = nt_dot(mixed, w_out[...]).astype(BF)
         return carry
 
     lax.fori_loop(0, normed.shape[0] // CHUNK, one, 0)
 
 
-def attention_chunk(rows, g, mats, pair_level, gain, w_qk, w_v, w_out, state):
+def attention_chunk(rows, g, mats, pair_level, gain, w_qk, w_v, state):
     g_hi = g.astype(BF)
     g_lo = (g - g_hi.astype(F32)).astype(BF)
 
@@ -262,8 +268,7 @@
     )
     state[...] = old * jnp.exp(before[CHUNK - 1 :, :]) + tn_dot(v, k_out)
     scale = lax.rsqrt(jnp.mean(readout * readout, axis=-1, keepdims=True) + EPS)
-    mixed = (readout * scale * gain[...]).astype(BF)
-    return nt_dot(mixed, w_out[...]).astype(BF)
+    return (readout * scale * gain[...]).astype(BF)
 
 
 UP_WIDTHS = (768, 640, 640)
@@ -289,16 +294,22 @@
 
 def up_kernel(table, normed_hbm, *rest):
     squared_out, weight, normed, sems = rest[6:]
-    fetch = pltpu.make_async_copy(normed_hbm, normed, sems.at[3])
-    fetch.start()
+
+    def fetch(i):
+        here = pl.ds(pl.multiple_of(i * 256, 256), 256)
+        return pltpu.make_async_copy(normed_hbm.at[here, :], normed.at[here, :], sems.at[3 + i])
+
+    fetch(0).start()
     for c in range(3):
         at = start_of(UP_WIDTHS, c)
         place_blocks(table, 3 + c, rest[2 * c : 2 * c + 2], weight, at, sems.at[c])
+    for i in range(1, 4):
+        fetch(i).start()
     for c in range(3):
         wait_part(weight, start_of(UP_WIDTHS, c), UP_WIDTHS[c], sems.at[c])
-    fetch.wait()
 
     def one(i, carry):
+        fetch(i).wait()
         here = pl.ds(pl.multiple_of(i * 256, 256), 256)
         hidden = jnp.dot(normed[here, :], weight[...], preferred_element_type=F32)
         hidden = jnp.maximum(hidden, 0.0)
@@ -497,7 +508,7 @@
         scratch_shapes=[
             pltpu.VMEM((2048, 2048), BF),
             pltpu.VMEM((length, 2048), BF),
-            pltpu.SemaphoreType.DMA((4,)),
+            pltpu.SemaphoreType.DMA((7,)),
         ],
         name="up_proj",
         **params(8_700_000_000, 16_000_000, 24),

time: 195 us -> 194 us (level)
  no operation moved by 1% of the time
where the time goes in v3:
time: 194 us; the launch traced here: 193 us
  Pallas kernels  56.5 us (29%)
  waiting for transfers between devices  53.4 us (28%)
  starting transfers between devices  50.3 us (26%)
  local copies, waits for them, and re-layouts  17.8 us (9%)
  other arithmetic  14.4 us (7%)
    ppermute x27, waiting for transfers between devices, over_link(): return lax.ppermute(array, ALL, partner_pairs(step, chain))  52.2 us
    ppermute x5, starting transfers between devices, swap_cores(): return lax.ppermute(array, 'tp', [(0, 1), (1, 0)])  27.2 us
    ppermute x27, starting transfers between devices, over_link(): return lax.ppermute(array, ALL, partner_pairs(step, chain))  23.2 us
    pallas_call x2, Pallas kernels, down_half(): pl.pallas_call(down_kernel, in_specs=[SMEM, SMEM, VMEM] + [HBM] * 6, out_...  16.5 us
    pallas_call x1, Pallas kernels, on_device(): pl.pallas_call(attention_kernel, in_specs=[SMEM] + [VMEM] * 5 + [HBM] * 6...  15.1 us
    pallas_call x1, Pallas kernels, on_device(): pl.pallas_call(up_kernel, in_specs=[SMEM] + [HBM] * 7, out_specs=VMEM, ou...  13 us
    concatenate x25, other arithmetic, joined(): return jnp.concatenate([a, b], axis=0)  11.2 us
    unnamed x53, local copies, waits for them, and re-layouts  10.5 us
  transfers between devices with their start and end apart: 32, of which 13 were waited for; matrix products, arithmetic and copies ran while one was open for 10% of the time, Pallas kernels for 25%

profile of v3, /device:TPU:1, one launch (start us, length us, event | category | flops | bytes accessed | tf_op | source)
XLA Modules:
  0.0 193.1 jit_solution(14777724244397699308)
XLA Ops:
  2.3 3.4 %collective-permute-start.1 = (bf16[32,1536]{1,0:T(8,128)(2,1)S(1)}, bf16[32,1536]{1,0:T(8,128)(2,1)S(1)}, u32[]{:S(2)}, u32[]{:S(2)}) collective-permute-start(bf16[32,1536]{1,0:T(8,128)(2,1)S(1)} %pad_maximum_fusion.25), channel_id=1, source_target_pairs={{0,2},{1,7},{2,0},{3,5},{4,6},{5,3},{6,4},{7,1},{8,10},{9,15},{10,... | collective-permute-start | bytes 294920 | tf_op jit(solution)/shard_map/ppermute | solution.py:98
  7.7 3.0 %collective-permute-start.2 = (bf16[64,1536]{1,0:T(8,128)(2,1)S(1)}, bf16[64,1536]{1,0:T(8,128)(2,1)S(1)}, u32[]{:S(2)}, u32[]{:S(2)}) collective-permute-start(bf16[64,1536]{1,0:T(8,128)(2,1)S(1)} %pad_maximum_fusion.24), channel_id=1, source_target_pairs={{0,8},{1,25},{2,10},{3,27},{4,12},{5,29},{6,14},{7,31},{8,0},{9,17... | collective-permute-start | bytes 589832 | tf_op jit(solution)/shard_map/ppermute | solution.py:98
  11.5 2.3 %collective-permute-done.2 = bf16[64,1536]{1,0:T(8,128)(2,1)S(1)} collective-permute-done((bf16[64,1536]{1,0:T(8,128)(2,1)S(1)}, bf16[64,1536]{1,0:T(8,128)(2,1)S(1)}, u32[]{:S(2)}, u32[]{:S(2)}) %collective-permute-start.2) | collective-permute-done | bytes 196640 | tf_op jit(solution)/shard_map/ppermute | solution.py:98
  13.8 3.8 %collective-permute-start.3 = (bf16[128,1536]{1,0:T(8,128)(2,1)S(1)}, bf16[128,1536]{1,0:T(8,128)(2,1)S(1)}, u32[]{:S(2)}, u32[]{:S(2)}) collective-permute-start(bf16[128,1536]{1,0:T(8,128)(2,1)S(1)} %pad_maximum_fusion.20), channel_id=1, source_target_pairs={{0,32},{1,97},{2,34},{3,99},{4,36},{5,101},{6,38},{7,103},{8,40},{... | collective-permute-start | bytes 1179656 | tf_op jit(solution)/shard_map/ppermute | solution.py:98
  17.7 2.6 %collective-permute-start.15 = (bf16[32,4096]{1,0:T(8,128)(2,1)S(1)}, bf16[32,4096]{1,0:T(8,128)(2,1)S(1)}, u32[]{:S(2)}, u32[]{:S(2)}) collective-permute-start(bf16[32,4096]{1,0:T(8,128)(2,1)S(1)} %slice_dynamic-update-slice_fusion.1), channel_id=1, source_target_pairs={{0,2},{1,7},{2,0},{3,5},{4,6},{5,3},{6,4},{7,1},{8,10},{9,15},{10,... | collective-permute-start | bytes 786440 | tf_op jit(solution)/shard_map/ppermute | solution.py:98
  20.3 2.6 %collective-permute-done.3 = bf16[128,1536]{1,0:T(8,128)(2,1)S(1)} collective-permute-done((bf16[128,1536]{1,0:T(8,128)(2,1)S(1)}, bf16[128,1536]{1,0:T(8,128)(2,1)S(1)}, u32[]{:S(2)}, u32[]{:S(2)}) %collective-permute-start.3) | collective-permute-done | bytes 393248 | tf_op jit(solution)/shard_map/ppermute | solution.py:98
  23.0 1.2 collective-permute-done.15
  24.2 2.8 %collective-permute-start.16 = (bf16[64,4096]{1,0:T(8,128)(2,1)S(1)}, bf16[64,4096]{1,0:T(8,128)(2,1)S(1)}, u32[]{:S(2)}, u32[]{:S(2)}) collective-permute-start(bf16[64,4096]{1,0:T(8,128)(2,1)S(1)} %pad_maximum_fusion.19), channel_id=1, source_target_pairs={{0,8},{1,25},{2,10},{3,27},{4,12},{5,29},{6,14},{7,31},{8,0},{9,17... | collective-permute-start | bytes 1572872 | tf_op jit(solution)/shard_map/ppermute | solution.py:98
  27.2 6.0 %collective-permute-start = (bf16[1024,1024]{1,0:T(8,128)(2,1)S(1)}, bf16[1024,1024]{1,0:T(8,128)(2,1)}, u32[]{:S(2)}, u32[]{:S(2)}) collective-permute-start(bf16[1024,1024]{1,0:T(8,128)(2,1)S(1)} %copy-done.2), channel_id=1, source_target_pairs={{0,1},{1,0},{2,3},{3,2},{4,5},{5,4},{6,7},{7,6},{8,9},{9,8},{10,11... | collective-permute-start | bytes 6291464 | tf_op jit(solution)/shard_map/ppermute | solution.py:94
  33.7 1.7 collective-permute-done.7
  37.5 2.1 %collective-permute-start.17 = (bf16[128,4096]{1,0:T(8,128)(2,1)}, bf16[128,4096]{1,0:T(8,128)(2,1)}, u32[]{:S(2)}, u32[]{:S(2)}) collective-permute-start(bf16[128,4096]{1,0:T(8,128)(2,1)} %pad_maximum_fusion.12), channel_id=1, source_target_pairs={{0,32},{1,97},{2,34},{3,99},{4,36},{5,101},{6,38},{7,103},{8,40},{... | collective-permute-start | bytes 3145736 | tf_op jit(solution)/shard_map/ppermute | solution.py:98
  39.6 2.7 %collective-permute-done.5 = bf16[512,512]{1,0:T(8,128)(2,1)S(1)} collective-permute-done((bf16[512,512]{1,0:T(8,128)(2,1)S(1)}, bf16[512,512]{1,0:T(8,128)(2,1)S(1)}, u32[]{:S(2)}, u32[]{:S(2)}) %collective-permute-start.5) | collective-permute-done | bytes 524320 | tf_op jit(solution)/shard_map/ppermute | solution.py:98
  49.9 14.3 %collective-permute-done.17 = bf16[128,4096]{1,0:T(8,128)(2,1)} collective-permute-done((bf16[128,4096]{1,0:T(8,128)(2,1)}, bf16[128,4096]{1,0:T(8,128)(2,1)}, u32[]{:S(2)}, u32[]{:S(2)}) %collective-permute-start.17) | collective-permute-done | bytes 1048608 | tf_op jit(solution)/shard_map/ppermute | solution.py:98
  65.6 5.1 %norm.1 = (bf16[1024,2048]{1,0:T(8,128)(2,1)S(1)}, f32[1024,256]{1,0:T(8,128)S(1)}) custom-call(s32[1]{0:T(128)} %bitcast.core, bf16[1024,1024]{1,0:T(8,128)(2,1)S(1)} %copy-done.2, bf16[1024,1024]{1,0:T(8,128)(2,1)} %collective-permute-done.other, f32[1,2048]{1,0:T(1,128)S(1)} %bitcast.30, bf16[2048,16]{1,0:T(8,128)(2,1)S(1)} %copy.22.first, ...), custom_call_target="tpu_custom_call" | custom-call | flops 400000000 | bytes 10000000 | tf_op jit(solution)/shard_map/norm/pallas_call | solution.py:417
  70.8 15.1 %attention.1.mine = bf16[1024,2048]{1,0:T(8,128)(2,1)S(1)} custom-call(s32[6,64]{1,0:T(8,128)S(1)} %xor_bitcast_fusion.2.table, bf16[1024,2048]{1,0:T(8,128)(2,1)S(1)} %get-tuple-element.9.normed, f32[1024,256]{1,0:T(8,128)S(1)} %get-tuple-element.10.decay, bf16[1024,256]{1,0:T(8,128)(2,1)S(1)} %copy-done.15, s32[256,256]{1,0:T(8,128)S(1)} %copy-done.16, ...), custom_call_target="tpu_custom_call" | custom-call | flops 11000000512 | bytes 14000000 | tf_op jit(solution)/shard_map/attention/pallas_call | solution.py:447
  85.9 6.0 %collective-permute-start.13 = (bf16[1024,2048]{1,0:T(8,128)(2,1)S(1)}, bf16[1024,2048]{1,0:T(8,128)(2,1)S(1)}, u32[]{:S(2)}, u32[]{:S(2)}) collective-permute-start(bf16[1024,2048]{1,0:T(8,128)(2,1)S(1)} %attention.1.mine), channel_id=1, source_target_pairs={{0,1},{1,0},{2,3},{3,2},{4,5},{5,4},{6,7},{7,6},{8,9},{9,8},{10,11... | collective-permute-start | bytes 12582920 | tf_op jit(solution)/shard_map/ppermute | solution.py:94
  95.0 8.6 %collective-permute-done.18 = bf16[256,1408]{1,0:T(8,128)(2,1)S(1)} collective-permute-done((bf16[256,1408]{1,0:T(8,128)(2,1)S(1)}, bf16[256,1408]{1,0:T(8,128)(2,1)S(1)}, u32[]{:S(2)}, u32[]{:S(2)}) %collective-permute-start.18) | collective-permute-done | bytes 720928 | tf_op jit(solution)/shard_map/ppermute | solution.py:98
  104.4 13.3 %collective-permute-done.25 = bf16[512,1280]{1,0:T(8,128)(2,1)S(1)} collective-permute-done((bf16[512,1280]{1,0:T(8,128)(2,1)S(1)}, bf16[512,1280]{1,0:T(8,128)(2,1)S(1)}, u32[]{:S(2)}, u32[]{:S(2)}) %collective-permute-start.25) | collective-permute-done | bytes 1310752 | tf_op jit(solution)/shard_map/ppermute | solution.py:98
  118.1 3.9 %collective-permute-done.19 = bf16[512,1408]{1,0:T(8,128)(2,1)S(1)} collective-permute-done((bf16[512,1408]{1,0:T(8,128)(2,1)S(1)}, bf16[512,1408]{1,0:T(8,128)(2,1)S(1)}, u32[]{:S(2)}, u32[]{:S(2)}) %collective-permute-start.19) | collective-permute-done | bytes 1441824 | tf_op jit(solution)/shard_map/ppermute | solution.py:98
  122.0 1.2 pad_maximum_fusion.rest_0_
  125.0 6.6 %collective-permute-start.14 = (f32[1024]{0:T(1024)S(1)}, f32[1024]{0:T(1024)S(1)}, u32[]{:S(2)}, u32[]{:S(2)}) collective-permute-start(f32[1024]{0:T(1024)S(1)} %copy-done.10), channel_id=1, source_target_pairs={{0,1},{1,0},{2,3},{3,2},{4,5},{5,4},{6,7},{7,6},{8,9},{9,8},{10,11... | collective-permute-start | bytes 12296 | tf_op jit(solution)/shard_map/ppermute | solution.py:94
  131.8 1.3 pad_maximum_fusion.1.rest_2_
  133.1 1.2 pad_maximum_fusion.8.rest_4_
  137.3 2.0 %copy-done.5 = bf16[1024,2048]{1,0:T(8,128)(2,1)} copy-done((bf16[1024,2048]{1,0:T(8,128)(2,1)}, bf16[1024,2048]{1,0:T(8,128)(2,1)S(1)}, u32[]{:S(2)}) %copy-start.5) | copy-done | bytes 4194328
  139.3 2.2 %copy-done.4 = bf16[1024,2048]{1,0:T(8,128)(2,1)S(1)} copy-done((bf16[1024,2048]{1,0:T(8,128)(2,1)S(1)}, bf16[1024,2048]{1,0:T(8,128)(2,1)}, u32[]{:S(2)}) %copy-start.4) | copy-done | bytes 4194328
  141.5 2.2 %copy-done.6 = bf16[1024,2048]{1,0:T(8,128)(2,1)S(1)} copy-done((bf16[1024,2048]{1,0:T(8,128)(2,1)S(1)}, bf16[1024,2048]{1,0:T(8,128)(2,1)}, u32[]{:S(2)}) %copy-start.6) | copy-done | bytes 4194328
  143.7 6.8 %middle.1 = (bf16[1024,1024]{1,0:T(8,128)(2,1)S(1)}, bf16[1024,2048]{1,0:T(8,128)(2,1)}) custom-call(s32[1]{0:T(128)} %bitcast.core, bf16[1024,1024]{1,0:T(8,128)(2,1)S(1)} %copy-done.2, bf16[1024,1024]{1,0:T(8,128)(2,1)} %collective-permute-done.other, bf16[1024,2048]{1,0:T(8,128)(2,1)S(1)} %copy-done.4, bf16[1024,2048]{1,0:T(8,128)(2,1)S(1)} %copy-done.6, ...), custom_call_target="tpu_custom_call" | custom-call | flops 60000000 | bytes 18000000 | tf_op jit(solution)/shard_map/middle/pallas_call | solution.py:472
  150.6 13.0 %up_proj.1.squared = bf16[1024,2048]{1,0:T(8,128)(2,1)S(1)} custom-call(s32[6,64]{1,0:T(8,128)S(1)} %xor_bitcast_fusion.2.table, bf16[1024,2048]{1,0:T(8,128)(2,1)} %get-tuple-element.12.normed_hbm, bf16[1024,768]{1,0:T(8,128)(2,1)} %pad_maximum_fusion.rest_0_, bf16[1024,768]{1,0:T(8,128)(2,1)} %collective-permute-done.20.rest_1_, ...), custom_call_target="tpu_custom_call" | custom-call | flops 8700000256 | bytes 16000000 | tf_op jit(solution)/shard_map/up_proj/pallas_call | solution.py:503
  163.6 8.3 %shard_map.200 = bf16[1024,1024]{1,0:T(8,128)(2,1)S(1)} custom-call(s32[6,16]{1,0:T(8,128)S(1)} %get-tuple-element.33.places, s32[6,16]{1,0:T(8,128)S(1)} %get-tuple-element.28.targets, bf16[1024,2048]{1,0:T(8,128)(2,1)S(1)} %up_proj.1.squared, bf16[1024,640]{1,0:T(8,128)(2,1)} %pad_maximum_fusion.7.rest_0_, ...), custom_call_target="tpu_custom_call" | custom-call | flops 4300000256 | bytes 10000000 | tf_op jit(solution)/shard_map/pallas_call | solution.py:518
  171.8 8.6 %collective-permute-start.30 = (bf16[1024,1024]{1,0:T(8,128)(2,1)S(1)}, bf16[1024,1024]{1,0:T(8,128)(2,1)S(1)}, u32[]{:S(2)}, u32[]{:S(2)}) collective-permute-start(bf16[1024,1024]{1,0:T(8,128)(2,1)S(1)} %shard_map.200), channel_id=1, source_target_pairs={{0,1},{1,0},{2,3},{3,2},{4,5},{5,4},{6,7},{7,6},{8,9},{9,8},{10,11... | collective-permute-start | bytes 6291464 | tf_op jit(solution)/shard_map/ppermute | solution.py:94
  180.4 8.2 %shard_map.199 = bf16[1024,1024]{1,0:T(8,128)(2,1)S(1)} custom-call(s32[6,16]{1,0:T(8,128)S(1)} %get-tuple-element.34.places, s32[6,16]{1,0:T(8,128)S(1)} %get-tuple-element.27.targets, bf16[1024,2048]{1,0:T(8,128)(2,1)S(1)} %up_proj.1.squared, bf16[1024,640]{1,0:T(8,128)(2,1)} %pad_maximum_fusion.7.rest_0_, ...), custom_call_target="tpu_custom_call" | custom-call | flops 4300000256 | bytes 10000000 | tf_op jit(solution)/shard_map/pallas_call | solution.py:518
  190.7 2.4 %add_convert_fusion = bf16[1024,1024]{1,0:T(8,128)(2,1)} fusion(bf16[1024,1024]{1,0:T(8,128)(2,1)S(1)} %get-tuple-element.11, bf16[1024,1024]{1,0:T(8,128)(2,1)S(1)} %collective-permute-done.30, bf16[1024,1024]{1,0:T(8,128)(2,1)S(1)} %shard_map.199, f32[1024]{0:T(1024)S(1)} %copy-done.18, f32[1024]{0:T(1024)S(1)} %fusion.2), kind=kLoop, calls=%fused_computation | loop fusion | flops 8388608 | bytes 8396800 | tf_op jit(solution)/shard_map/convert_element_type | solution.py:539
  (143 shorter events, 28.1 us)
Async XLA Ops:
  2.3 5.4 %collective-permute-start.1 = (bf16[32,1536]{1,0:T(8,128)(2,1)S(1)}, bf16[32,1536]{1,0:T(8,128)(2,1)S(1)}, u32[]{:S(2)}, u32[]{:S(2)}) collective-permute-start(bf16[32,1536]{1,0:T(8,128)(2,1)S(1)} %pad_maximum_fusion.25), channel_id=1, source_target_pairs={{0,2},{1,7},{2,0},{3,5},{4,6},{5,3},{6,4},{7,1},{8,10},{9,15},{10,... | collective-permute-start | bytes 294920 | tf_op jit(solution)/shard_map/ppermute | solution.py:98
  7.7 6.1 %collective-permute-start.2 = (bf16[64,1536]{1,0:T(8,128)(2,1)S(1)}, bf16[64,1536]{1,0:T(8,128)(2,1)S(1)}, u32[]{:S(2)}, u32[]{:S(2)}) collective-permute-start(bf16[64,1536]{1,0:T(8,128)(2,1)S(1)} %pad_maximum_fusion.24), channel_id=1, source_target_pairs={{0,8},{1,25},{2,10},{3,27},{4,12},{5,29},{6,14},{7,31},{8,0},{9,17... | collective-permute-start | bytes 589832 | tf_op jit(solution)/shard_map/ppermute | solution.py:98
  13.8 9.0 %collective-permute-start.3 = (bf16[128,1536]{1,0:T(8,128)(2,1)S(1)}, bf16[128,1536]{1,0:T(8,128)(2,1)S(1)}, u32[]{:S(2)}, u32[]{:S(2)}) collective-permute-start(bf16[128,1536]{1,0:T(8,128)(2,1)S(1)} %pad_maximum_fusion.20), channel_id=1, source_target_pairs={{0,32},{1,97},{2,34},{3,99},{4,36},{5,101},{6,38},{7,103},{8,40},{... | collective-permute-start | bytes 1179656 | tf_op jit(solution)/shard_map/ppermute | solution.py:98
  17.7 6.5 %collective-permute-start.15 = (bf16[32,4096]{1,0:T(8,128)(2,1)S(1)}, bf16[32,4096]{1,0:T(8,128)(2,1)S(1)}, u32[]{:S(2)}, u32[]{:S(2)}) collective-permute-start(bf16[32,4096]{1,0:T(8,128)(2,1)S(1)} %slice_dynamic-update-slice_fusion.1), channel_id=1, source_target_pairs={{0,2},{1,7},{2,0},{3,5},{4,6},{5,3},{6,4},{7,1},{8,10},{9,15},{10,... | collective-permute-start | bytes 786440 | tf_op jit(solution)/shard_map/ppermute | solution.py:98
  22.9 10.3 %collective-permute-start.4 = (bf16[256,512]{1,0:T(8,128)(2,1)S(1)}, bf16[256,512]{1,0:T(8,128)(2,1)S(1)}, u32[]{:S(2)}, u32[]{:S(2)}) collective-permute-start(bf16[256,512]{1,0:T(8,128)(2,1)S(1)} %pad_maximum_fusion.21), channel_id=1, source_target_pairs={{0,6},{1,3},{2,4},{3,1},{4,2},{5,7},{6,0},{7,5},{8,14},{9,11},{10,... | collective-permute-start | bytes 786440 | tf_op jit(solution)/shard_map/ppermute | solution.py:98
  24.2 12.2 %collective-permute-start.16 = (bf16[64,4096]{1,0:T(8,128)(2,1)S(1)}, bf16[64,4096]{1,0:T(8,128)(2,1)S(1)}, u32[]{:S(2)}, u32[]{:S(2)}) collective-permute-start(bf16[64,4096]{1,0:T(8,128)(2,1)S(1)} %pad_maximum_fusion.19), channel_id=1, source_target_pairs={{0,8},{1,25},{2,10},{3,27},{4,12},{5,29},{6,14},{7,31},{8,0},{9,17... | collective-permute-start | bytes 1572872 | tf_op jit(solution)/shard_map/ppermute | solution.py:98
  27.0 8.4 %collective-permute-start.7 = (bf16[256,512]{1,0:T(8,128)(2,1)S(1)}, bf16[256,512]{1,0:T(8,128)(2,1)S(1)}, u32[]{:S(2)}, u32[]{:S(2)}) collective-permute-start(bf16[256,512]{1,0:T(8,128)(2,1)S(1)} %pad_maximum_fusion.22), channel_id=1, source_target_pairs={{0,24},{1,9},{2,26},{3,11},{4,28},{5,13},{6,30},{7,15},{8,16},{9,1... | collective-permute-start | bytes 786440 | tf_op jit(solution)/shard_map/ppermute | solution.py:98
  27.1 8.4 %collective-permute-start.10 = (bf16[256,512]{1,0:T(8,128)(2,1)S(1)}, bf16[256,512]{1,0:T(8,128)(2,1)S(1)}, u32[]{:S(2)}, u32[]{:S(2)}) collective-permute-start(bf16[256,512]{1,0:T(8,128)(2,1)S(1)} %pad_maximum_fusion.23), channel_id=1, source_target_pairs={{0,96},{1,33},{2,98},{3,35},{4,100},{5,37},{6,102},{7,39},{8,104},... | collective-permute-start | bytes 786440 | tf_op jit(solution)/shard_map/ppermute | solution.py:98
  27.2 38.4 %collective-permute-start = (bf16[1024,1024]{1,0:T(8,128)(2,1)S(1)}, bf16[1024,1024]{1,0:T(8,128)(2,1)}, u32[]{:S(2)}, u32[]{:S(2)}) collective-permute-start(bf16[1024,1024]{1,0:T(8,128)(2,1)S(1)} %copy-done.2), channel_id=1, source_target_pairs={{0,1},{1,0},{2,3},{3,2},{4,5},{5,4},{6,7},{7,6},{8,9},{9,8},{10,11... | collective-permute-start | bytes 6291464 | tf_op jit(solution)/shard_map/ppermute | solution.py:94
  33.2 9.2 %collective-permute-start.5 = (bf16[512,512]{1,0:T(8,128)(2,1)S(1)}, bf16[512,512]{1,0:T(8,128)(2,1)S(1)}, u32[]{:S(2)}, u32[]{:S(2)}) collective-permute-start(bf16[512,512]{1,0:T(8,128)(2,1)S(1)} %pad_maximum_fusion.16), channel_id=1, source_target_pairs={{0,24},{1,9},{2,26},{3,11},{4,28},{5,13},{6,30},{7,15},{8,16},{9,1... | collective-permute-start | bytes 1572872 | tf_op jit(solution)/shard_map/ppermute | solution.py:98
  35.4 9.0 %collective-permute-start.8 = (bf16[512,512]{1,0:T(8,128)(2,1)S(1)}, bf16[512,512]{1,0:T(8,128)(2,1)S(1)}, u32[]{:S(2)}, u32[]{:S(2)}) collective-permute-start(bf16[512,512]{1,0:T(8,128)(2,1)S(1)} %pad_maximum_fusion.17), channel_id=1, source_target_pairs={{0,96},{1,33},{2,98},{3,35},{4,100},{5,37},{6,102},{7,39},{8,104},... | collective-permute-start | bytes 1572872 | tf_op jit(solution)/shard_map/ppermute | solution.py:98
  35.6 10.5 %collective-permute-start.11 = (bf16[512,512]{1,0:T(8,128)(2,1)S(1)}, bf16[512,512]{1,0:T(8,128)(2,1)S(1)}, u32[]{:S(2)}, u32[]{:S(2)}) collective-permute-start(bf16[512,512]{1,0:T(8,128)(2,1)S(1)} %pad_maximum_fusion.18), channel_id=1, source_target_pairs={{0,6},{1,3},{2,4},{3,1},{4,2},{5,7},{6,0},{7,5},{8,14},{9,11},{10,... | collective-permute-start | bytes 1572872 | tf_op jit(solution)/shard_map/ppermute | solution.py:98
  37.5 26.7 %collective-permute-start.17 = (bf16[128,4096]{1,0:T(8,128)(2,1)}, bf16[128,4096]{1,0:T(8,128)(2,1)}, u32[]{:S(2)}, u32[]{:S(2)}) collective-permute-start(bf16[128,4096]{1,0:T(8,128)(2,1)} %pad_maximum_fusion.12), channel_id=1, source_target_pairs={{0,32},{1,97},{2,34},{3,99},{4,36},{5,101},{6,38},{7,103},{8,40},{... | collective-permute-start | bytes 3145736 | tf_op jit(solution)/shard_map/ppermute | solution.py:98
  43.4 27.3 %collective-permute-start.6 = (bf16[1024,512]{1,0:T(8,128)(2,1)}, bf16[1024,512]{1,0:T(8,128)(2,1)}, u32[]{:S(2)}, u32[]{:S(2)}) collective-permute-start(bf16[1024,512]{1,0:T(8,128)(2,1)} %pad_maximum_fusion.9.rest_0_), channel_id=1, source_target_pairs={{0,96},{1,33},{2,98},{3,35},{4,100},{5,37},{6,102},{7,39},{8,104},... | collective-permute-start | bytes 3145736 | tf_op jit(solution)/shard_map/ppermute | solution.py:98
  45.5 25.2 %collective-permute-start.9 = (bf16[1024,512]{1,0:T(8,128)(2,1)}, bf16[1024,512]{1,0:T(8,128)(2,1)}, u32[]{:S(2)}, u32[]{:S(2)}) collective-permute-start(bf16[1024,512]{1,0:T(8,128)(2,1)} %pad_maximum_fusion.10.rest_2_), channel_id=1, source_target_pairs={{0,6},{1,3},{2,4},{3,1},{4,2},{5,7},{6,0},{7,5},{8,14},{9,11},{10,... | collective-permute-start | bytes 3145736 | tf_op jit(solution)/shard_map/ppermute | solution.py:98
  47.1 23.6 %collective-permute-start.12 = (bf16[1024,512]{1,0:T(8,128)(2,1)}, bf16[1024,512]{1,0:T(8,128)(2,1)}, u32[]{:S(2)}, u32[]{:S(2)}) collective-permute-start(bf16[1024,512]{1,0:T(8,128)(2,1)} %pad_maximum_fusion.11.rest_4_), channel_id=1, source_target_pairs={{0,24},{1,9},{2,26},{3,11},{4,28},{5,13},{6,30},{7,15},{8,16},{9,1... | collective-permute-start | bytes 3145736 | tf_op jit(solution)/shard_map/ppermute | solution.py:98
  65.3 29.1 %collective-permute-start.24 = (bf16[256,1280]{1,0:T(8,128)(2,1)S(1)}, bf16[256,1280]{1,0:T(8,128)(2,1)S(1)}, u32[]{:S(2)}, u32[]{:S(2)}) collective-permute-start(bf16[256,1280]{1,0:T(8,128)(2,1)S(1)} %pad_maximum_fusion.15), channel_id=1, source_target_pairs={{0,96},{1,33},{2,98},{3,35},{4,100},{5,37},{6,102},{7,39},{8,104},... | collective-permute-start | bytes 1966088 | tf_op jit(solution)/shard_map/ppermute | solution.py:98
  85.9 51.3 %collective-permute-start.13 = (bf16[1024,2048]{1,0:T(8,128)(2,1)S(1)}, bf16[1024,2048]{1,0:T(8,128)(2,1)S(1)}, u32[]{:S(2)}, u32[]{:S(2)}) collective-permute-start(bf16[1024,2048]{1,0:T(8,128)(2,1)S(1)} %attention.1.mine), channel_id=1, source_target_pairs={{0,1},{1,0},{2,3},{3,2},{4,5},{5,4},{6,7},{7,6},{8,9},{9,8},{10,11... | collective-permute-start | bytes 12582920 | tf_op jit(solution)/shard_map/ppermute | solution.py:94
  93.1 10.5 %collective-permute-start.18 = (bf16[256,1408]{1,0:T(8,128)(2,1)S(1)}, bf16[256,1408]{1,0:T(8,128)(2,1)S(1)}, u32[]{:S(2)}, u32[]{:S(2)}) collective-permute-start(bf16[256,1408]{1,0:T(8,128)(2,1)S(1)} %pad_maximum_fusion.13), channel_id=1, source_target_pairs={{0,6},{1,3},{2,4},{3,1},{4,2},{5,7},{6,0},{7,5},{8,14},{9,11},{10,... | collective-permute-start | bytes 2162696 | tf_op jit(solution)/shard_map/ppermute | solution.py:98
  93.3 10.6 %collective-permute-start.21 = (bf16[256,1408]{1,0:T(8,128)(2,1)S(1)}, bf16[256,1408]{1,0:T(8,128)(2,1)S(1)}, u32[]{:S(2)}, u32[]{:S(2)}) collective-permute-start(bf16[256,1408]{1,0:T(8,128)(2,1)S(1)} %pad_maximum_fusion.14), channel_id=1, source_target_pairs={{0,24},{1,9},{2,26},{3,11},{4,28},{5,13},{6,30},{7,15},{8,16},{9,1... | collective-permute-start | bytes 2162696 | tf_op jit(solution)/shard_map/ppermute | solution.py:98
  94.5 23.2 %collective-permute-start.25 = (bf16[512,1280]{1,0:T(8,128)(2,1)S(1)}, bf16[512,1280]{1,0:T(8,128)(2,1)S(1)}, u32[]{:S(2)}, u32[]{:S(2)}) collective-permute-start(bf16[512,1280]{1,0:T(8,128)(2,1)S(1)} %pad_maximum_fusion.5), channel_id=1, source_target_pairs={{0,6},{1,3},{2,4},{3,1},{4,2},{5,7},{6,0},{7,5},{8,14},{9,11},{10,... | collective-permute-start | bytes 3932168 | tf_op jit(solution)/shard_map/ppermute | solution.py:98
  103.7 18.2 %collective-permute-start.19 = (bf16[512,1408]{1,0:T(8,128)(2,1)S(1)}, bf16[512,1408]{1,0:T(8,128)(2,1)S(1)}, u32[]{:S(2)}, u32[]{:S(2)}) collective-permute-start(bf16[512,1408]{1,0:T(8,128)(2,1)S(1)} %pad_maximum_fusion.2), channel_id=1, source_target_pairs={{0,24},{1,9},{2,26},{3,11},{4,28},{5,13},{6,30},{7,15},{8,16},{9,1... | collective-permute-start | bytes 4325384 | tf_op jit(solution)/shard_map/ppermute | solution.py:98
  104.0 19.4 %collective-permute-start.22 = (bf16[512,1408]{1,0:T(8,128)(2,1)S(1)}, bf16[512,1408]{1,0:T(8,128)(2,1)S(1)}, u32[]{:S(2)}, u32[]{:S(2)}) collective-permute-start(bf16[512,1408]{1,0:T(8,128)(2,1)S(1)} %pad_maximum_fusion.3), channel_id=1, source_target_pairs={{0,96},{1,33},{2,98},{3,35},{4,100},{5,37},{6,102},{7,39},{8,104},... | collective-permute-start | bytes 4325384 | tf_op jit(solution)/shard_map/ppermute | solution.py:98
  117.9 18.2 %collective-permute-start.26 = (bf16[1024,640]{1,0:T(8,128)(2,1)S(1)}, bf16[1024,640]{1,0:T(8,128)(2,1)S(1)}, u32[]{:S(2)}, u32[]{:S(2)}) collective-permute-start(bf16[1024,640]{1,0:T(8,128)(2,1)S(1)} %pad_maximum_fusion.6.rest_4_), channel_id=1, source_target_pairs={{0,24},{1,9},{2,26},{3,11},{4,28},{5,13},{6,30},{7,15},{8,16},{9,1... | collective-permute-start | bytes 3932168 | tf_op jit(solution)/shard_map/ppermute | solution.py:98
  123.3 27.3 %collective-permute-start.20 = (bf16[1024,768]{1,0:T(8,128)(2,1)}, bf16[1024,768]{1,0:T(8,128)(2,1)}, u32[]{:S(2)}, u32[]{:S(2)}) collective-permute-start(bf16[1024,768]{1,0:T(8,128)(2,1)} %pad_maximum_fusion.rest_0_), channel_id=1, source_target_pairs={{0,96},{1,33},{2,98},{3,35},{4,100},{5,37},{6,102},{7,39},{8,104},... | collective-permute-start | bytes 4718600 | tf_op jit(solution)/shard_map/ppermute | solution.py:98
  124.6 25.9 %collective-permute-start.23 = (bf16[1024,640]{1,0:T(8,128)(2,1)}, bf16[1024,640]{1,0:T(8,128)(2,1)}, u32[]{:S(2)}, u32[]{:S(2)}) collective-permute-start(bf16[1024,640]{1,0:T(8,128)(2,1)} %pad_maximum_fusion.4.rest_2_), channel_id=1, source_target_pairs={{0,6},{1,3},{2,4},{3,1},{4,2},{5,7},{6,0},{7,5},{8,14},{9,11},{10,... | collective-permute-start | bytes 3932168 | tf_op jit(solution)/shard_map/ppermute | solution.py:98
  125.0 8.0 %collective-permute-start.14 = (f32[1024]{0:T(1024)S(1)}, f32[1024]{0:T(1024)S(1)}, u32[]{:S(2)}, u32[]{:S(2)}) collective-permute-start(f32[1024]{0:T(1024)S(1)} %copy-done.10), channel_id=1, source_target_pairs={{0,1},{1,0},{2,3},{3,2},{4,5},{5,4},{6,7},{7,6},{8,9},{9,8},{10,11... | collective-permute-start | bytes 12296 | tf_op jit(solution)/shard_map/ppermute | solution.py:94
  133.1 30.5 %collective-permute-start.28 = (bf16[1024,768]{1,0:T(8,128)(2,1)}, bf16[1024,768]{1,0:T(8,128)(2,1)}, u32[]{:S(2)}, u32[]{:S(2)}) collective-permute-start(bf16[1024,768]{1,0:T(8,128)(2,1)} %pad_maximum_fusion.1.rest_2_), channel_id=1, source_target_pairs={{0,6},{1,3},{2,4},{3,1},{4,2},{5,7},{6,0},{7,5},{8,14},{9,11},{10,... | collective-permute-start | bytes 4718600 | tf_op jit(solution)/shard_map/ppermute | solution.py:98
  137.2 26.3 %collective-permute-start.29 = (bf16[1024,640]{1,0:T(8,128)(2,1)}, bf16[1024,640]{1,0:T(8,128)(2,1)}, u32[]{:S(2)}, u32[]{:S(2)}) collective-permute-start(bf16[1024,640]{1,0:T(8,128)(2,1)} %pad_maximum_fusion.8.rest_4_), channel_id=1, source_target_pairs={{0,24},{1,9},{2,26},{3,11},{4,28},{5,13},{6,30},{7,15},{8,16},{9,1... | collective-permute-start | bytes 3932168 | tf_op jit(solution)/shard_map/ppermute | solution.py:98
  139.3 24.3 %collective-permute-start.27 = (bf16[1024,640]{1,0:T(8,128)(2,1)}, bf16[1024,640]{1,0:T(8,128)(2,1)}, u32[]{:S(2)}, u32[]{:S(2)}) collective-permute-start(bf16[1024,640]{1,0:T(8,128)(2,1)} %pad_maximum_fusion.7.rest_0_), channel_id=1, source_target_pairs={{0,96},{1,33},{2,98},{3,35},{4,100},{5,37},{6,102},{7,39},{8,104},... | collective-permute-start | bytes 3932168 | tf_op jit(solution)/shard_map/ppermute | solution.py:98
  171.8 16.8 %collective-permute-start.30 = (bf16[1024,1024]{1,0:T(8,128)(2,1)S(1)}, bf16[1024,1024]{1,0:T(8,128)(2,1)S(1)}, u32[]{:S(2)}, u32[]{:S(2)}) collective-permute-start(bf16[1024,1024]{1,0:T(8,128)(2,1)S(1)} %shard_map.200), channel_id=1, source_target_pairs={{0,1},{1,0},{2,3},{3,2},{4,5},{5,4},{6,7},{7,6},{8,9},{9,8},{10,11... | collective-permute-start | bytes 6291464 | tf_op jit(solution)/shard_map/ppermute | solution.py:94
  189.5 1.2 collective-permute-start.31
  (23 other events, 138.0 us)
